TPU v7x, 512 devices: a whole 4x4x16 slice. The times are simulated.
512 devices in a mesh: sp: 16 (over z), fs: 4 (over y), tp: 8 (over x, core).
Axes of the slice: x: 4, y: 4, z: 16, core: 2. Of those that a mesh axis runs over, the one named last changes fastest.
Arguments:
- tokens: bfloat16 [4, 16384, 2048], P('fs', ('sp', 'tp')), may hold values from -6 to 6
- norm_gain: float32 [2048], replicated, may hold values from 0.1 to 1.9
- w_gate: bfloat16 [2048, 1024], P(('sp', 'fs'), 'tp'), may hold values from -0.125 to 0.125
- w_value: bfloat16 [2048, 1024], P(('sp', 'fs'), 'tp'), may hold values from -0.125 to 0.125
- w_bkey: bfloat16 [2048, 1024], P(('sp', 'fs'), 'tp'), may hold values from -0.125 to 0.125
- w_query: bfloat16 [2048, 1024], P(('sp', 'fs'), 'tp'), may hold values from -0.125 to 0.125
- w_pool_in: bfloat16 [2048, 1024], P(('sp', 'fs'), 'tp'), may hold values from -0.125 to 0.125
- w_step: bfloat16 [2048, 2, 16], replicated, may hold values from -0.125 to 0.125
- step_bias: float32 [2, 16], replicated, may hold values from -1 to 1
- decay_rate: float32 [2, 16], replicated, may hold values from 1.2207031e-06 to 0.06
- decay_shift: float32 [4, 16, 2, 16384], P('fs', 'tp', None, 'sp'), may hold values from 0 to 2.2
- conv_value: bfloat16 [5, 1024], replicated, may hold values from -2.5 to 2.5
- conv_bkey: bfloat16 [5, 1024], replicated, may hold values from -2.5 to 2.5
- conv_query: bfloat16 [5, 1024], replicated, may hold values from -2.5 to 2.5
- mix_gain: float32 [1024], replicated, may hold values from 0.1 to 1.9
- pool_mix: bfloat16 [8, 128, 128], replicated, may hold values from -0.5 to 0.5
- pool_gain: float32 [1024], replicated, may hold values from 0.1 to 1.9
- w_out_ssd: bfloat16 [1024, 2048], P('tp', ('sp', 'fs')), may hold values from -0.125 to 0.125
- w_out_pool: bfloat16 [1024, 2048], P('tp', ('sp', 'fs')), may hold values from -0.125 to 0.125
Outputs:
- mixed: bfloat16 [4, 16384, 2048], P('fs', ('sp', 'tp'))
All inputs are finite; a program needn't handle non-finite values.
Results may differ from a plain program's by a relative error of at most 0.014.
Values may be sent and summed in bfloat16 or wider, within the bound.
A program may use at most 128 MiB of HBM per device.

v0:
```python
import jax
import jax.numpy as jnp
from jax import lax
from jax.sharding import PartitionSpec as P

HEAD_DIM = 64
DUALITY_HEADS = 16
GROUPS = 8
STATE = 128
CONV_WIDTH = 5
POOL_GROUPS = 8
POOL_DIM = 128
SPAN = 128
REACH = 8
D_SSM = 1024


EPSILON = 1e-06
HIGHEST = lax.Precision.HIGHEST
WINDOWS = (2, 4, 8, 16)


def turned_gather(arrays, axis, dims):
    turned = [jnp.moveaxis(a, dim, 0) for a, dim in zip(arrays, dims)]
    both = jnp.concatenate([t.reshape(len(t), -1) for t in turned], axis=1)
    out, at, gathered = (lax.all_gather(both, axis, axis=0, tiled=True), 0, [])
    for t, dim in zip(turned, dims):
        slab = out[:, at : at + t[0].size].reshape(-1, *t.shape[1:])
        gathered.append(jnp.moveaxis(slab, 0, dim))
        at += t[0].size
    return tuple(gathered)


def padded_2(cells, sides, width):
    for axis, dim in sides:
        count = lax.axis_size(axis)
        ends = count - 1
        head = lax.slice_in_dim(cells, 0, width, axis=dim)
        tail = lax.slice_in_dim(cells, cells.shape[dim] - width, cells.shape[dim], axis=dim)
        cells = jnp.concatenate(
            [
                lax.ppermute(tail, axis, [(i, (i + 1) % count) for i in range(ends)]),
                cells,
                lax.ppermute(head, axis, [((i + 1) % count, i) for i in range(ends)]),
            ],
            axis=dim,
        )
    return cells


def from_everyone(x, axis):
    length = lax.axis_size(axis)
    return lax.all_to_all(jnp.broadcast_to(x[None], (length, *x.shape)), axis, 0, 0, tiled=True)


def gathered_once(x, axis):
    leaves = jax.tree.leaves(x)
    sequence = sorted(range(len(leaves)), key=lambda k: -leaves[k].size)
    width = (1, *leaves[sequence[0]].shape)[-1]
    lines = [
        jnp.pad(leaves[k].reshape(-1), (0, -leaves[k].size % width)).reshape(-1, width)
        for k in sequence
    ]
    both, at, found = (from_everyone(jnp.concatenate(lines), axis), 0, {})
    for k, line in zip(sequence, lines):
        slab = both[:, at : at + len(line)].reshape(len(both), -1)
        found[k] = slab[:, : leaves[k].size].reshape(-1, *leaves[k].shape)
        at += len(line)
    numbers = iter(range(len(leaves)))
    return jax.tree.map(lambda _: found[next(numbers)], x)


def joined_by_halves(pieces, combine):
    while len(jax.tree.leaves(pieces)[0]) > 1:
        pieces = jax.vmap(combine)(
            *(jax.tree.map(lambda part: part[side::2], pieces) for side in (0, 1))
        )
    return jax.tree.map(lambda part: part[0], pieces)


def carried_in(x, axis, combine, identity, reverse):
    length, here = (lax.axis_size(axis), lax.axis_index(axis))
    passed = jnp.arange(length) > here if reverse else jnp.arange(length) < here

    def kept(part, zero, own):
        part = jnp.where(
            passed.reshape(-1, *(1 for _ in own.shape)),
            part.astype(own.dtype),
            jnp.asarray(zero, own.dtype),
        )
        return part[::-1] if reverse else part

    pieces = gathered_once(
        jax.tree.map(lambda part, kind: part.astype(kind), x, (jnp.bfloat16, jnp.bfloat16)), axis
    )
    return joined_by_halves(jax.tree.map(kept, pieces, identity, x), combine)


def over_copies(x, axis):
    return from_everyone(x, axis).sum(axis=0)


def cut_along(x, dim, length):
    before, after = (x.shape[:dim], x.shape[dim + 1 :])
    return jnp.moveaxis(x.reshape(*before, length, -1, *after), dim, 0)


def sent_and_summed(x, axis, dim):
    tiles = cut_along(x, dim, lax.axis_size(axis))
    arrived = lax.all_to_all(tiles, axis, split_axis=0, concat_axis=0, tiled=True)
    return arrived.astype(jnp.float32).sum(axis=0)


def local_pass(values, bkeys, queries, steps, logs):
    length, heads, head_width = values.shape
    groups, state_width = (bkeys.shape[1], bkeys.shape[2])
    per_group = heads // groups
    blocks = length // SPAN
    weighted = (values * jnp.transpose(steps)[:, :, None]).reshape(
        blocks, SPAN, groups, per_group, head_width
    )
    key_blocks = bkeys.reshape(blocks, SPAN, groups, state_width)
    query_blocks = queries.reshape(blocks, SPAN, groups, state_width)
    inner = jnp.cumsum(logs.reshape(heads, blocks, SPAN), axis=-1)
    lower = jnp.tril(jnp.ones((SPAN, SPAN), dtype=bool))
    within = jnp.exp(jnp.where(lower, inner[..., :, None] - inner[..., None, :], -jnp.inf))
    within = within.reshape(groups, per_group, blocks, SPAN, SPAN)
    scores = jnp.einsum("clgn,csgn->cgls", query_blocks, key_blocks, precision=HIGHEST)
    diagonal = jnp.einsum("cgls,gkcls,csgkp->clgkp", scores, within, weighted, precision=HIGHEST)
    tails = jnp.exp(inner[..., -1:] - inner).reshape(groups, per_group, blocks, SPAN)
    ends = jnp.einsum("clgn,gkcl,clgkp->cgkpn", key_blocks, tails, weighted, precision=HIGHEST)
    totals = inner[..., -1]
    upto = jnp.cumsum(totals, axis=-1)
    before = upto - totals
    block_ids = jnp.arange(blocks, dtype=jnp.int32)
    earlier = block_ids[None, :] < block_ids[:, None]
    between = jnp.exp(jnp.where(earlier[None], before[:, :, None] - upto[:, None, :], -jnp.inf))
    between = between.reshape(groups, per_group, blocks, blocks)
    prior = jnp.einsum("gkcj,jgkpn->cgkpn", between, ends, precision=HIGHEST)
    reach = jnp.exp(inner).reshape(groups, per_group, blocks, SPAN)
    offdiag = jnp.einsum("clgn,cgkpn,gkcl->clgkp", query_blocks, prior, reach, precision=HIGHEST)
    outputs = (diagonal + offdiag).reshape(length, heads, head_width)
    last_weight = jnp.exp(upto[:, -1:] - upto).reshape(groups, per_group, blocks)
    final = jnp.einsum("gkj,jgkpn->gkpn", last_weight, ends, precision=HIGHEST)
    final = final.reshape(heads, head_width, state_width)
    token_position = (before[:, :, None] + inner).reshape(heads, length)
    return (outputs, final, upto[:, -1], token_position)


def apply_carry(queries, incoming, token_position):
    length, groups, state_width = queries.shape
    heads, head_width = (incoming.shape[0], incoming.shape[1])
    per_group = heads // groups
    reach = jnp.exp(token_position).reshape(groups, per_group, length)
    carried = jnp.einsum(
        "lgn,gkpn,gkl->lgkp",
        queries,
        incoming.reshape(groups, per_group, head_width, state_width),
        reach,
        precision=HIGHEST,
    )
    return carried.reshape(length, heads, head_width)


def chain_combine(earlier, later):
    return (earlier[0] + later[0], jnp.exp(later[0])[:, None, None] * earlier[1] + later[1])


def local(
    tokens,
    norm_gain,
    w_gate,
    w_value,
    w_bkey,
    w_query,
    w_pool_in,
    w_step,
    step_bias,
    decay_rate,
    decay_shift,
    conv_value,
    conv_bkey,
    conv_query,
    mix_gain,
    pool_mix,
    pool_gain,
    w_out_ssd,
    w_out_pool,
):
    tp_count = lax.axis_size("tp")
    sp_count = lax.axis_size("sp")
    tp_rank = lax.axis_index("tp")
    sp_rank = lax.axis_index("sp")
    heads_dev = DUALITY_HEADS // tp_count
    groups_dev = GROUPS // tp_count
    pools_dev = POOL_GROUPS // tp_count
    width_ssd = heads_dev * HEAD_DIM
    width_key = groups_dev * STATE
    width_pool = pools_dev * POOL_DIM
    gathered = turned_gather(
        (w_gate, w_value, w_bkey, w_query, w_pool_in, w_out_ssd, w_out_pool),
        ("sp", "fs"),
        (0, 0, 0, 0, 0, 1, 1),
    )
    step_cols = lax.dynamic_slice_in_dim(w_step, tp_rank * heads_dev, heads_dev, 2)
    step_cols = step_cols.reshape(w_step.shape[0], 2 * heads_dev)
    combined = jnp.concatenate(
        [gathered[0], gathered[1], gathered[2], gathered[3], gathered[4], step_cols], axis=1
    )
    widened = lax.all_gather(tokens, "tp", axis=1, tiled=True)[0].astype(jnp.float32)
    scaling = lax.rsqrt(jnp.mean(widened * widened, axis=-1, keepdims=True) + EPSILON)
    normed = (widened * scaling * norm_gain).astype(jnp.bfloat16)
    projected = jnp.dot(normed, combined, preferred_element_type=jnp.float32)[None][0]
    length = projected.shape[0]
    stored_cols = 2 * width_ssd + 2 * width_key + width_pool
    stored = projected[:, :stored_cols].astype(jnp.bfloat16)
    raw_steps = projected[:, stored_cols:]
    padded = padded_2(stored[:, width_ssd:], (("sp", 0),), REACH)
    conv_cols = width_ssd + 2 * width_key
    taps = jnp.concatenate(
        [
            lax.dynamic_slice_in_dim(conv_value, tp_rank * width_ssd, width_ssd, 1),
            lax.dynamic_slice_in_dim(conv_bkey, tp_rank * width_key, width_key, 1),
            lax.dynamic_slice_in_dim(conv_query, tp_rank * width_key, width_key, 1),
        ],
        axis=1,
    ).astype(jnp.float32)
    margin = CONV_WIDTH // 2
    convolved = jnp.zeros((length, conv_cols), jnp.float32)
    for offset in range(CONV_WIDTH):
        begin = REACH - margin + offset
        convolved = (
            convolved
            + padded[begin : begin + length, :conv_cols].astype(jnp.float32) * taps[offset]
        )
    activated = jax.nn.silu(convolved)
    values = activated[:, :width_ssd].reshape(length, heads_dev, HEAD_DIM)
    bkeys = activated[:, width_ssd : width_ssd + width_key].reshape(length, groups_dev, STATE)
    queries = activated[:, width_ssd + width_key :].reshape(length, groups_dev, STATE)
    bias_dev = lax.dynamic_slice_in_dim(step_bias, tp_rank * heads_dev, heads_dev, 1)
    rate_dev = lax.dynamic_slice_in_dim(decay_rate, tp_rank * heads_dev, heads_dev, 1)
    steps = jax.nn.softplus(raw_steps.reshape(length, 2, heads_dev) + bias_dev).transpose(1, 2, 0)
    logs = -rate_dev[:, :, None] * steps - decay_shift[0].transpose(1, 0, 2)
    forward_out, forward_final, forward_total, forward_pos = local_pass(
        values, bkeys, queries, steps[0], logs[0]
    )
    backward_out, backward_final, backward_total, backward_pos = local_pass(
        values[::-1], bkeys[::-1], queries[::-1], steps[1][:, ::-1], logs[1][:, ::-1]
    )
    identity = (jnp.zeros_like(forward_total), jnp.zeros_like(forward_final))
    forward_in = carried_in((forward_total, forward_final), "sp", chain_combine, identity, False)[1]
    backward_in = carried_in((backward_total, backward_final), "sp", chain_combine, identity, True)[
        1
    ]
    forward_out = forward_out + apply_carry(queries, forward_in, forward_pos)
    backward_out = backward_out + apply_carry(queries[::-1], backward_in, backward_pos)
    heads_out = forward_out + backward_out[::-1]
    gated = heads_out.reshape(length, width_ssd) * jax.nn.silu(
        stored[:, :width_ssd].astype(jnp.float32)
    )
    squares = over_copies(jnp.sum(gated * gated, axis=-1), "tp")
    gain_dev = lax.dynamic_slice_in_dim(mix_gain, tp_rank * width_ssd, width_ssd, 0)
    ssd_mix = (gated * lax.rsqrt(squares / D_SSM + EPSILON)[:, None] * gain_dev).astype(
        jnp.bfloat16
    )
    pool_rows = padded[:, conv_cols:].astype(jnp.float32)
    own_rows = pool_rows[REACH : REACH + length]
    where_global = sp_rank * length + jnp.arange(length, dtype=jnp.int32)
    seq_length = length * sp_count
    window_means = []
    for window in WINDOWS:
        running = jnp.zeros((length, width_pool), jnp.float32)
        for offset in range(-(window // 2), window - window // 2):
            running = running + pool_rows[REACH + offset : REACH + offset + length]
        lower = jnp.clip(where_global - window // 2, 0, seq_length)
        upper = jnp.clip(where_global + window - window // 2, 0, seq_length)
        window_means.append(running / (upper - lower).astype(jnp.float32)[:, None])
    stacked = jnp.stack(window_means).reshape(4, length, pools_dev, POOL_DIM)
    group_ids = tp_rank * pools_dev + jnp.arange(pools_dev, dtype=jnp.int32)
    selector = (jnp.arange(4, dtype=jnp.int32)[:, None] == (group_ids % 4)[None, :]).astype(
        jnp.float32
    )
    means = jnp.sum(stacked * selector[:, None, :, None], axis=0)
    differences = (means - own_rows.reshape(length, pools_dev, POOL_DIM)).astype(jnp.bfloat16)
    pool_weights = lax.dynamic_slice_in_dim(pool_mix, tp_rank * pools_dev, pools_dev, 0)
    mapped = jnp.einsum(
        "rgc,gcd->rgd", differences, pool_weights, preferred_element_type=jnp.float32
    )
    pool_gain_dev = lax.dynamic_slice_in_dim(pool_gain, tp_rank * width_pool, width_pool, 0)
    pool_out = (mapped.reshape(length, width_pool) * pool_gain_dev).astype(jnp.bfloat16)
    out_ssd_rows = gathered[5]
    out_pool_rows = gathered[6]
    summed = sent_and_summed(
        (
            jnp.dot(ssd_mix, out_ssd_rows, preferred_element_type=jnp.float32)
            + jnp.dot(pool_out, out_pool_rows, preferred_element_type=jnp.float32)
        ).astype(jnp.bfloat16),
        "tp",
        0,
    )
    return summed.astype(jnp.bfloat16)[None]


def solution(mesh):
    return jax.shard_map(
        local,
        mesh=mesh,
        in_specs=(
            P("fs", ("sp", "tp"), None),
            P(),
            P(("sp", "fs"), "tp"),
            P(("sp", "fs"), "tp"),
            P(("sp", "fs"), "tp"),
            P(("sp", "fs"), "tp"),
            P(("sp", "fs"), "tp"),
            P(),
            P(),
            P(),
            P("fs", "tp", None, "sp"),
            P(),
            P(),
            P(),
            P(),
            P(),
            P(),
            P("tp", ("sp", "fs")),
            P("tp", ("sp", "fs")),
        ),
        out_specs=P("fs", ("sp", "tp"), None),
        check_vma=False,
    )
```

profile of v0, /device:TPU:1, one launch (start us, length us, event | category | flops | bytes accessed | tf_op | source)
XLA Modules:
  0.0 428.0 jit_solution(13822765884436530171)
XLA Ops:
  6.5 0.7 constant_dynamic-update-slice_fusion.6
  7.3 0.7 constant_dynamic-update-slice_fusion.5
  12.9 1.3 dynamic_slice.33
  14.3 1.3 dynamic_slice.35
  15.5 0.8 constant_dynamic-slice_fusion.3
  16.5 0.9 constant_dynamic-slice_fusion.4
  22.6 131.2 %all-gather.5.cloned.1.call-done = bf16[2048,896]{1,0:T(8,128)(2,1)} async-done(((bf16[32,896]{1,0:T(8,128)(2,1)}), bf16[2048,896]{1,0:T(8,128)(2,1)}) %all-gather.5.cloned.1.call-update) | async-done | bytes 3670032 | tf_op jit(solution)/shard_map/all_gather | solution.py:26
  153.7 3.5 slice.388
  157.2 42.3 %all-gather.3.cloned.1.call-done = bf16[1,1024,2048]{2,1,0:T(8,128)(2,1)} async-done(((bf16[1,128,2048]{2,1,0:T(8,128)(2,1)}), bf16[1,1024,2048]{2,1,0:T(8,128)(2,1)}) %all-gather.3.cloned.1.call-update) | async-done | bytes 4194320 | tf_op jit(solution)/shard_map/all_gather | solution.py:210
  199.5 3.2 fusion
  202.9 5.0 %fusion.144 = (bf16[1024,644]{0,1:T(8,128)(2,1)S(1)}, f32[1024,644]{0,1:T(8,128)S(1)}) fusion(bf16[2048,4]{1,0:T(8,128)(2,1)S(1)} %copy.185, bf16[2048,640]{1,0:T(8,128)(2,1)} %slice.388, bf16[1,1024,2048]{2,1,0:T(8,128)(2,1)S(1)} %copy-done.5, f32[2048]{0:T(1024)S(1)} %copy-done.45, f32[1024]{0:T(1024)S(1)} %add_rsqrt_fusion.1), kind=kOutput, calls=%fused_computation.256 | convolution fusion | flops 2715455488 | bytes 10801152 | tf_op jit(solution)/shard_map/dot_general | solution.py:213
  209.9 0.7 rev.8
  214.9 3.2 collective-permute-start
  218.1 1.3 collective-permute-start.1
  224.8 2.7 rev.19
  228.1 4.2 divide_multiply_fusion
  232.3 2.1 slice_bitcast_fusion.3
  234.4 3.0 rev.18
  237.4 3.8 reverse.11
  241.3 1.2 broadcast_multiply_fusion.1
  242.7 1.2 fusion.61
  244.0 0.8 fusion.82
  244.8 0.9 broadcast_in_dim.141
  245.7 14.1 %all-to-all-start.1 = ((bf16[16,129,128]{2,1,0:T(8,128)(2,1)}), bf16[16,129,128]{2,1,0:T(8,128)(2,1)}, u32[]{:S(2)}, u32[]{:S(2)}) async-start(bf16[16,129,128]{2,1,0:T(8,128)(2,1)} %broadcast_in_dim.141), calls=%async_computation.1 | async-start | bytes 1114112 | tf_op jit(solution)/shard_map/all_to_all | solution.py:53
  259.8 2.3 convolution_bitcast_fusion.1
  262.1 3.8 reverse.10
  266.1 1.8 fusion.13
  267.9 1.0 fusion.37
  269.0 2.3 fusion.19
  271.2 1.1 copy.216
  272.3 1.9 reshape.459
  274.3 1.2 copy.254
  275.5 1.1 copy.255
  276.8 1.2 fusion.65
  278.1 0.8 fusion.85
  279.6 0.9 convolution_bitcast_fusion.3
  280.5 1.5 fusion.14
  282.0 1.8 fusion.42
  284.2 1.6 broadcast_in_dim.82
  285.9 12.3 %all-to-all-start = ((bf16[16,129,128]{2,1,0:T(8,128)(2,1)}), bf16[16,129,128]{2,1,0:T(8,128)(2,1)}, u32[]{:S(2)}, u32[]{:S(2)}) async-start(bf16[16,129,128]{2,1,0:T(8,128)(2,1)} %broadcast_in_dim.82), calls=%async_computation | async-start | bytes 1114112 | tf_op jit(solution)/shard_map/all_to_all | solution.py:53
  298.2 3.5 fusion.18
  301.8 1.1 copy.201
  302.9 1.9 reshape.449
  304.8 3.2 concatenate.41
  308.0 1.0 slice_convert_fusion
  309.1 2.9 fusion.49
  312.0 2.3 divide_bitcast_fusion.2
  314.3 0.8 slice.412
  315.3 7.2 %all-to-all-done = bf16[16,129,128]{2,1,0:T(8,128)(2,1)} async-done(((bf16[16,129,128]{2,1,0:T(8,128)(2,1)}), bf16[16,129,128]{2,1,0:T(8,128)(2,1)}, u32[]{:S(2)}, u32[]{:S(2)}) %all-to-all-start) | async-done | bytes 528416 | tf_op jit(solution)/shard_map/all_to_all | solution.py:53
  322.5 0.8 slice.404
  323.5 1.1 slice.414
  325.2 0.7 copy-done.8
  325.9 1.4 fusion.15
  327.4 3.8 rev.20
  331.2 1.1 slice.406
  332.7 0.7 copy-done.7
  334.1 1.2 multiply_reduce_fusion
  336.0 9.9 %all-to-all-start.2 = ((f32[8,1,1024]{2,1,0:T(1,128)}), f32[8,1,1024]{2,1,0:T(1,128)S(1)}, u32[]{:S(2)}, u32[]{:S(2)}) async-start(f32[8,1,1024]{2,1,0:T(1,128)} %broadcast_in_dim.143), calls=%async_computation.2 | async-start | bytes 65536 | tf_op jit(solution)/shard_map/all_to_all | solution.py:53
  345.9 1.5 fusion.11
  347.5 3.2 all-to-all-done.2
  350.7 5.7 %fusion.58 = f32[1024,2048]{1,0:T(8,128)} fusion(bf16[2048,896]{1,0:T(8,128)(2,1)} %all-gather.5.cloned.1.call-done, f32[1024,128]{0,1:T(8,128)S(1)} %get-tuple-element.11, f32[128]{0:T(128)S(1)} %copy-done.38, f32[1024]{0:T(1024)S(1)} %add_rsqrt_fusion), kind=kOutput, calls=%fused_computation.88 | convolution fusion | flops 537264128 | bytes 9441792 | tf_op jit(solution)/shard_map/dot_general | solution.py:295
  356.4 7.1 %add_convert_fusion = bf16[1024,2048]{1,0:T(8,128)(2,1)} fusion(f32[1024,2048]{1,0:T(8,128)} %fusion.58, bf16[2048,896]{1,0:T(8,128)(2,1)} %all-gather.5.cloned.1.call-done, f32[1024,128]{0,1:T(8,128)S(1)} %fusion.11, f32[1040,128]{0,1:T(8,128)S(1)} %slice_convert_fusion, f32[128]{0:T(128)S(1)} %copy-done.41, bf16[8,128,128]{2,1,0:T(8,128)(2,1)S(1)} %copy-done, ...), kind=kOutput, calls=%fused_computation.5 | convolution fusion | flops 575143936 | bytes 14189060 | tf_op jit(solution)/shard_map/dot_general | solution.py:296
  363.5 53.9 %all_to_all.21 = bf16[8,128,2048]{2,1,0:T(8,128)(2,1)} all-to-all(bf16[8,128,2048]{2,1,0:T(8,128)(2,1)} %bitcast.260), channel_id=1, replica_groups=mesh['sp'=16,'fs'=4,'tp'=8] {'tp'}, dimensions={0} | all-to-all | bytes 8388608 | tf_op jit(solution)/shard_map/all_to_all | solution.py:110
  417.3 3.8 reduce_sum.52
  (203 shorter events, 27.0 us)
Async XLA Ops:
  6.5 349.8 %copy-start = (bf16[8,128,128]{2,1,0:T(8,128)(2,1)S(1)}, bf16[8,128,128]{2,1,0:T(8,128)(2,1)}, u32[]{:S(2)}) copy-start(bf16[8,128,128]{2,1,0:T(8,128)(2,1)} %param.34) | copy-start | bytes 786436
  6.5 147.2 %all-gather.5.cloned.1.call-start = ((), (), s32[]{:S(2)}) async-start(), calls=%async_computation.5 | async-start | bytes 3727360 | tf_op jit(solution)/shard_map/all_gather | solution.py:26
  11.5 0.6 copy-start.15
  12.2 187.3 %all-gather.3.cloned.1.call-start = ((), (), s32[]{:S(2)}) async-start(), calls=%async_computation.4 | async-start | bytes 4718592 | tf_op jit(solution)/shard_map/all_gather | solution.py:210
  157.2 45.5 %copy-start.45 = (f32[2048]{0:T(1024)S(1)}, f32[2048]{0:T(1024)}, u32[]{:S(2)}) copy-start(f32[2048]{0:T(1024)} %param.20) | copy-start | bytes 24580
  199.5 3.4 copy-start.5
  202.9 5.1 %copy-start.31 = (f32[1,2,2,1024]{3,2,1,0:T(2,128)S(1)}, f32[1,2,2,1024]{3,2,1,0:T(2,128)}, u32[]{:S(2)}) copy-start(f32[1,2,2,1024]{3,2,1,0:T(2,128)} %param.29) | copy-start | bytes 49156
  208.0 13.8 %copy-start.6 = (bf16[1024,644]{0,1:T(8,128)(2,1)}, bf16[1024,644]{0,1:T(8,128)(2,1)S(1)}, u32[]{:S(2)}) copy-start(bf16[1024,644]{0,1:T(8,128)(2,1)S(1)} %get-tuple-element.51) | copy-start | bytes 3956740
  209.1 5.7 %copy-start.28 = (f32[2,8]{1,0:T(2,128)}, f32[2,8]{1,0:T(2,128)S(1)}, u32[]{:S(2)}) copy-start(f32[2,8]{1,0:T(2,128)S(1)} %reduce_window_sum.39) | copy-start | bytes 196
  211.6 3.2 copy-start.30
  213.2 1.6 copy-start.32
  213.4 0.6 copy-start.34
  214.9 12.6 %collective-permute-start = (bf16[8,512]{0,1:T(8,128)(2,1)S(1)}, bf16[8,512]{0,1:T(8,128)(2,1)S(1)}, u32[]{:S(2)}, u32[]{:S(2)}) collective-permute-start(bf16[8,512]{0,1:T(8,128)(2,1)S(1)} %get-tuple-element.22), channel_id=1, source_target_pairs={{0,32},{32,64},{64,96},{96,128},{128,160},{160,192},{192,224},{224... | collective-permute-start | bytes 24584 | tf_op jit(solution)/shard_map/ppermute | solution.py:42
  218.1 9.4 %collective-permute-start.1 = (bf16[8,512]{0,1:T(8,128)(2,1)S(1)}, bf16[8,512]{0,1:T(8,128)(2,1)S(1)}, u32[]{:S(2)}, u32[]{:S(2)}) collective-permute-start(bf16[8,512]{0,1:T(8,128)(2,1)S(1)} %get-tuple-element.23), channel_id=1, source_target_pairs={{32,0},{64,32},{96,64},{128,96},{160,128},{192,160},{224,192},{256... | collective-permute-start | bytes 24584 | tf_op jit(solution)/shard_map/ppermute | solution.py:44
  227.5 0.7 copy-start.14
  241.2 1.4 copy-start.1
  241.2 1.4 copy-start.19
  242.6 1.3 copy-start.37
  242.7 2.1 copy-start.43
  245.7 38.6 %all-to-all-start.1 = ((bf16[16,129,128]{2,1,0:T(8,128)(2,1)}), bf16[16,129,128]{2,1,0:T(8,128)(2,1)}, u32[]{:S(2)}, u32[]{:S(2)}) async-start(bf16[16,129,128]{2,1,0:T(8,128)(2,1)} %broadcast_in_dim.141), calls=%async_computation.1 | async-start | bytes 1114112 | tf_op jit(solution)/shard_map/all_to_all | solution.py:53
  265.9 2.0 copy-start.2
  266.0 2.9 copy-start.4
  266.0 2.9 copy-start.17
  266.0 2.9 copy-start.18
  274.3 2.4 copy-start.13
  274.3 2.5 copy-start.16
  274.3 2.5 copy-start.23
  276.6 1.5 copy-start.36
  276.6 2.3 copy-start.42
  276.6 2.9 copy-start.29
  276.6 2.9 copy-start.33
  276.7 2.9 copy-start.35
  276.8 3.7 copy-start.3
  276.8 3.7 copy-start.22
  278.1 3.9 copy-start.11
  278.1 3.9 copy-start.12
  285.9 36.6 %all-to-all-start = ((bf16[16,129,128]{2,1,0:T(8,128)(2,1)}), bf16[16,129,128]{2,1,0:T(8,128)(2,1)}, u32[]{:S(2)}, u32[]{:S(2)}) async-start(bf16[16,129,128]{2,1,0:T(8,128)(2,1)} %broadcast_in_dim.82), calls=%async_computation | async-start | bytes 1114112 | tf_op jit(solution)/shard_map/all_to_all | solution.py:53
  304.8 4.2 copy-start.27
  309.0 2.9 copy-start.24
  309.0 2.9 copy-start.25
  309.1 2.9 copy-start.26
  312.0 3.1 copy-start.40
  312.0 11.3 %copy-start.39 = (pred[16]{0:T(512)(128)(4,1)S(1)}, pred[16]{0:T(512)(128)(4,1)}, u32[]{:S(2)}) copy-start(pred[16]{0:T(512)(128)(4,1)} %iota_compare_fusion.3) | copy-start | bytes 52
  324.9 1.0 copy-start.8
  324.9 1.0 copy-start.21
  332.4 1.0 copy-start.7
  332.4 1.0 copy-start.20
  333.4 12.5 %copy-start.44 = (f32[4]{0:T(128)S(1)}, f32[4]{0:T(128)}, u32[]{:S(2)}) copy-start(f32[4]{0:T(128)} %compare_convert_fusion) | copy-start | bytes 52
  334.1 11.8 %copy-start.9 = (f32[1,1024,1,128]{1,3,2,0:T(8,128)S(1)}, f32[1,1024,1,128]{1,3,2,0:T(8,128)}, u32[]{:S(2)}) copy-start(f32[1,1024,1,128]{1,3,2,0:T(8,128)} %fusion.49) | copy-start | bytes 1572868
  334.1 11.8 %copy-start.10 = (f32[1,1024,1,128]{1,3,2,0:T(8,128)S(1)}, f32[1,1024,1,128]{1,3,2,0:T(8,128)}, u32[]{:S(2)}) copy-start(f32[1,1024,1,128]{1,3,2,0:T(8,128)} %get-tuple-element.26) | copy-start | bytes 1572868
  335.4 15.3 %copy-start.38 = (f32[128]{0:T(128)S(1)}, f32[128]{0:T(128)}, u32[]{:S(2)}) copy-start(f32[128]{0:T(128)} %dynamic_slice.33) | copy-start | bytes 1540
  336.0 14.6 %all-to-all-start.2 = ((f32[8,1,1024]{2,1,0:T(1,128)}), f32[8,1,1024]{2,1,0:T(1,128)S(1)}, u32[]{:S(2)}, u32[]{:S(2)}) async-start(f32[8,1,1024]{2,1,0:T(1,128)} %broadcast_in_dim.143), calls=%async_computation.2 | async-start | bytes 65536 | tf_op jit(solution)/shard_map/all_to_all | solution.py:53
  350.7 5.7 %copy-start.41 = (f32[128]{0:T(128)S(1)}, f32[128]{0:T(128)}, u32[]{:S(2)}) copy-start(f32[128]{0:T(128)} %dynamic_slice.35) | copy-start | bytes 1540
Sparse Core Ops, SparseCore 0:
  12.3 141.4 all-gather.4
  155.9 43.5 all-gather.2
where the time goes:
time: 430 us; the launch traced here: 428 us
  waiting for transfers between devices  185 us (43%)
  local copies, waits for them, and re-layouts  63.5 us (15%)
  blocking collectives  53.9 us (13%)
  starting transfers between devices  40.8 us (9%)
  matrix products  39.2 us (9%)
  other arithmetic  31.4 us (7%)
  between operations  14.3 us (3%)
    all_gather x1, waiting for transfers between devices, turned_gather(): out, at, gathered = (lax.all_gather(both, axis, axis=0, tiled=True), 0, [])  131 us
    all_to_all x1, blocking collectives, sent_and_summed(): lax.all_to_all(tiles, axis, split_axis=0, concat_axis=0, tiled=True)  53.9 us
    all_gather x1, waiting for transfers between devices, local(): lax.all_gather(tokens, 'tp', axis=1, tiled=True)[0].astype(jnp.float32)  42.3 us
    all_to_all x3, starting transfers between devices, from_everyone(): lax.all_to_all(jnp.broadcast_to(x[None], (length, *x.shape)), axis, 0, 0,...  36.3 us
    unnamed x113, local copies, waits for them, and re-layouts  14.6 us
    all_to_all x3, waiting for transfers between devices, from_everyone(): lax.all_to_all(jnp.broadcast_to(x[None], (length, *x.shape)), axis, 0, 0,...  10.8 us
  transfers between devices with their start and end apart: 7, of which 5 were waited for; matrix products, arithmetic and copies ran while one was open for 15% of the time, Pallas kernels for 0%

commit v1 on v0

--- a/solution.py
+++ b/solution.py
@@ -1,6 +1,10 @@
+import functools
+
 import jax
 import jax.numpy as jnp
 from jax import lax
+from jax.experimental import pallas as pl
+from jax.experimental.pallas import tpu as pltpu
 from jax.sharding import PartitionSpec as P
 
 HEAD_DIM = 64
@@ -18,6 +22,270 @@
 EPSILON = 1e-06
 HIGHEST = lax.Precision.HIGHEST
 WINDOWS = (2, 4, 8, 16)
+
+MESH = pl.DeviceIdType.MESH
+A_COLS = 384
+W_COLS = 896
+HALO = 16
+TOK_ROWS = 128
+PIECE = 32
+
+
+def remote(src, dst, send, recv, where):
+    return pltpu.make_async_remote_copy(
+        src_ref=src, dst_ref=dst, send_sem=send, recv_sem=recv, device_id=where, device_id_type=MESH
+    )
+
+
+def entry_barrier(places):
+    barrier = pltpu.get_barrier_semaphore()
+    for where in places:
+        pl.semaphore_signal(barrier, inc=1, device_id=where, device_id_type=MESH)
+    pl.semaphore_wait(barrier, len(places))
+
+
+def gather_kernel(
+    n_sp, n_fs, n_x,
+    tok, wg, wv, wk, wq, wp, wo, wstep, gain,
+    proj, raw, wout,
+    tokbuf, wbuf,
+    local_sem, out_sem,
+    tp_sem, tm_sem, tr_sem, td_sem,
+    ay_sem, azp_sem, azm_sem, bzp_sem, bzm_sem, byp_sem, bym_sem, byo_sem, h_sem,
+    send_sem,
+):
+    z, y, t = lax.axis_index("sp"), lax.axis_index("fs"), lax.axis_index("tp")
+    x, c = t // 2, t % 2
+    xp, xm = (x + 1) % n_x, (x + n_x - 1) % n_x
+    yp, ym = (y + 1) % n_fs, (y + n_fs - 1) % n_fs
+    zp, zm = (z + 1) % n_sp, (z + n_sp - 1) % n_sp
+    to_xp, to_xm, to_d = {"tp": xp * 2 + c}, {"tp": xm * 2 + c}, {"tp": x * 2 + 1 - c}
+    to_yp, to_ym = {"fs": yp}, {"fs": ym}
+    to_zp, to_zm = {"sp": zp}, {"sp": zm}
+
+    def trow(xx, cc, q):
+        return pl.multiple_of(HALO + (xx * 2 + cc) * TOK_ROWS + q * PIECE, 16)
+
+    def wrow(zz, yy):
+        return pl.multiple_of((zz * n_fs + yy) * PIECE, PIECE)
+
+    def a_at(zz, yy):
+        return wbuf.at[pl.ds(wrow(zz, yy), PIECE), pl.ds(0, A_COLS)]
+
+    def b_at(zz, yy):
+        return wbuf.at[pl.ds(wrow(zz, yy), PIECE), pl.ds(A_COLS, W_COLS - A_COLS)]
+
+    def t_at(xx, cc, q, rows=PIECE):
+        return tokbuf.at[pl.ds(trow(xx, cc, q), rows), :]
+
+    locals_ = [pltpu.make_async_copy(tok.at[0], t_at(x, c, 0, TOK_ROWS), local_sem.at[0])]
+    for i, w in enumerate((wg, wv, wk, wq, wp)):
+        locals_.append(
+            pltpu.make_async_copy(
+                w, wbuf.at[pl.ds(wrow(z, y), PIECE), pl.ds(i * 128, 128)], local_sem.at[1 + i]
+            )
+        )
+    locals_.append(
+        pltpu.make_async_copy(
+            wo, wbuf.at[pl.ds(wrow(z, y), PIECE), pl.ds(640, 256)], local_sem.at[6]
+        )
+    )
+    for copy in locals_:
+        copy.start()
+    entry_barrier((to_xp, to_xm, to_yp, to_ym, to_zp, to_zm, to_d))
+
+    sent = []
+
+    def send(ref, recv, where):
+        copy = remote(ref, ref, send_sem.at[len(sent)], recv, where)
+        copy.start()
+        sent.append(copy)
+
+    def arrived(ref, recv):
+        remote(ref, ref, send_sem.at[0], recv, to_d).wait_recv()
+
+    for copy in locals_[1:]:
+        copy.wait()
+    own_a, own_b = a_at(z, y), b_at(z, y)
+    send(own_a, ay_sem.at[0], to_yp)
+    send(own_a, ay_sem.at[1], to_ym)
+    send(own_a, azp_sem.at[4], to_zp)
+    send(own_a, azm_sem.at[4], to_zm)
+    send(own_b, bzp_sem.at[1], to_zp)
+    send(own_b, bzm_sem.at[1], to_zm)
+    locals_[0].wait()
+    for q in (0, 1, 2, 3):
+        send(t_at(x, c, q), tp_sem.at[q], to_xp)
+    for q in (2, 3, 0, 1):
+        send(t_at(x, c, q), tm_sem.at[q], to_xm)
+    send(own_b, byp_sem.at[0], to_yp)
+    send(own_b, bym_sem.at[0], to_ym)
+    send(t_at(x, c, 0, TOK_ROWS), td_sem.at[12], to_d)
+
+    yo = (y + 2) % n_fs
+    y_of = (y, ym, yp, yo)
+    arrived(a_at(z, ym), ay_sem.at[0])
+    send(a_at(z, ym), ay_sem.at[2], to_yp)
+    send(a_at(z, ym), azp_sem.at[5], to_zp)
+    send(a_at(z, ym), azm_sem.at[5], to_zm)
+    arrived(a_at(z, yp), ay_sem.at[1])
+    send(a_at(z, yp), azp_sem.at[6], to_zp)
+    send(a_at(z, yp), azm_sem.at[6], to_zm)
+    arrived(a_at(z, yo), ay_sem.at[2])
+    send(a_at(z, yo), azp_sem.at[7], to_zp)
+    send(a_at(z, yo), azm_sem.at[7], to_zm)
+
+    half = n_sp // 2
+
+    def back(o):
+        return (z + n_sp - o) % n_sp
+
+    def relay_y(o):
+        arrived(b_at(back(o), ym), byp_sem.at[o])
+        if o % 2 == 0:
+            send(b_at(back(o), ym), byo_sem.at[o], to_yp)
+        arrived(b_at(back(o), yp), bym_sem.at[o])
+        if o % 2 == 1:
+            send(b_at(back(o), yp), byo_sem.at[o], to_ym)
+
+    def token_step(k):
+        if k <= 4:
+            q = k - 1
+            arrived(t_at(xm, c, q), tp_sem.at[q])
+            if q < 2:
+                send(t_at(xm, c, q), tr_sem.at[q], to_xp)
+            send(t_at(xm, c, q), td_sem.at[q], to_d)
+            q = (2, 3, 0, 1)[k - 1]
+            arrived(t_at(xp, c, q), tm_sem.at[q])
+            if q >= 2:
+                send(t_at(xp, c, q), tr_sem.at[q], to_xm)
+            send(t_at(xp, c, q), td_sem.at[4 + q], to_d)
+        elif k <= 6:
+            for q in (k - 5, k - 3):
+                xo = (x + 2) % n_x
+                arrived(t_at(xo, c, q), tr_sem.at[q])
+                send(t_at(xo, c, q), td_sem.at[8 + q], to_d)
+
+    pending = [0]
+    for k in range(1, half + 1):
+        far = k == half
+        for j in range(4):
+            if not far or j < 2:
+                ref = a_at(back(k), y_of[j])
+                arrived(ref, azp_sem.at[4 * k + j])
+                if k + 1 < half or (k + 1 == half and j < 2):
+                    send(ref, azp_sem.at[4 * (k + 1) + j], to_zp)
+            if not far or j >= 2:
+                ref = a_at((z + k) % n_sp, y_of[j])
+                arrived(ref, azm_sem.at[4 * k + j])
+                if k + 1 < half or (k + 1 == half and j >= 2):
+                    send(ref, azm_sem.at[4 * (k + 1) + j], to_zm)
+            if j == 1:
+                token_step(k)
+        fresh = []
+        ref = b_at(back(k), y)
+        arrived(ref, bzp_sem.at[k])
+        if k < half:
+            send(ref, bzp_sem.at[k + 1], to_zp)
+        send(ref, byp_sem.at[k], to_yp)
+        send(ref, bym_sem.at[k], to_ym)
+        fresh.append(k)
+        if not far:
+            o = n_sp - k
+            ref = b_at(back(o), y)
+            arrived(ref, bzm_sem.at[k])
+            if k + 1 < half:
+                send(ref, bzm_sem.at[k + 1], to_zm)
+            send(ref, byp_sem.at[o], to_yp)
+            send(ref, bym_sem.at[o], to_ym)
+            fresh.append(o)
+        for o in pending:
+            relay_y(o)
+        pending = fresh
+
+    cs = 1 - c
+    arrived(t_at(x, cs, 0, TOK_ROWS), td_sem.at[12])
+    for q in range(4):
+        arrived(t_at(xm, cs, q), td_sem.at[q])
+        arrived(t_at(xp, cs, q), td_sem.at[4 + q])
+        arrived(t_at((x + 2) % n_x, cs, q), td_sem.at[8 + q])
+    rows = 2 * n_x * TOK_ROWS
+    last = tokbuf.at[pl.ds(rows, HALO), :]
+    first = tokbuf.at[pl.ds(HALO, HALO), :]
+    before = tokbuf.at[pl.ds(0, HALO), :]
+    after = tokbuf.at[pl.ds(HALO + rows, HALO), :]
+    halo_up = remote(last, before, send_sem.at[len(sent)], h_sem.at[0], to_zp)
+    halo_up.start()
+    sent.append(halo_up)
+    halo_down = remote(first, after, send_sem.at[len(sent)], h_sem.at[1], to_zm)
+    halo_down.start()
+    sent.append(halo_down)
+    for o in pending:
+        relay_y(o)
+    for o in range(n_sp):
+        arrived(b_at(back(o), yo), byo_sem.at[o])
+    to_out = pltpu.make_async_copy(wbuf.at[:, pl.ds(640, 256)], wout, out_sem)
+    to_out.start()
+
+    def project(begin, count):
+        part = tokbuf[pl.ds(begin, count), :].astype(jnp.float32)
+        scaling = lax.rsqrt(jnp.mean(part * part, axis=-1, keepdims=True) + EPSILON)
+        normed = (part * scaling * gain[...]).astype(jnp.bfloat16)
+        proj[pl.ds(begin, count), :] = jnp.dot(
+            normed, wbuf[:, 0:640], preferred_element_type=jnp.float32
+        ).astype(jnp.bfloat16)
+        return normed
+
+    def step(i, carry):
+        begin = pl.multiple_of(HALO + i * 256, 16)
+        normed = project(begin, 256)
+        raw[pl.ds(pl.multiple_of(i * 256, 256), 256), :] = jnp.dot(
+            normed, wstep[...], preferred_element_type=jnp.float32
+        )
+        return carry
+
+    lax.fori_loop(0, rows // 256, step, 0)
+    remote(before, before, send_sem.at[0], h_sem.at[0], to_d).wait_recv()
+    remote(after, after, send_sem.at[0], h_sem.at[1], to_d).wait_recv()
+    project(0, HALO)
+    project(HALO + rows, HALO)
+    to_out.wait()
+    for copy in sent:
+        copy.wait_send()
+
+
+N_SENDS = 191
+
+
+def gather_and_project(n_sp, n_fs, n_x, tok, ws, wo, wstep, gain):
+    rows = 2 * n_x * TOK_ROWS
+    any_spec = pl.BlockSpec(memory_space=pl.ANY)
+    vmem = pl.BlockSpec(memory_space=pltpu.VMEM)
+    dma = pltpu.SemaphoreType.DMA
+    return pl.pallas_call(
+        functools.partial(gather_kernel, n_sp, n_fs, n_x),
+        out_shape=(
+            jax.ShapeDtypeStruct((rows + 2 * HALO, 640), jnp.bfloat16),
+            jax.ShapeDtypeStruct((rows, 128), jnp.float32),
+            jax.ShapeDtypeStruct((2048, 256), jnp.bfloat16),
+        ),
+        in_specs=[any_spec] * 7 + [vmem, vmem],
+        out_specs=(vmem, vmem, any_spec),
+        scratch_shapes=[
+            pltpu.VMEM((rows + 2 * HALO, 2048), jnp.bfloat16),
+            pltpu.VMEM((2048, W_COLS), jnp.bfloat16),
+            dma((7,)),
+            dma,
+            dma((4,)), dma((4,)), dma((4,)), dma((13,)),
+            dma((3,)), dma((36,)), dma((36,)), dma((9,)), dma((9,)),
+            dma((16,)), dma((16,)), dma((16,)), dma((2,)),
+            dma((N_SENDS,)),
+        ],
+        compiler_params=pltpu.CompilerParams(
+            collective_id=0, has_side_effects=True, vmem_limit_bytes=48 * 1024 * 1024
+        ),
+        name="gather_and_project",
+    )(tok, *ws, wo, wstep, gain)
 
 
 def turned_gather(arrays, axis, dims):
@@ -197,25 +465,24 @@
     width_ssd = heads_dev * HEAD_DIM
     width_key = groups_dev * STATE
     width_pool = pools_dev * POOL_DIM
-    gathered = turned_gather(
-        (w_gate, w_value, w_bkey, w_query, w_pool_in, w_out_ssd, w_out_pool),
-        ("sp", "fs"),
-        (0, 0, 0, 0, 0, 1, 1),
-    )
     step_cols = lax.dynamic_slice_in_dim(w_step, tp_rank * heads_dev, heads_dev, 2)
-    step_cols = step_cols.reshape(w_step.shape[0], 2 * heads_dev)
-    combined = jnp.concatenate(
-        [gathered[0], gathered[1], gathered[2], gathered[3], gathered[4], step_cols], axis=1
-    )
-    widened = lax.all_gather(tokens, "tp", axis=1, tiled=True)[0].astype(jnp.float32)
-    scaling = lax.rsqrt(jnp.mean(widened * widened, axis=-1, keepdims=True) + EPSILON)
-    normed = (widened * scaling * norm_gain).astype(jnp.bfloat16)
-    projected = jnp.dot(normed, combined, preferred_element_type=jnp.float32)[None][0]
-    length = projected.shape[0]
-    stored_cols = 2 * width_ssd + 2 * width_key + width_pool
-    stored = projected[:, :stored_cols].astype(jnp.bfloat16)
-    raw_steps = projected[:, stored_cols:]
-    padded = padded_2(stored[:, width_ssd:], (("sp", 0),), REACH)
+    step_cols = jnp.pad(step_cols.reshape(w_step.shape[0], 2 * heads_dev), ((0, 0), (0, 124)))
+    out_turned = jnp.concatenate([w_out_ssd.T, w_out_pool.T], axis=1)
+    projected, raw_steps, wout = gather_and_project(
+        sp_count, lax.axis_size("fs"), tp_count // 2,
+        tokens, (w_gate, w_value, w_bkey, w_query, w_pool_in), out_turned, step_cols,
+        norm_gain[None],
+    )
+    raw_steps = raw_steps[:, : 2 * heads_dev]
+    length = raw_steps.shape[0]
+    stored = projected[HALO : HALO + length]
+    row_ids = jnp.arange(length + 2 * REACH)
+    inside = ((row_ids >= REACH) | (sp_rank > 0)) & (
+        (row_ids < REACH + length) | (sp_rank < sp_count - 1)
+    )
+    padded = jnp.where(
+        inside[:, None], projected[HALO - REACH : HALO + REACH + length, width_ssd:], 0
+    )
     conv_cols = width_ssd + 2 * width_key
     taps = jnp.concatenate(
         [
@@ -288,8 +555,8 @@
     )
     pool_gain_dev = lax.dynamic_slice_in_dim(pool_gain, tp_rank * width_pool, width_pool, 0)
     pool_out = (mapped.reshape(length, width_pool) * pool_gain_dev).astype(jnp.bfloat16)
-    out_ssd_rows = gathered[5]
-    out_pool_rows = gathered[6]
+    out_ssd_rows = wout[:, :width_ssd].T
+    out_pool_rows = wout[:, width_ssd:].T
     summed = sent_and_summed(
         (
             jnp.dot(ssd_mix, out_ssd_rows, preferred_element_type=jnp.float32)

time: 430 us -> 262 us (0.61)
  waiting for transfers between devices: 185 us -> 16.2 us
  Pallas kernels: 0 us -> 55.8 us
  local copies, waits for them, and re-layouts: 63.5 us -> 48 us
  between operations: 14.3 us -> 0.75 us
  other arithmetic: 31.4 us -> 19.4 us
  starting transfers between devices: 40.8 us -> 32.2 us
  matrix products: 39.2 us -> 34 us
    all_gather x2 -> x0, waiting for transfers between devices: 173 us -> none  [the longest x1 131 us: turned_gather(): out, at, gathered = (lax.all_gather(both, axis, axis=0, tiled=True), 0, [])]
    pallas_call x0 -> x1, Pallas kernels: none -> 55.8 us  [gather_and_project(): pl.pallas_call(functools.partial(gather_kernel, n_sp, n_fs, n_x), out_sha...]
    unnamed x113 -> x71, local copies, waits for them, and re-layouts: 14.6 us -> 5.92 us
    all_to_all x3, waiting for transfers between devices: 10.8 us -> 16.2 us  [from_everyone(): lax.all_to_all(jnp.broadcast_to(x[None], (length, *x.shape)), axis, 0, 0,...]
    dot_general x1 -> x0, matrix products: 5.05 us -> none  [local(): jnp.dot(normed, combined, preferred_element_type=jnp.float32)[None][0]]
    ppermute x2 -> x0, starting transfers between devices: 4.48 us -> none  [the longest x1 3.19 us: padded_2(): lax.ppermute(tail, axis, [(i, (i + 1) % count) for i in range(ends)])]
  transfers between devices with their start and end apart: 7 -> 3, of which waited for: 5 -> 2; matrix products, arithmetic and copies ran while one was open for 15% -> 15% of each run, Pallas kernels for 0% -> 0%
where the time goes in v1:
time: 262 us; the launch traced here: 260 us
  Pallas kernels  55.8 us (21%)
  blocking collectives  53.8 us (21%)
  local copies, waits for them, and re-layouts  48 us (18%)
  matrix products  34 us (13%)
  starting transfers between devices  32.2 us (12%)
  other arithmetic  19.4 us (7%)
  waiting for transfers between devices  16.2 us (6%)
    pallas_call x1, Pallas kernels, gather_and_project(): pl.pallas_call(functools.partial(gather_kernel, n_sp, n_fs, n_x), out_sha...  55.8 us
    all_to_all x1, blocking collectives, sent_and_summed(): lax.all_to_all(tiles, axis, split_axis=0, concat_axis=0, tiled=True)  53.8 us
    all_to_all x3, starting transfers between devices, from_everyone(): lax.all_to_all(jnp.broadcast_to(x[None], (length, *x.shape)), axis, 0, 0,...  32.2 us
    all_to_all x3, waiting for transfers between devices, from_everyone(): lax.all_to_all(jnp.broadcast_to(x[None], (length, *x.shape)), axis, 0, 0,...  16.2 us
    dot_general x1, matrix products, local(): jnp.dot(pool_out, out_pool_rows, preferred_element_type=jnp.float32)  7.06 us
    another operation x2, local copies, waits for them, and re-layouts  6.01 us
    unnamed x71, local copies, waits for them, and re-layouts  5.92 us
    dot_general x1, matrix products, local(): jnp.dot(ssd_mix, out_ssd_rows, preferred_element_type=jnp.float32)  5.57 us
  transfers between devices with their start and end apart: 3, of which 2 were waited for; matrix products, arithmetic and copies ran while one was open for 15% of the time, Pallas kernels for 0%

profile of v1, /device:TPU:1, one launch (start us, length us, event | category | flops | bytes accessed | tf_op | source)
XLA Modules:
  0.0 260.2 jit_solution(15322491057301599936)
XLA Ops:
  0.1 1.0 constant_dynamic-slice_fusion.4
  1.4 0.7 pad_maximum_fusion.2.wo
  2.3 55.8 %gather_and_project.1 = (bf16[1056,640]{1,0:T(8,128)(2,1)S(1)}, f32[1024,128]{1,0:T(8,128)S(1)}, bf16[2048,256]{1,0:T(8,128)(2,1)S(1)}) custom-call(bf16[1,128,2048]{2,1,0:T(8,128)(2,1)S(1)} %copy-done.1, bf16[32,128]{1,0:T(8,128)(2,1)S(1)} %copy-done.3, bf16[32,128]{1,0:T(8,128)(2,1)S(1)} %copy-done.4, bf16[32,128]{1,0:T(8,128)(2,1)S(1)} %copy-done.5, ...), custom_call_target="tpu_custom_call" | custom-call | tf_op jit(solution)/shard_map/gather_and_project/pallas_call | solution.py:265
  58.1 0.8 copy-done.2
  58.9 1.2 copy.149
  60.4 0.7 rev.8
  62.6 0.7 rev.19
  63.3 0.7 constant_dynamic-slice_fusion.2
  64.0 0.7 constant_dynamic-slice_fusion
  65.0 1.2 divide_multiply_fusion
  66.2 1.2 fusion.107
  67.7 2.2 copy.153
  69.9 5.0 %rev.18 = f32[1024,2,64]{0,2,1:T(8,128)} reverse(f32[1024,2,64]{0,2,1:T(8,128)} %bitcast.243), dimensions={0} | reverse | bytes 1048576 | tf_op jit(solution)/shard_map/rev | solution.py:515
  75.0 2.6 reverse.11
  77.6 1.1 broadcast_multiply_fusion.1
  78.9 0.7 fusion.37
  79.6 0.8 copy-done.21
  80.4 0.8 fusion.56
  81.3 0.9 broadcast_in_dim.158
  82.1 7.8 %all-to-all-start.1 = ((bf16[16,129,128]{2,1,0:T(8,128)(2,1)}), bf16[16,129,128]{2,1,0:T(8,128)(2,1)}, u32[]{:S(2)}, u32[]{:S(2)}) async-start(bf16[16,129,128]{2,1,0:T(8,128)(2,1)} %broadcast_in_dim.158), calls=%async_computation.1 | async-start | bytes 1114112 | tf_op jit(solution)/shard_map/all_to_all | solution.py:321
  91.3 3.4 %reverse.10 = f32[1024,128]{1,0:T(8,128)S(1)} reverse(f32[1024,128]{1,0:T(8,128)} %get-tuple-element.22), dimensions={0} | reverse | bytes 1048576 | tf_op jit(solution)/shard_map/reverse
  94.7 2.1 convolution_bitcast_fusion.1
  96.9 1.2 copy.190
  98.1 0.9 broadcast_multiply_fusion.2
  98.9 0.7 fusion.40
  99.7 0.8 copy-done.17
  100.4 1.7 convolution_bitcast_fusion.3
  102.1 1.2 fusion.116
  103.3 1.2 fusion.2
  104.6 2.3 fusion.8
  107.1 1.1 copy.171
  108.2 2.0 reshape.457
  110.2 2.5 fusion.3
  112.7 1.2 fusion.115
  113.9 2.3 fusion.7
  116.2 1.1 copy.160
  117.3 1.9 reshape.447
  119.3 0.8 fusion.59
  120.2 0.9 broadcast_in_dim.153
  121.1 11.5 %all-to-all-start = ((bf16[16,129,128]{2,1,0:T(8,128)(2,1)}), bf16[16,129,128]{2,1,0:T(8,128)(2,1)}, u32[]{:S(2)}, u32[]{:S(2)}) async-start(bf16[16,129,128]{2,1,0:T(8,128)(2,1)} %broadcast_in_dim.153), calls=%async_computation | async-start | bytes 1114112 | tf_op jit(solution)/shard_map/all_to_all | solution.py:321
  132.6 1.0 slice_convert_fusion
  133.6 1.6 divide_bitcast_fusion.2
  135.2 1.3 fusion.25
  136.6 0.8 slice.378
  137.6 15.6 %all-to-all-done = bf16[16,129,128]{2,1,0:T(8,128)(2,1)} async-done(((bf16[16,129,128]{2,1,0:T(8,128)(2,1)}), bf16[16,129,128]{2,1,0:T(8,128)(2,1)}, u32[]{:S(2)}, u32[]{:S(2)}) %all-to-all-start) | async-done | bytes 528416 | tf_op jit(solution)/shard_map/all_to_all | solution.py:321
  153.1 0.8 slice.370
  154.2 1.1 slice.380
  155.8 0.7 copy-done.12
  156.7 1.4 fusion.4
  158.2 5.0 %rev.20 = f32[1024,2,64]{0,2,1:T(8,128)} reverse(f32[1024,2,64]{0,2,1:T(8,128)} %fusion.4), dimensions={0} | reverse | bytes 1048576 | tf_op jit(solution)/shard_map/rev | solution.py:524
  163.2 1.1 slice.372
  164.8 0.7 copy-done.23
  165.7 2.5 fusion.6
  168.2 2.1 copy.173
  170.2 1.3 multiply_reduce_fusion
  172.1 13.0 %all-to-all-start.2 = ((f32[8,1,1024]{2,1,0:T(1,128)}), f32[8,1,1024]{2,1,0:T(1,128)S(1)}, u32[]{:S(2)}, u32[]{:S(2)}) async-start(f32[8,1,1024]{2,1,0:T(1,128)} %broadcast_in_dim.160), calls=%async_computation.2 | async-start | bytes 65536 | tf_op jit(solution)/shard_map/all_to_all | solution.py:321
  185.1 2.6 fusion
  187.7 0.8 dynamic_slice.33
  188.4 0.8 dynamic_slice.35
  189.2 0.6 all-to-all-done.2
  189.9 5.6 %fusion.44 = f32[1024,2048]{1,0:T(8,128)} fusion(bf16[2048,256]{1,0:T(8,128)(2,1)S(1)} %get-tuple-element.10, f32[128]{0:T(128)S(1)} %dynamic_slice.33, f32[1024]{0:T(1024)S(1)} %add_rsqrt_fusion, f32[1024,128]{1,0:T(8,128)} %copy.173, bf16[1056,640]{1,0:T(8,128)(2,1)S(1)} %get-tuple-element.9), kind=kOutput, calls=%fused_computation.72 | convolution fusion | flops 538050560 | bytes 9703936 | tf_op jit(solution)/shard_map/dot_general | solution.py:562
  195.5 7.1 %add_convert_fusion = bf16[1024,2048]{1,0:T(8,128)(2,1)} fusion(f32[1024,2048]{1,0:T(8,128)} %fusion.44, bf16[2048,256]{1,0:T(8,128)(2,1)S(1)} %get-tuple-element.10, f32[1024,128]{1,0:T(8,128)} %fusion, f32[1040,128]{1,0:T(8,128)S(1)} %slice_convert_fusion, f32[128]{0:T(128)S(1)} %dynamic_slice.35, bf16[8,128,128]{2,1,0:T(8,128)(2,1)S(1)} %copy-done, ...), kind=kOutput, calls=%fused_computation | convolution fusion | flops 575143936 | bytes 14189060 | tf_op jit(solution)/shard_map/dot_general | solution.py:563
  202.5 53.8 %all_to_all.21 = bf16[8,128,2048]{2,1,0:T(8,128)(2,1)} all-to-all(bf16[8,128,2048]{2,1,0:T(8,128)(2,1)} %bitcast.234), channel_id=1, replica_groups=mesh['sp'=16,'fs'=4,'tp'=8] {'tp'}, dimensions={0} | all-to-all | bytes 8388608 | tf_op jit(solution)/shard_map/all_to_all | solution.py:378
  256.4 3.8 %reduce_sum.42 = bf16[128,2048]{1,0:T(8,128)(2,1)} reduce(bf16[8,128,2048]{2,1,0:T(8,128)(2,1)} %all_to_all.21, bf16[]{:T(256)} %constant.81.clone.1), dimensions={0}, to_apply=%region_7.8 | reduce | flops 1835008 | bytes 4718594 | tf_op jit(solution)/shard_map/reduce_sum | solution.py:379
  (147 shorter events, 7.1 us)
Async XLA Ops:
  0.0 195.5 %copy-start = (bf16[8,128,128]{2,1,0:T(8,128)(2,1)S(1)}, bf16[8,128,128]{2,1,0:T(8,128)(2,1)}, u32[]{:S(2)}) copy-start(bf16[8,128,128]{2,1,0:T(8,128)(2,1)} %param.34) | copy-start | bytes 786436
  0.0 2.2 copy-start.7
  0.0 2.2 copy-start.6
  0.0 2.2 copy-start.5
  0.0 2.2 copy-start.4
  0.0 2.2 copy-start.3
  0.0 2.2 copy-start.8
  0.1 2.2 copy-start.1
  1.1 59.1 %copy-start.28 = (f32[2,16]{1,0:T(2,128)S(1)}, f32[2,16]{1,0:T(2,128)}, u32[]{:S(2)}) copy-start(f32[2,16]{1,0:T(2,128)} %param.27) | copy-start | bytes 388
  1.1 59.1 %copy-start.29 = (f32[2,16]{1,0:T(2,128)S(1)}, f32[2,16]{1,0:T(2,128)}, u32[]{:S(2)}) copy-start(f32[2,16]{1,0:T(2,128)} %param.28) | copy-start | bytes 388
  1.1 59.1 %copy-start.27 = (f32[1,2,2,1024]{3,2,1,0:T(2,128)S(1)}, f32[1,2,2,1024]{3,2,1,0:T(2,128)}, u32[]{:S(2)}) copy-start(f32[1,2,2,1024]{3,2,1,0:T(2,128)} %param.29) | copy-start | bytes 49156
  58.1 0.8 copy-start.2
  64.9 1.2 copy-start.9
  66.2 1.5 copy-start.10
  67.7 9.8 %copy-start.13 = (f32[1024,128]{1,0:T(8,128)}, f32[1024,128]{1,0:T(8,128)S(1)}, u32[]{:S(2)}) copy-start(f32[1024,128]{1,0:T(8,128)S(1)} %get-tuple-element.21) | copy-start | bytes 1572868
  77.6 1.3 copy-start.19
  79.6 0.8 copy-start.21
  82.1 38.1 %all-to-all-start.1 = ((bf16[16,129,128]{2,1,0:T(8,128)(2,1)}), bf16[16,129,128]{2,1,0:T(8,128)(2,1)}, u32[]{:S(2)}, u32[]{:S(2)}) async-start(bf16[16,129,128]{2,1,0:T(8,128)(2,1)} %broadcast_in_dim.158), calls=%async_computation.1 | async-start | bytes 1114112 | tf_op jit(solution)/shard_map/all_to_all | solution.py:321
  94.7 8.6 %copy-start.11 = (f32[1024,128]{1,0:T(8,128)}, f32[1024,128]{1,0:T(8,128)S(1)}, u32[]{:S(2)}) copy-start(f32[1024,128]{1,0:T(8,128)S(1)} %reverse.10) | copy-start | bytes 1572868
  96.8 2.1 copy-start.14
  98.9 3.2 %copy-start.20 = (f32[1024,128]{1,0:T(8,128)S(1)}, f32[1024,128]{1,0:T(8,128)}, u32[]{:S(2)}) copy-start(f32[1024,128]{1,0:T(8,128)} %reverse.11) | copy-start | bytes 1572868
  99.7 0.8 copy-start.17
  102.1 2.4 copy-start.22
  108.2 4.5 %copy-start.15 = (f32[1024,128]{1,0:T(8,128)S(1)}, f32[1024,128]{1,0:T(8,128)}, u32[]{:S(2)}) copy-start(f32[1024,128]{1,0:T(8,128)} %copy-done.13) | copy-start | bytes 1572868
  110.2 2.5 copy-start.16
  110.2 3.7 %copy-start.26 = (f32[8,128,2,64]{1,0,3,2:T(8,128)S(1)}, f32[8,128,2,64]{1,0,3,2:T(8,128)}, u32[]{:S(2)}) copy-start(f32[8,128,2,64]{1,0,3,2:T(8,128)} %get-tuple-element.17) | copy-start | bytes 1572868
  116.2 3.1 %copy-start.18 = (f32[8,2,64,128]{3,2,1,0:T(8,128)S(1)}, f32[8,2,64,128]{3,2,1,0:T(8,128)}, u32[]{:S(2)}) copy-start(f32[8,2,64,128]{3,2,1,0:T(8,128)} %copy-done.17) | copy-start | bytes 1572868
  121.1 32.0 %all-to-all-start = ((bf16[16,129,128]{2,1,0:T(8,128)(2,1)}), bf16[16,129,128]{2,1,0:T(8,128)(2,1)}, u32[]{:S(2)}, u32[]{:S(2)}) async-start(bf16[16,129,128]{2,1,0:T(8,128)(2,1)} %broadcast_in_dim.153), calls=%async_computation | async-start | bytes 1114112 | tf_op jit(solution)/shard_map/all_to_all | solution.py:321
  155.5 1.0 copy-start.12
  155.5 1.2 copy-start.25
  164.5 1.0 copy-start.23
  164.5 1.2 copy-start.24
  172.1 17.7 %all-to-all-start.2 = ((f32[8,1,1024]{2,1,0:T(1,128)}), f32[8,1,1024]{2,1,0:T(1,128)S(1)}, u32[]{:S(2)}, u32[]{:S(2)}) async-start(f32[8,1,1024]{2,1,0:T(1,128)} %broadcast_in_dim.160), calls=%async_computation.2 | async-start | bytes 65536 | tf_op jit(solution)/shard_map/all_to_all | solution.py:321

commit v2 on v1

v2 whole, which is shorter than its diff:
```python
import functools

import jax
import jax.numpy as jnp
from jax import lax
from jax.experimental import pallas as pl
from jax.experimental.pallas import tpu as pltpu
from jax.sharding import PartitionSpec as P

DUALITY_HEADS = 16
STATE = 128
SPAN = 128
D_SSM = 1024
EPSILON = 1e-06
HIGHEST = lax.Precision.HIGHEST

MESH = pl.DeviceIdType.MESH
A_COLS = 384
W_COLS = 896
HALO = 16
TOK_ROWS = 128
PIECE = 32


def remote(src, dst, send, recv, where):
    return pltpu.make_async_remote_copy(
        src_ref=src, dst_ref=dst, send_sem=send, recv_sem=recv, device_id=where, device_id_type=MESH
    )


def entry_barrier(places):
    barrier = pltpu.get_barrier_semaphore()
    for where in places:
        pl.semaphore_signal(barrier, inc=1, device_id=where, device_id_type=MESH)
    pl.semaphore_wait(barrier, len(places))


def gather_kernel(
    n_sp, n_fs, n_x,
    tok, wg, wv, wk, wq, wp, wo, wstep, gain,
    proj, raw, wout,
    tokbuf, wbuf,
    local_sem, out_sem,
    tp_sem, tm_sem, tr_sem, td_sem,
    ay_sem, azp_sem, azm_sem, bzp_sem, bzm_sem, byp_sem, bym_sem, byo_sem, h_sem,
    send_sem,
):
    z, y, t = lax.axis_index("sp"), lax.axis_index("fs"), lax.axis_index("tp")
    x, c = t // 2, t % 2
    xp, xm = (x + 1) % n_x, (x + n_x - 1) % n_x
    yp, ym = (y + 1) % n_fs, (y + n_fs - 1) % n_fs
    zp, zm = (z + 1) % n_sp, (z + n_sp - 1) % n_sp
    to_xp, to_xm, to_d = {"tp": xp * 2 + c}, {"tp": xm * 2 + c}, {"tp": x * 2 + 1 - c}
    to_yp, to_ym = {"fs": yp}, {"fs": ym}
    to_zp, to_zm = {"sp": zp}, {"sp": zm}

    def trow(xx, cc, q):
        return pl.multiple_of(HALO + (xx * 2 + cc) * TOK_ROWS + q * PIECE, 16)

    def wrow(zz, yy):
        return pl.multiple_of((zz * n_fs + yy) * PIECE, PIECE)

    def a_at(zz, yy):
        return wbuf.at[pl.ds(wrow(zz, yy), PIECE), pl.ds(0, A_COLS)]

    def b_at(zz, yy):
        return wbuf.at[pl.ds(wrow(zz, yy), PIECE), pl.ds(A_COLS, W_COLS - A_COLS)]

    def t_at(xx, cc, q, rows=PIECE):
        return tokbuf.at[pl.ds(trow(xx, cc, q), rows), :]

    locals_ = [pltpu.make_async_copy(tok.at[0], t_at(x, c, 0, TOK_ROWS), local_sem.at[0])]
    for i, w in enumerate((wg, wv, wk, wq, wp)):
        locals_.append(
            pltpu.make_async_copy(
                w, wbuf.at[pl.ds(wrow(z, y), PIECE), pl.ds(i * 128, 128)], local_sem.at[1 + i]
            )
        )
    locals_.append(
        pltpu.make_async_copy(
            wo, wbuf.at[pl.ds(wrow(z, y), PIECE), pl.ds(640, 256)], local_sem.at[6]
        )
    )
    for copy in locals_:
        copy.start()
    entry_barrier((to_xp, to_xm, to_yp, to_ym, to_zp, to_zm, to_d))

    sent = []

    def send(ref, recv, where):
        copy = remote(ref, ref, send_sem.at[len(sent)], recv, where)
        copy.start()
        sent.append(copy)

    def arrived(ref, recv):
        remote(ref, ref, send_sem.at[0], recv, to_d).wait_recv()

    for copy in locals_[1:]:
        copy.wait()
    own_a, own_b = a_at(z, y), b_at(z, y)
    send(own_a, ay_sem.at[0], to_yp)
    send(own_a, ay_sem.at[1], to_ym)
    send(own_a, azp_sem.at[4], to_zp)
    send(own_a, azm_sem.at[4], to_zm)
    send(own_b, bzp_sem.at[1], to_zp)
    send(own_b, bzm_sem.at[1], to_zm)
    locals_[0].wait()
    for q in (0, 1, 2, 3):
        send(t_at(x, c, q), tp_sem.at[q], to_xp)
    for q in (2, 3, 0, 1):
        send(t_at(x, c, q), tm_sem.at[q], to_xm)
    send(own_b, byp_sem.at[0], to_yp)
    send(own_b, bym_sem.at[0], to_ym)
    send(t_at(x, c, 0, TOK_ROWS), td_sem.at[12], to_d)

    yo = (y + 2) % n_fs
    y_of = (y, ym, yp, yo)
    arrived(a_at(z, ym), ay_sem.at[0])
    send(a_at(z, ym), ay_sem.at[2], to_yp)
    send(a_at(z, ym), azp_sem.at[5], to_zp)
    send(a_at(z, ym), azm_sem.at[5], to_zm)
    arrived(a_at(z, yp), ay_sem.at[1])
    send(a_at(z, yp), azp_sem.at[6], to_zp)
    send(a_at(z, yp), azm_sem.at[6], to_zm)
    arrived(a_at(z, yo), ay_sem.at[2])
    send(a_at(z, yo), azp_sem.at[7], to_zp)
    send(a_at(z, yo), azm_sem.at[7], to_zm)

    half = n_sp // 2

    def back(o):
        return (z + n_sp - o) % n_sp

    def relay_y(o):
        arrived(b_at(back(o), ym), byp_sem.at[o])
        if o % 2 == 0:
            send(b_at(back(o), ym), byo_sem.at[o], to_yp)
        arrived(b_at(back(o), yp), bym_sem.at[o])
        if o % 2 == 1:
            send(b_at(back(o), yp), byo_sem.at[o], to_ym)

    def token_step(k):
        if k <= 4:
            q = k - 1
            arrived(t_at(xm, c, q), tp_sem.at[q])
            if q < 2:
                send(t_at(xm, c, q), tr_sem.at[q], to_xp)
            send(t_at(xm, c, q), td_sem.at[q], to_d)
            q = (2, 3, 0, 1)[k - 1]
            arrived(t_at(xp, c, q), tm_sem.at[q])
            if q >= 2:
                send(t_at(xp, c, q), tr_sem.at[q], to_xm)
            send(t_at(xp, c, q), td_sem.at[4 + q], to_d)
        elif k <= 6:
            for q in (k - 5, k - 3):
                xo = (x + 2) % n_x
                arrived(t_at(xo, c, q), tr_sem.at[q])
                send(t_at(xo, c, q), td_sem.at[8 + q], to_d)

    pending = [0]
    for k in range(1, half + 1):
        far = k == half
        for j in range(4):
            if not far or j < 2:
                ref = a_at(back(k), y_of[j])
                arrived(ref, azp_sem.at[4 * k + j])
                if k + 1 < half or (k + 1 == half and j < 2):
                    send(ref, azp_sem.at[4 * (k + 1) + j], to_zp)
            if not far or j >= 2:
                ref = a_at((z + k) % n_sp, y_of[j])
                arrived(ref, azm_sem.at[4 * k + j])
                if k + 1 < half or (k + 1 == half and j >= 2):
                    send(ref, azm_sem.at[4 * (k + 1) + j], to_zm)
            if j == 1:
                token_step(k)
        fresh = []
        ref = b_at(back(k), y)
        arrived(ref, bzp_sem.at[k])
        if k < half:
            send(ref, bzp_sem.at[k + 1], to_zp)
        send(ref, byp_sem.at[k], to_yp)
        send(ref, bym_sem.at[k], to_ym)
        fresh.append(k)
        if not far:
            o = n_sp - k
            ref = b_at(back(o), y)
            arrived(ref, bzm_sem.at[k])
            if k + 1 < half:
                send(ref, bzm_sem.at[k + 1], to_zm)
            send(ref, byp_sem.at[o], to_yp)
            send(ref, bym_sem.at[o], to_ym)
            fresh.append(o)
        for o in pending:
            relay_y(o)
        pending = fresh

    cs = 1 - c
    arrived(t_at(x, cs, 0, TOK_ROWS), td_sem.at[12])
    for q in range(4):
        arrived(t_at(xm, cs, q), td_sem.at[q])
        arrived(t_at(xp, cs, q), td_sem.at[4 + q])
        arrived(t_at((x + 2) % n_x, cs, q), td_sem.at[8 + q])
    rows = 2 * n_x * TOK_ROWS
    last = tokbuf.at[pl.ds(rows, HALO), :]
    first = tokbuf.at[pl.ds(HALO, HALO), :]
    before = tokbuf.at[pl.ds(0, HALO), :]
    after = tokbuf.at[pl.ds(HALO + rows, HALO), :]
    halo_up = remote(last, before, send_sem.at[len(sent)], h_sem.at[0], to_zp)
    halo_up.start()
    sent.append(halo_up)
    halo_down = remote(first, after, send_sem.at[len(sent)], h_sem.at[1], to_zm)
    halo_down.start()
    sent.append(halo_down)
    for o in pending:
        relay_y(o)
    for o in range(n_sp):
        arrived(b_at(back(o), yo), byo_sem.at[o])
    to_out = pltpu.make_async_copy(wbuf.at[:, pl.ds(640, 256)], wout, out_sem)
    to_out.start()

    def project(begin, count):
        part = tokbuf[pl.ds(begin, count), :].astype(jnp.float32)
        scaling = lax.rsqrt(jnp.mean(part * part, axis=-1, keepdims=True) + EPSILON)
        normed = (part * scaling * gain[...]).astype(jnp.bfloat16)
        proj[pl.ds(begin, count), :] = jnp.dot(
            normed, wbuf[:, 0:640], preferred_element_type=jnp.float32
        ).astype(jnp.bfloat16)
        return normed

    def step(i, carry):
        begin = pl.multiple_of(HALO + i * 256, 16)
        normed = project(begin, 256)
        raw[pl.ds(pl.multiple_of(i * 256, 256), 256), :] = jnp.dot(
            normed, wstep[...], preferred_element_type=jnp.float32
        )
        return carry

    lax.fori_loop(0, rows // 256, step, 0)
    remote(before, before, send_sem.at[0], h_sem.at[0], to_d).wait_recv()
    remote(after, after, send_sem.at[0], h_sem.at[1], to_d).wait_recv()
    project(0, HALO)
    project(HALO + rows, HALO)
    to_out.wait()
    for copy in sent:
        copy.wait_send()


N_SENDS = 191


def gather_and_project(n_sp, n_fs, n_x, tok, ws, wo, wstep, gain):
    rows = 2 * n_x * TOK_ROWS
    any_spec = pl.BlockSpec(memory_space=pl.ANY)
    vmem = pl.BlockSpec(memory_space=pltpu.VMEM)
    dma = pltpu.SemaphoreType.DMA
    return pl.pallas_call(
        functools.partial(gather_kernel, n_sp, n_fs, n_x),
        out_shape=(
            jax.ShapeDtypeStruct((rows + 2 * HALO, 640), jnp.bfloat16),
            jax.ShapeDtypeStruct((rows, 128), jnp.float32),
            jax.ShapeDtypeStruct((2048, 256), jnp.bfloat16),
        ),
        in_specs=[any_spec] * 7 + [vmem, vmem],
        out_specs=(vmem, vmem, any_spec),
        scratch_shapes=[
            pltpu.VMEM((rows + 2 * HALO, 2048), jnp.bfloat16),
            pltpu.VMEM((2048, W_COLS), jnp.bfloat16),
            dma((7,)),
            dma,
            dma((4,)), dma((4,)), dma((4,)), dma((13,)),
            dma((3,)), dma((36,)), dma((36,)), dma((9,)), dma((9,)),
            dma((16,)), dma((16,)), dma((16,)), dma((2,)),
            dma((N_SENDS,)),
        ],
        compiler_params=pltpu.CompilerParams(
            collective_id=0, has_side_effects=True, vmem_limit_bytes=48 * 1024 * 1024
        ),
        name="gather_and_project",
    )(tok, *ws, wo, wstep, gain)


NT = (((1,), (1,)), ((), ()))
TN = (((0,), (0,)), ((), ()))
N_BLOCKS = 8
MSG = STATE + 16


def silu(v):
    return v / (1.0 + jnp.exp(-v))


def mix_kernel(
    n_sp, n_x,
    proj, raw, wout, bias, rate, shift, tap_v, tap_k, tap_q, mgain, pmix, pgain,
    out,
    p32, xbuf, kbuf, qbuf, ends, ybuf, mix,
    incl, excl, itot, etot, msg_out, msg_in, ss_out, ss_in,
    d_out, d_in, r_out, r_in, n_out, n_in,
    msg_send, msg_recv, ss_send, ss_recv, d_send, d_recv, r_send, r_recv, n_send, n_recv,
):
    f32, bf16 = jnp.float32, jnp.bfloat16
    z, t = lax.axis_index("sp"), lax.axis_index("tp")
    x, c = t // 2, t % 2
    n_tp = 2 * n_x
    xp, xm, xo = (x + 1) % n_x, (x + n_x - 1) % n_x, (x + 2) % n_x
    to_xp, to_xm, to_d = {"tp": xp * 2 + c}, {"tp": xm * 2 + c}, {"tp": x * 2 + 1 - c}
    distances = [1, 2, 4, 8]
    barrier = pltpu.get_barrier_semaphore()
    partners = [{"tp": (t + r) % n_tp} for r in range(1, n_tp)]
    partners += [{"sp": (z + d) % n_sp} for d in distances]
    partners += [{"sp": (z + n_sp - d) % n_sp} for d in distances if 2 * d != n_sp]
    for where in partners:
        pl.semaphore_signal(barrier, inc=1, device_id=where, device_id_type=MESH)

    lane0 = pl.multiple_of(t * 128, 128)
    rows = N_BLOCKS * SPAN
    p32[...] = proj[:, 128:640].astype(f32)

    @pl.when(z == 0)
    def _():
        p32[0:HALO, :] = jnp.zeros((HALO, 512), f32)

    @pl.when(z == n_sp - 1)
    def _():
        p32[HALO + rows : HALO + rows + HALO, :] = jnp.zeros((HALO, 512), f32)

    row8 = lax.broadcasted_iota(jnp.int32, (8, 128), 0)

    def by_kind(parts):
        found = jnp.zeros((8, 128), f32)
        for i, part in enumerate(parts):
            found = jnp.where(row8 == i, part, found)
        return found

    kinds = ((0, 0), (0, 1), (1, 0), (1, 1))
    bias8 = by_kind([bias[r, 2 * t + h] for r, h in kinds])
    rate8 = by_kind([rate[r, 2 * t + h] for r, h in kinds])
    steps_l, logs_l = [], []
    for b in range(N_BLOCKS):
        cols = raw[b * SPAN : (b + 1) * SPAN, :].T[0:8, :] + bias8
        steps = jnp.maximum(cols, 0.0) + jnp.log1p(jnp.exp(-jnp.abs(cols)))
        moved = by_kind([shift[0, h, r : r + 1, b * SPAN : (b + 1) * SPAN] for r, h in kinds])
        steps_l.append(steps)
        logs_l.append(jnp.where(row8 < 4, -rate8 * steps - moved, 0.0))
    steps = jnp.concatenate(steps_l, axis=0)
    logs = jnp.concatenate(logs_l, axis=0)
    lane = lax.broadcasted_iota(jnp.int32, (64, 128), 1)
    kind = lax.broadcasted_iota(jnp.int32, (64, 128), 0) % 8
    prefix, suffix = logs, logs
    for k in (1, 2, 4, 8, 16, 32, 64):
        prefix = prefix + jnp.where(lane >= k, pltpu.roll(prefix, k, 1), 0.0)
        suffix = suffix + jnp.where(lane < 128 - k, pltpu.roll(suffix, 128 - k, 1), 0.0)
    cum = jnp.where(kind < 2, prefix, suffix)
    total = jnp.broadcast_to(jnp.sum(logs, axis=1, keepdims=True), (64, 128))
    tail = jnp.exp(jnp.minimum(total - cum, 0.0)) * steps
    decay = jnp.exp(total)
    cum_tail_t = jnp.concatenate([cum, tail], axis=0).T
    reach_t = jnp.concatenate([jnp.exp(cum), jnp.zeros((64, 128), f32)], axis=0).T

    def wide(cols, b, first):
        j = b * 8 + first
        left = jnp.broadcast_to(cols[:, j : j + 1], (128, 64))
        right = jnp.broadcast_to(cols[:, j + 1 : j + 2], (128, 64))
        return jnp.concatenate([left, right], axis=1)

    def tall(rows_, b, first):
        j = b * 8 + first
        top = jnp.broadcast_to(rows_[j : j + 1, :], (64, 128))
        bottom = jnp.broadcast_to(rows_[j + 1 : j + 2, :], (64, 128))
        return jnp.concatenate([top, bottom], axis=0)

    def window(b, j):
        begin = HALO - 8 + b * SPAN
        return p32[begin : begin + SPAN + 16, j * 128 : (j + 1) * 128]

    def conv(b, j, taps):
        v = window(b, j)
        weights = taps[:, pl.ds(lane0, 128)].astype(f32)
        total_ = v * weights[2:3, :]
        for i in (0, 1, 3, 4):
            total_ = total_ + pltpu.roll(v, (2 - i) % (SPAN + 16), 0) * weights[i : i + 1, :]
        return silu(total_[8 : 8 + SPAN, :])

    for b in range(N_BLOCKS):
        at = slice(b * SPAN, (b + 1) * SPAN)
        values = conv(b, 0, tap_v)
        keys = conv(b, 1, tap_k).astype(bf16)
        xbuf[at, :] = values
        kbuf[at, :] = keys
        both = jnp.concatenate(
            [values * wide(cum_tail_t, b, 64), values * wide(cum_tail_t, b, 66)], axis=1
        )
        ends[b] = lax.dot_general(both.astype(bf16), keys, TN, preferred_element_type=f32)

    forward = ends[0, 0:128, :]
    backward = ends[N_BLOCKS - 1, 128:256, :]
    for i in range(1, N_BLOCKS):
        b = N_BLOCKS - 1 - i
        forward = forward * tall(decay, i, 0) + ends[i, 0:128, :]
        backward = backward * tall(decay, b, 2) + ends[b, 128:256, :]
    sums = total[0:8, :]
    for b in range(1, N_BLOCKS):
        sums = sums + total[b * 8 : b * 8 + 8, :]
    incl[0] = forward
    incl[1] = backward
    excl[...] = jnp.zeros_like(excl)
    itot[...] = jnp.broadcast_to(sums[None], (2, 8, 128))
    etot[...] = jnp.zeros_like(etot)

    def heads_decay(logs8, direction):
        return jnp.exp(tall(logs8, 0, 2 * direction))

    def exchange(i):
        d = distances[i]
        for way in (0, 1):
            there = z + d if way == 0 else z - d
            ok = there < n_sp if way == 0 else there >= 0
            logs8 = itot[way]
            high = logs8.astype(bf16)
            low = (logs8 - high.astype(f32)).astype(bf16)
            msg_out[way, i, 0:STATE, :] = incl[way].astype(bf16)
            msg_out[way, i, STATE:MSG, :] = jnp.concatenate([high, low], axis=0)
            where = {"sp": (z + d) % n_sp if way == 0 else (z + n_sp - d) % n_sp}

            @pl.when(ok)
            def _():
                remote(
                    msg_out.at[way, i], msg_in.at[way, i],
                    msg_send.at[way, i], msg_recv.at[way, i], where,
                ).start()

    def combine(i):
        d = distances[i]
        for way in (0, 1):
            ok = z >= d if way == 0 else z + d < n_sp

            @pl.when(ok)
            def _():
                remote(
                    msg_out.at[way, i], msg_in.at[way, i],
                    msg_send.at[way, i], msg_recv.at[way, i], to_d,
                ).wait_recv()
                state = msg_in[way, i, 0:STATE, :].astype(f32)
                pair = msg_in[way, i, STATE:MSG, :].astype(f32)
                logs8 = pair[0:8, :] + pair[8:16, :]
                excl[way] = excl[way] + heads_decay(etot[way], way) * state
                etot[way] = etot[way] + logs8
                incl[way] = incl[way] + heads_decay(itot[way], way) * state
                itot[way] = itot[way] + logs8

    row = lax.broadcasted_iota(jnp.int32, (128, 128), 0)
    col = lax.broadcasted_iota(jnp.int32, (128, 128), 1)

    def within(b):
        at = slice(b * SPAN, (b + 1) * SPAN)
        queries = conv(b, 2, tap_q).astype(bf16)
        qbuf[at, :] = queries
        scores = lax.dot_general(queries, kbuf[at, :], NT, preferred_element_type=f32)
        masked = []
        for h in (0, 1):
            jf, jb = b * 8 + h, b * 8 + 2 + h
            ahead = cum_tail_t[:, jf : jf + 1] - cum[jf : jf + 1, :]
            behind = cum_tail_t[:, jb : jb + 1] - cum[jb : jb + 1, :]
            gaps = jnp.where(col < row, ahead, jnp.where(col > row, behind, 0.0))
            df, db = steps[jf : jf + 1, :], steps[jb : jb + 1, :]
            sizes = jnp.where(col < row, df, jnp.where(col > row, db, df + db))
            masked.append((scores * jnp.exp(jnp.minimum(gaps, 0.0)) * sizes).astype(bf16))
        values = xbuf[at, :]
        stacked = jnp.concatenate(
            [jnp.where(col < 64, values, 0.0), jnp.where(col >= 64, values, 0.0)], axis=0
        ).astype(bf16)
        ybuf[at, :] = jnp.dot(
            jnp.concatenate(masked, axis=1), stacked, preferred_element_type=f32
        )

    def pool(b):
        at = slice(b * SPAN, (b + 1) * SPAN)
        n = SPAN + 16
        v = window(b, 3)
        w2 = v + pltpu.roll(v, 1, 0)
        w4 = pltpu.roll(w2, 1, 0) + pltpu.roll(w2, n - 1, 0)
        w8 = pltpu.roll(w4, 2, 0) + pltpu.roll(w4, n - 2, 0)
        w16 = pltpu.roll(w8, 4, 0) + pltpu.roll(w8, n - 4, 0)
        which = t % 4
        summed = jnp.where(
            which == 0, w2, jnp.where(which == 1, w4, jnp.where(which == 2, w8, w16))
        )[8 : 8 + SPAN, :]
        reach = jnp.where(which == 0, 1, jnp.where(which == 1, 2, jnp.where(which == 2, 4, 8)))
        place = z * rows + b * SPAN + row
        upper = jnp.minimum(place + reach, n_sp * rows)
        lower = jnp.maximum(place - reach, 0)
        differences = summed / (upper - lower).astype(f32) - v[8 : 8 + SPAN, :]
        mapped = jnp.dot(differences.astype(bf16), pmix[t], preferred_element_type=f32)
        mix[at, 128:256] = (mapped * pgain[:, pl.ds(lane0, 128)]).astype(bf16)

    pl.semaphore_wait(barrier, len(partners))
    exchange(0)
    within(0)
    within(1)
    combine(0)
    exchange(1)
    within(2)
    within(3)
    combine(1)
    exchange(2)
    within(4)
    within(5)
    within(6)
    within(7)
    combine(2)
    exchange(3)
    for b in range(N_BLOCKS):
        pool(b)
    combine(3)

    forward, backward = excl[0], excl[1]
    entering = [None] * N_BLOCKS
    leaving = [None] * N_BLOCKS
    for i in range(N_BLOCKS):
        b = N_BLOCKS - 1 - i
        entering[i] = forward.astype(bf16)
        leaving[b] = backward.astype(bf16)
        forward = forward * tall(decay, i, 0) + ends[i, 0:128, :]
        backward = backward * tall(decay, b, 2) + ends[b, 128:256, :]
    squares = []
    for b in range(N_BLOCKS):
        at = slice(b * SPAN, (b + 1) * SPAN)
        states = jnp.concatenate([entering[b], leaving[b]], axis=0)
        carried = lax.dot_general(qbuf[at, :], states, NT, preferred_element_type=f32)
        heads_out = (
            ybuf[at, :]
            + carried[:, 0:128] * wide(reach_t, b, 0)
            + carried[:, 128:256] * wide(reach_t, b, 2)
        )
        gate = proj[HALO + b * SPAN : HALO + (b + 1) * SPAN, 0:128].astype(f32)
        gated = heads_out * silu(gate)
        ybuf[at, :] = gated
        squares.append(
            lax.dot_general(
                jnp.ones((8, 128), f32), gated * gated, NT,
                precision=HIGHEST, preferred_element_type=f32,
            )[0:1, :]
        )
    own_squares = jnp.concatenate(squares, axis=0)
    ss_out[...] = own_squares
    ss_copies = []
    for r in range(1, n_tp):
        copy = remote(
            ss_out, ss_in.at[r - 1], ss_send.at[r - 1], ss_recv.at[r - 1],
            {"tp": (t + r) % n_tp},
        )
        copy.start()
        ss_copies.append(copy)
    all_squares = own_squares
    for r in range(1, n_tp):
        ss_copies[r - 1].wait_recv()
        all_squares = all_squares + ss_in[r - 1]
    scale = lax.rsqrt(all_squares / D_SSM + EPSILON)
    scale_t = jnp.concatenate([scale, jnp.zeros((120, 128), f32)], axis=0).T
    gain = mgain[:, pl.ds(lane0, 128)]
    for b in range(N_BLOCKS):
        at = slice(b * SPAN, (b + 1) * SPAN)
        mix[at, 0:128] = (ybuf[at, :] * scale_t[:, b : b + 1] * gain).astype(bf16)

    def partial(xx, cc, begin=0, count=TOK_ROWS):
        at = pl.multiple_of((xx * 2 + cc) * TOK_ROWS + begin, 16)
        return lax.dot_general(
            mix[pl.ds(at, count), :], wout[...], NT, preferred_element_type=f32
        )

    half = TOK_ROWS // 2
    d_copies = []
    for i, xx in enumerate((xo, xp, xm, x)):
        d_out[i] = partial(xx, 1 - c).astype(bf16)
        copy = remote(d_out.at[i], d_in.at[i], d_send.at[i], d_recv.at[i], to_d)
        copy.start()
        d_copies.append(copy)

    def chip(i, xx, begin, count=half):
        return partial(xx, c, begin, count) + d_in[i, begin : begin + count, :].astype(f32)

    def send(i, value, where, out_ref, in_ref, send_sem, recv_sem):
        out_ref[i] = value.astype(bf16)
        copy = remote(out_ref.at[i], in_ref.at[i], send_sem.at[i], recv_sem.at[i], where)
        copy.start()
        return copy

    relay = (r_out, r_in, r_send, r_recv)
    near = (n_out, n_in, n_send, n_recv)
    d_copies[0].wait_recv()
    relay_p = send(0, chip(0, xo, 0), to_xp, *relay)
    relay_m = send(1, chip(0, xo, half), to_xm, *relay)
    d_copies[1].wait_recv()
    dir_p = send(0, chip(1, xp, half), to_xp, *near)
    d_copies[2].wait_recv()
    dir_m = send(1, chip(2, xm, 0), to_xm, *near)
    relay_p.wait_recv()
    comb_p = send(2, chip(1, xp, 0) + r_in[0].astype(f32), to_xp, *near)
    relay_m.wait_recv()
    comb_m = send(3, chip(2, xm, half) + r_in[1].astype(f32), to_xm, *near)
    d_copies[3].wait_recv()
    top, bottom = chip(3, x, 0), chip(3, x, half)
    dir_p.wait_recv()
    dir_m.wait_recv()
    bottom = bottom + n_in[0].astype(f32)
    top = top + n_in[1].astype(f32)
    comb_p.wait_recv()
    out[0, 0:half, :] = (top + n_in[2].astype(f32)).astype(bf16)
    comb_m.wait_recv()
    out[0, half:TOK_ROWS, :] = (bottom + n_in[3].astype(f32)).astype(bf16)

    for i, d in enumerate(distances):
        for way in (0, 1):
            ok = z + d < n_sp if way == 0 else z >= d

            @pl.when(ok)
            def _():
                remote(
                    msg_out.at[way, i], msg_in.at[way, i],
                    msg_send.at[way, i], msg_recv.at[way, i], to_d,
                ).wait_send()

    for copy in ss_copies + d_copies + [relay_p, relay_m, dir_p, dir_m, comb_p, comb_m]:
        copy.wait_send()


def mixed_and_summed(
    n_sp, n_x, proj, raw, wout, bias, rate, shift, tap_v, tap_k, tap_q, mgain, pmix, pgain
):
    vmem = pl.BlockSpec(memory_space=pltpu.VMEM)
    smem = pl.BlockSpec(memory_space=pltpu.SMEM)
    dma = pltpu.SemaphoreType.DMA
    f32, bf16 = jnp.float32, jnp.bfloat16
    rows = N_BLOCKS * SPAN
    half = TOK_ROWS // 2
    return pl.pallas_call(
        functools.partial(mix_kernel, n_sp, n_x),
        out_shape=jax.ShapeDtypeStruct((1, TOK_ROWS, 2048), bf16),
        in_specs=[vmem] * 3 + [smem] * 2 + [vmem] * 7,
        out_specs=vmem,
        scratch_shapes=[
            pltpu.VMEM((rows + 2 * HALO, 512), f32),
            pltpu.VMEM((rows, 128), f32),
            pltpu.VMEM((rows, 128), bf16),
            pltpu.VMEM((rows, 128), bf16),
            pltpu.VMEM((N_BLOCKS, 256, 128), f32),
            pltpu.VMEM((rows, 128), f32),
            pltpu.VMEM((rows, 256), bf16),
            pltpu.VMEM((2, 128, 128), f32),
            pltpu.VMEM((2, 128, 128), f32),
            pltpu.VMEM((2, 8, 128), f32),
            pltpu.VMEM((2, 8, 128), f32),
            pltpu.VMEM((2, 4, MSG, 128), bf16),
            pltpu.VMEM((2, 4, MSG, 128), bf16),
            pltpu.VMEM((8, 128), f32),
            pltpu.VMEM((7, 8, 128), f32),
            pltpu.VMEM((4, TOK_ROWS, 2048), bf16),
            pltpu.VMEM((4, TOK_ROWS, 2048), bf16),
            pltpu.VMEM((2, half, 2048), bf16),
            pltpu.VMEM((2, half, 2048), bf16),
            pltpu.VMEM((4, half, 2048), bf16),
            pltpu.VMEM((4, half, 2048), bf16),
            dma((2, 4)), dma((2, 4)), dma((7,)), dma((7,)),
            dma((4,)), dma((4,)), dma((2,)), dma((2,)), dma((4,)), dma((4,)),
        ],
        compiler_params=pltpu.CompilerParams(
            collective_id=1, has_side_effects=True, vmem_limit_bytes=56 * 1024 * 1024
        ),
        name="mixed_and_summed",
    )(proj, raw, wout, bias, rate, shift, tap_v, tap_k, tap_q, mgain, pmix, pgain)


def local(
    tokens, norm_gain, w_gate, w_value, w_bkey, w_query, w_pool_in, w_step, step_bias,
    decay_rate, decay_shift, conv_value, conv_bkey, conv_query, mix_gain, pool_mix, pool_gain,
    w_out_ssd, w_out_pool,
):
    n_tp, n_sp, n_fs = lax.axis_size("tp"), lax.axis_size("sp"), lax.axis_size("fs")
    heads_dev = DUALITY_HEADS // n_tp
    step_cols = lax.dynamic_slice_in_dim(w_step, lax.axis_index("tp") * heads_dev, heads_dev, 2)
    step_cols = jnp.pad(step_cols.reshape(w_step.shape[0], 2 * heads_dev), ((0, 0), (0, 124)))
    out_turned = jnp.concatenate([w_out_ssd.T, w_out_pool.T], axis=1)
    projected, raw_steps, wout = gather_and_project(
        n_sp, n_fs, n_tp // 2, tokens, (w_gate, w_value, w_bkey, w_query, w_pool_in),
        out_turned, step_cols, norm_gain[None],
    )
    return mixed_and_summed(
        n_sp, n_tp // 2, projected, raw_steps, wout, step_bias, decay_rate, decay_shift,
        conv_value, conv_bkey, conv_query, mix_gain[None], pool_mix, pool_gain[None],
    )


def solution(mesh):
    return jax.shard_map(
        local,
        mesh=mesh,
        in_specs=(
            P("fs", ("sp", "tp"), None),
            P(),
            P(("sp", "fs"), "tp"),
            P(("sp", "fs"), "tp"),
            P(("sp", "fs"), "tp"),
            P(("sp", "fs"), "tp"),
            P(("sp", "fs"), "tp"),
            P(),
            P(),
            P(),
            P("fs", "tp", None, "sp"),
            P(),
            P(),
            P(),
            P(),
            P(),
            P(),
            P("tp", ("sp", "fs")),
            P("tp", ("sp", "fs")),
        ),
        out_specs=P("fs", ("sp", "tp"), None),
        check_vma=False,
    )
```

time: 262 us -> 130 us (0.50)
  Pallas kernels: 55.8 us -> 123 us
  blocking collectives: 53.8 us -> 0 us
  local copies, waits for them, and re-layouts: 48 us -> 6.05 us
  matrix products: 34 us -> 0 us
  starting transfers between devices: 32.2 us -> 0 us
  other arithmetic: 19.4 us -> 0.72 us
  waiting for transfers between devices: 16.2 us -> 0 us
    pallas_call x0 -> x1, Pallas kernels: none -> 66.9 us  [mixed_and_summed(): pl.pallas_call(functools.partial(mix_kernel, n_sp, n_x), out_shape=jax.Sh...]
    all_to_all x1 -> x0, blocking collectives: 53.8 us -> none  [sent_and_summed(): lax.all_to_all(tiles, axis, split_axis=0, concat_axis=0, tiled=True)]
    dot_general x16 -> x0, matrix products: 34 us -> none  [the longest x1 7.06 us: local(): jnp.dot(pool_out, out_pool_rows, preferred_element_type=jnp.float32)]
    all_to_all x3 -> x0, starting transfers between devices: 32.2 us -> none  [from_everyone(): lax.all_to_all(jnp.broadcast_to(x[None], (length, *x.shape)), axis, 0, 0,...]
    all_to_all x3 -> x0, waiting for transfers between devices: 16.2 us -> none  [from_everyone(): lax.all_to_all(jnp.broadcast_to(x[None], (length, *x.shape)), axis, 0, 0,...]
    rev x4 -> x0, local copies, waits for them, and re-layouts: 11.5 us -> none  [the longest x1 5.04 us: local(): values[::-1]]
    slice x26 -> x0, local copies, waits for them, and re-layouts: 9.4 us -> none  [the longest x4 3.71 us: gathered_once(): slab = both[:, at:at + len(line)].reshape(len(both), -1)]
    reduce_sum x4 -> x0, other arithmetic: 7.73 us -> none  [the longest x1 3.85 us: sent_and_summed(): return arrived.astype(jnp.float32).sum(axis=0)]
  transfers between devices with their start and end apart: 3 -> 0, of which waited for: 2 -> 0; matrix products, arithmetic and copies ran while one was open for 15% -> 0% of each run, Pallas kernels for 0% -> 0%
where the time goes in v2:
time: 130 us; the launch traced here: 129 us
  Pallas kernels  123 us (95%)
  local copies, waits for them, and re-layouts  6.05 us (5%)
    pallas_call x1, Pallas kernels, mixed_and_summed(): pl.pallas_call(functools.partial(mix_kernel, n_sp, n_x), out_shape=jax.Sh...  66.9 us
    pallas_call x1, Pallas kernels, gather_and_project(): pl.pallas_call(functools.partial(gather_kernel, n_sp, n_fs, n_x), out_sha...  55.7 us
    unnamed x23, local copies, waits for them, and re-layouts  5.59 us

profile of v2, /device:TPU:1, one launch (start us, length us, event | category | flops | bytes accessed | tf_op | source)
XLA Modules:
  0.0 129.5 jit_solution(17043162143268047921)
XLA Ops:
  0.0 0.0 copy-start
  0.0 0.0 copy-start.9
  0.0 0.0 copy-start.8
  0.0 0.0 copy-start.7
  0.0 0.0 copy-start.6
  0.0 0.0 copy-start.5
  0.0 0.0 copy-start.10
  0.1 0.0 copy-start.4
  0.1 0.8 copy-done
  1.0 0.7 pad_maximum_fusion.wo
  1.7 0.3 copy.21
  2.0 0.1 pad.4.wstep
  2.1 0.0 copy-done.9
  2.1 0.0 copy-done.8
  2.1 0.0 copy-done.7
  2.1 0.0 copy-done.6
  2.1 0.0 copy-done.5
  2.1 0.0 copy-done.10
  2.2 0.0 copy-done.4
  2.2 55.7 %gather_and_project.1 = (bf16[1056,640]{1,0:T(8,128)(2,1)S(1)}, f32[1024,128]{1,0:T(8,128)S(1)}, bf16[2048,256]{1,0:T(8,128)(2,1)S(1)}) custom-call(bf16[1,128,2048]{2,1,0:T(8,128)(2,1)S(1)} %copy-done.4, bf16[32,128]{1,0:T(8,128)(2,1)S(1)} %copy-done.5, bf16[32,128]{1,0:T(8,128)(2,1)S(1)} %copy-done.6, bf16[32,128]{1,0:T(8,128)(2,1)S(1)} %copy-done.7, ...), custom_call_target="tpu_custom_call" | custom-call | tf_op jit(solution)/shard_map/gather_and_project/pallas_call | solution.py:256
  57.9 0.0 copy-start.1
  57.9 1.1 copy-done.1
  59.0 0.0 copy-start.2
  59.0 1.0 copy-done.2
  59.9 0.0 copy-start.3
  59.9 0.8 copy-done.3
  60.7 66.9 %mixed_and_summed.1 = bf16[1,128,2048]{2,1,0:T(8,128)(2,1)} custom-call(bf16[1056,640]{1,0:T(8,128)(2,1)} %copy-done.1, f32[1024,128]{1,0:T(8,128)} %copy-done.3, bf16[2048,256]{1,0:T(8,128)(2,1)} %copy-done.2, f32[2,16]{1,0:T(2,128)} %bias.1, f32[2,16]{1,0:T(2,128)} %rate.1, f32[1,2,2,1024]{3,2,1,0:T(2,128)} %shift.1, bf16[5,1024]{1,0:T(8,128)(2,1)} %tap_v.1, ...), custom_call_target="tpu_custom_call" | custom-call | tf_op jit(solution)/shard_map/mixed_and_summed/pallas_call | solution.py:636
  127.6 1.9 %copy.23 = bf16[1,128,2048]{2,1,0:T(8,128)(2,1)} copy(bf16[1,128,2048]{2,1,0:T(8,128)(2,1)} %mixed_and_summed.1) | data formatting | bytes 1048576
  (2 shorter events, 0.0 us)
Async XLA Ops:
  0.0 0.9 copy-start
  0.0 2.1 %copy-start.9 = (bf16[32,128]{1,0:T(8,128)(2,1)S(1)}, bf16[32,128]{1,0:T(8,128)(2,1)}, u32[]{:S(2)}) copy-start(bf16[32,128]{1,0:T(8,128)(2,1)} %wp.1) | copy-start | bytes 24580
  0.0 2.1 %copy-start.8 = (bf16[32,128]{1,0:T(8,128)(2,1)S(1)}, bf16[32,128]{1,0:T(8,128)(2,1)}, u32[]{:S(2)}) copy-start(bf16[32,128]{1,0:T(8,128)(2,1)} %wq.1) | copy-start | bytes 24580
  0.0 2.1 %copy-start.7 = (bf16[32,128]{1,0:T(8,128)(2,1)S(1)}, bf16[32,128]{1,0:T(8,128)(2,1)}, u32[]{:S(2)}) copy-start(bf16[32,128]{1,0:T(8,128)(2,1)} %wk.1) | copy-start | bytes 24580
  0.0 2.1 %copy-start.6 = (bf16[32,128]{1,0:T(8,128)(2,1)S(1)}, bf16[32,128]{1,0:T(8,128)(2,1)}, u32[]{:S(2)}) copy-start(bf16[32,128]{1,0:T(8,128)(2,1)} %wv.1) | copy-start | bytes 24580
  0.0 2.1 %copy-start.5 = (bf16[32,128]{1,0:T(8,128)(2,1)S(1)}, bf16[32,128]{1,0:T(8,128)(2,1)}, u32[]{:S(2)}) copy-start(bf16[32,128]{1,0:T(8,128)(2,1)} %wg.1) | copy-start | bytes 24580
  0.0 2.1 %copy-start.10 = (f32[2048]{0:T(1024)S(1)}, f32[2048]{0:T(1024)}, u32[]{:S(2)}) copy-start(f32[2048]{0:T(1024)} %param.20) | copy-start | bytes 24580
  0.1 2.1 %copy-start.4 = (bf16[1,128,2048]{2,1,0:T(8,128)(2,1)S(1)}, bf16[1,128,2048]{2,1,0:T(8,128)(2,1)}, u32[]{:S(2)}) copy-start(bf16[1,128,2048]{2,1,0:T(8,128)(2,1)} %tok.1) | copy-start | bytes 1572868
  57.9 1.1 copy-start.1
  59.0 1.0 copy-start.2
  59.9 0.8 copy-start.3

commit v3 on v2

v3 whole, which is shorter than its diff:
```python
import functools

import jax
import jax.numpy as jnp
from jax import lax
from jax.experimental import pallas as pl
from jax.experimental.pallas import tpu as pltpu
from jax.sharding import PartitionSpec as P

DUALITY_HEADS = 16
STATE = 128
SPAN = 128
D_SSM = 1024
EPSILON = 1e-06
HIGHEST = lax.Precision.HIGHEST

MESH = pl.DeviceIdType.MESH
HALO = 16
TOK_ROWS = 128
PIECE = 32
NT = (((1,), (1,)), ((), ()))
TN = (((0,), (0,)), ((), ()))
N_BLOCKS = 8
MSG = 64 + 16


def remote(src, dst, send, recv, where):
    return pltpu.make_async_remote_copy(
        src_ref=src, dst_ref=dst, send_sem=send, recv_sem=recv, device_id=where, device_id_type=MESH
    )


def silu(v):
    return v / (1.0 + jnp.exp(-v))


class Rings:
    def __init__(self, buf, a_cols, b_cols, sems, send_sem, place, sizes):
        self.buf, self.a_cols, self.b_cols = buf, a_cols, b_cols
        self.ay, self.azp, self.azm, self.bzp, self.bzm, self.byp, self.bym, self.byo = sems
        self.send_sem, self.sent = send_sem, []
        self.z, self.y = place
        self.n_sp, self.n_fs = sizes
        z, y, n_sp, n_fs = self.z, self.y, *sizes
        self.yp, self.ym, self.yo = (y + 1) % n_fs, (y + n_fs - 1) % n_fs, (y + 2) % n_fs
        self.to_yp, self.to_ym = {"fs": self.yp}, {"fs": self.ym}
        self.to_zp, self.to_zm = {"sp": (z + 1) % n_sp}, {"sp": (z + n_sp - 1) % n_sp}
        self.half = n_sp // 2
        self.pending = [0]

    def at(self, zz, yy, cols):
        row = pl.multiple_of((zz * self.n_fs + yy) * PIECE, PIECE)
        return self.buf.at[pl.ds(row, PIECE), pl.ds(*cols)]

    def a(self, zz, yy):
        return self.at(zz, yy, self.a_cols)

    def b(self, zz, yy):
        return self.at(zz, yy, self.b_cols)

    def send(self, ref, recv, where):
        copy = remote(ref, ref, self.send_sem.at[len(self.sent)], recv, where)
        copy.start()
        self.sent.append(copy)

    def arrived(self, ref, recv):
        remote(ref, ref, self.send_sem.at[0], recv, self.to_yp).wait_recv()

    def begin(self):
        own_a, own_b = self.a(self.z, self.y), self.b(self.z, self.y)
        self.send(own_b, self.bzp.at[1], self.to_zp)
        self.send(own_b, self.bzm.at[1], self.to_zm)
        self.send(own_a, self.ay.at[0], self.to_yp)
        self.send(own_a, self.ay.at[1], self.to_ym)
        self.send(own_a, self.azp.at[4], self.to_zp)
        self.send(own_a, self.azm.at[4], self.to_zm)
        self.send(own_b, self.byp.at[0], self.to_yp)
        self.send(own_b, self.bym.at[0], self.to_ym)

    def spread(self):
        for j, yy in ((1, self.ym), (2, self.yp), (3, self.yo)):
            ref = self.a(self.z, yy)
            self.arrived(ref, self.ay.at[j - 1])
            if j == 1:
                self.send(ref, self.ay.at[2], self.to_yp)
            self.send(ref, self.azp.at[4 + j], self.to_zp)
            self.send(ref, self.azm.at[4 + j], self.to_zm)

    def back(self, o):
        return (self.z + self.n_sp - o) % self.n_sp

    def relay(self, o):
        low, high = self.b(self.back(o), self.ym), self.b(self.back(o), self.yp)
        self.arrived(low, self.byp.at[o])
        if o % 2 == 0:
            self.send(low, self.byo.at[o], self.to_yp)
        self.arrived(high, self.bym.at[o])
        if o % 2 == 1:
            self.send(high, self.byo.at[o], self.to_ym)

    def relay_pending(self):
        for o in self.pending:
            self.relay(o)
        self.pending = []

    def step(self, k, between=None):
        half, fresh = self.half, []
        far = k == half
        for o, recv, onward, where in (
            (k, self.bzp, k < half, self.to_zp),
            (self.n_sp - k, self.bzm, k + 1 < half, self.to_zm),
        ):
            if o in fresh:
                continue
            ref = self.b(self.back(o), self.y)
            self.arrived(ref, recv.at[k])
            if onward:
                self.send(ref, recv.at[k + 1], where)
            self.send(ref, self.byp.at[o], self.to_yp)
            self.send(ref, self.bym.at[o], self.to_ym)
            fresh.append(o)
        y_of = (self.y, self.ym, self.yp, self.yo)
        for j in range(4):
            for recv, zz, mine, where in (
                (self.azp, self.back(k), j < 2, self.to_zp),
                (self.azm, (self.z + k) % self.n_sp, j >= 2, self.to_zm),
            ):
                if far and not mine:
                    continue
                ref = self.a(zz, y_of[j])
                self.arrived(ref, recv.at[4 * k + j])
                if k + 1 < half or (k + 1 == half and mine):
                    self.send(ref, recv.at[4 * (k + 1) + j], where)
            if j == 1:
                self.relay_pending()
                if between is not None:
                    between()
        self.pending = fresh

    def finish(self):
        self.relay_pending()
        for o in range(self.n_sp):
            self.arrived(self.b(self.back(o), self.yo), self.byo.at[o])


def mixer_kernel(
    n_sp, n_fs, n_x,
    tok, wg, wv, wk, wq, wp, wo, wstep, gain,
    bias, rate, shift, tap_v, tap_k, tap_q, mgain, pmix, pgain,
    out,
    tokbuf, normbuf, wbuf, wout, gates, raw,
    p32, xbuf, kbuf, qbuf, ends, ybuf, mix,
    incl, excl, itot, etot, msg_out, msg_in, ss_out, ss_in,
    d_out, d_in, r_out, r_in, n_out, n_in,
    local_sem, tp_sem, tm_sem, tr_sem, td_sem, h_sem, t_send,
    w_ay, w_azp, w_azm, w_bzp, w_bzm, w_byp, w_bym, w_byo, w_send,
    o_ay, o_azp, o_azm, o_bzp, o_bzm, o_byp, o_bym, o_byo, o_send,
    msg_send, msg_recv, ss_send, ss_recv, d_send, d_recv, r_send, r_recv, n_send, n_recv,
):
    f32, bf16 = jnp.float32, jnp.bfloat16
    z, y, t = lax.axis_index("sp"), lax.axis_index("fs"), lax.axis_index("tp")
    x, c = t // 2, t % 2
    n_tp = 2 * n_x
    xp, xm, xo = (x + 1) % n_x, (x + n_x - 1) % n_x, (x + 2) % n_x
    to_xp, to_xm, to_d = {"tp": xp * 2 + c}, {"tp": xm * 2 + c}, {"tp": x * 2 + 1 - c}
    to_zp, to_zm = {"sp": (z + 1) % n_sp}, {"sp": (z + n_sp - 1) % n_sp}
    distances = [1, 2, 4, 8]
    rows = N_BLOCKS * SPAN

    w_rings = Rings(
        wbuf, (0, 256), (256, 384),
        (w_ay, w_azp, w_azm, w_bzp, w_bzm, w_byp, w_bym, w_byo), w_send, (z, y), (n_sp, n_fs),
    )
    o_rings = Rings(
        wout, (0, 128), (128, 128),
        (o_ay, o_azp, o_azm, o_bzp, o_bzm, o_byp, o_bym, o_byo), o_send, (z, y), (n_sp, n_fs),
    )

    def t_at(xx, cc, q=0, count=PIECE):
        row = pl.multiple_of(HALO + (xx * 2 + cc) * TOK_ROWS + q * PIECE, 16)
        return tokbuf.at[pl.ds(row, count), :]

    own_row = pl.ds(pl.multiple_of((z * n_fs + y) * PIECE, PIECE), PIECE)
    locals_ = [
        pltpu.make_async_copy(w, wbuf.at[own_row, pl.ds(i * 128, 128)], local_sem.at[i])
        for i, w in enumerate((wg, wv, wk, wq, wp))
    ]
    locals_.append(pltpu.make_async_copy(tok.at[0], t_at(x, c, 0, TOK_ROWS), local_sem.at[5]))
    locals_.append(pltpu.make_async_copy(wo, wout.at[own_row, :], local_sem.at[6]))
    locals_.append(pltpu.make_async_copy(wstep, wbuf.at[:, pl.ds(640, 128)], local_sem.at[7]))
    for copy in locals_:
        copy.start()

    barrier = pltpu.get_barrier_semaphore()
    partners = [{"tp": (t + r) % n_tp} for r in range(1, n_tp)]
    partners += [{"sp": (z + d) % n_sp} for d in distances]
    partners += [{"sp": (z + n_sp - d) % n_sp} for d in distances if 2 * d != n_sp]
    partners += [w_rings.to_yp, w_rings.to_ym]
    for where in partners:
        pl.semaphore_signal(barrier, inc=1, device_id=where, device_id_type=MESH)
    pl.semaphore_wait(barrier, len(partners))

    t_sent = []

    def t_go(src, dst, recv, where):
        copy = remote(src, dst, t_send.at[len(t_sent)], recv, where)
        copy.start()
        t_sent.append(copy)

    def t_came(ref, recv):
        remote(ref, ref, t_send.at[0], recv, to_d).wait_recv()

    def relay_tokens(xx, q, recv, where, onward, slot):
        ref = t_at(xx, c, q)
        t_came(ref, recv)
        if onward:
            t_go(ref, ref, tr_sem.at[q], where)
        t_go(ref, ref, td_sem.at[slot + q], to_d)

    def norm_rows(begin, count):
        part = tokbuf[pl.ds(begin, count), :].astype(f32)
        scaling = lax.rsqrt(jnp.mean(part * part, axis=-1, keepdims=True) + EPSILON)
        normbuf[pl.ds(begin, count), :] = (part * scaling * gain[...]).astype(bf16)

    def norm_block(xx, cc):
        norm_rows(pl.multiple_of(HALO + (xx * 2 + cc) * TOK_ROWS, 16), TOK_ROWS)

    cs = 1 - c

    def token_step(k):
        if k <= 4:
            q = k - 1
            relay_tokens(xm, q, tp_sem.at[q], to_xp, q < 2, 0)
            q = (2, 3, 0, 1)[k - 1]
            relay_tokens(xp, q, tm_sem.at[q], to_xm, q >= 2, 4)
            if k == 2:
                norm_block(x, c)
            if k == 3:
                t_came(t_at(x, cs, 0, TOK_ROWS), td_sem.at[12])
                norm_block(x, cs)
        elif k <= 6:
            for q in (k - 5, k - 3):
                relay_tokens(xo, q, tr_sem.at[q], to_d, False, 8)
            norm_block(xm if k == 5 else xp, c)
        elif k == 7:
            for q in range(4):
                t_came(t_at(xm, cs, q), td_sem.at[q])
                t_came(t_at(xp, cs, q), td_sem.at[4 + q])
            norm_block(xm, cs)
            norm_block(xp, cs)
        else:
            norm_block(xo, c)

    for copy in locals_[:5]:
        copy.wait()
    w_rings.begin()
    locals_[5].wait()
    for q in (0, 1, 2, 3):
        t_go(t_at(x, c, q), t_at(x, c, q), tp_sem.at[q], to_xp)
    for q in (2, 3, 0, 1):
        t_go(t_at(x, c, q), t_at(x, c, q), tm_sem.at[q], to_xm)
    t_go(t_at(x, c, 0, TOK_ROWS), t_at(x, c, 0, TOK_ROWS), td_sem.at[12], to_d)
    w_rings.spread()
    for k in range(1, n_sp // 2 + 1):
        w_rings.step(k, functools.partial(token_step, k))
    for q in range(4):
        t_came(t_at(xo, cs, q), td_sem.at[8 + q])
    before, after = tokbuf.at[pl.ds(0, HALO), :], tokbuf.at[pl.ds(HALO + rows, HALO), :]
    t_go(tokbuf.at[pl.ds(rows, HALO), :], before, h_sem.at[0], to_zp)
    t_go(tokbuf.at[pl.ds(HALO, HALO), :], after, h_sem.at[1], to_zm)
    w_rings.relay_pending()
    locals_[6].wait()
    o_rings.begin()
    norm_block(xo, cs)
    locals_[7].wait()
    w_rings.finish()

    def rounded(v):
        return v.astype(bf16).astype(f32)

    def project(i):
        at = HALO + i * 256
        dots = jnp.dot(normbuf[at : at + 256, :], wbuf[...], preferred_element_type=f32)
        gates[i * 256 : (i + 1) * 256, :] = dots[:, 0:128].astype(bf16)
        p32[at : at + 256, :] = rounded(dots[:, 128:640])
        raw[i * 256 : (i + 1) * 256, :] = dots[:, 640:768]

    project(0)
    o_rings.spread()
    project(1)
    project(2)
    o_rings.step(1)
    project(3)
    t_came(before, h_sem.at[0])
    t_came(after, h_sem.at[1])
    for begin, real in ((0, z > 0), (HALO + rows, z < n_sp - 1)):
        norm_rows(begin, HALO)
        edge = jnp.dot(
            normbuf[begin : begin + HALO, :], wbuf[:, 128:640], preferred_element_type=f32
        )
        p32[begin : begin + HALO, :] = jnp.where(real, rounded(edge), 0.0)
    o_rings.step(2)

    lane0 = pl.multiple_of(t * 128, 128)
    row8 = lax.broadcasted_iota(jnp.int32, (8, 128), 0)

    def by_kind(parts):
        found = jnp.zeros((8, 128), f32)
        for i, part in enumerate(parts):
            found = jnp.where(row8 == i, part, found)
        return found

    kinds = ((0, 0), (0, 1), (1, 0), (1, 1))
    bias8 = by_kind([bias[r, 2 * t + h] for r, h in kinds])
    rate8 = by_kind([rate[r, 2 * t + h] for r, h in kinds])
    steps_l, logs_l = [], []
    for b in range(N_BLOCKS):
        cols = raw[b * SPAN : (b + 1) * SPAN, :].T[0:8, :] + bias8
        steps = jnp.maximum(cols, 0.0) + jnp.log1p(jnp.exp(-jnp.abs(cols)))
        moved = by_kind([shift[0, h, r : r + 1, b * SPAN : (b + 1) * SPAN] for r, h in kinds])
        steps_l.append(steps)
        logs_l.append(jnp.where(row8 < 4, -rate8 * steps - moved, 0.0))
    steps = jnp.concatenate(steps_l, axis=0)
    logs = jnp.concatenate(logs_l, axis=0)
    lane = lax.broadcasted_iota(jnp.int32, (64, 128), 1)
    kind = lax.broadcasted_iota(jnp.int32, (64, 128), 0) % 8
    prefix, suffix = logs, logs
    for k in (1, 2, 4, 8, 16, 32, 64):
        prefix = prefix + jnp.where(lane >= k, pltpu.roll(prefix, k, 1), 0.0)
        suffix = suffix + jnp.where(lane < 128 - k, pltpu.roll(suffix, 128 - k, 1), 0.0)
    cum = jnp.where(kind < 2, prefix, suffix)
    total = jnp.broadcast_to(jnp.sum(logs, axis=1, keepdims=True), (64, 128))
    tail = jnp.exp(jnp.minimum(total - cum, 0.0)) * steps
    decay = jnp.exp(total)
    cum_tail_t = jnp.concatenate([cum, tail], axis=0).T
    reach_t = jnp.concatenate([jnp.exp(cum), jnp.zeros((64, 128), f32)], axis=0).T

    def wide(cols, b, first):
        j = b * 8 + first
        left = jnp.broadcast_to(cols[:, j : j + 1], (128, 64))
        right = jnp.broadcast_to(cols[:, j + 1 : j + 2], (128, 64))
        return jnp.concatenate([left, right], axis=1)

    def tall(rows_, b, first):
        j = b * 8 + first
        top = jnp.broadcast_to(rows_[j : j + 1, :], (64, 128))
        bottom = jnp.broadcast_to(rows_[j + 1 : j + 2, :], (64, 128))
        return jnp.concatenate([top, bottom], axis=0)

    def window(b, j):
        begin = HALO - 8 + b * SPAN
        return p32[begin : begin + SPAN + 16, j * 128 : (j + 1) * 128]

    def conv(b, j, taps):
        v = window(b, j)
        weights = taps[:, pl.ds(lane0, 128)].astype(f32)
        total_ = v * weights[2:3, :]
        for i in (0, 1, 3, 4):
            total_ = total_ + pltpu.roll(v, (2 - i) % (SPAN + 16), 0) * weights[i : i + 1, :]
        return silu(total_[8 : 8 + SPAN, :])

    for b in range(N_BLOCKS):
        at = slice(b * SPAN, (b + 1) * SPAN)
        values = conv(b, 0, tap_v)
        keys = conv(b, 1, tap_k).astype(bf16)
        xbuf[at, :] = values
        kbuf[at, :] = keys
        both = jnp.concatenate(
            [values * wide(cum_tail_t, b, 64), values * wide(cum_tail_t, b, 66)], axis=1
        )
        ends[b] = lax.dot_general(both.astype(bf16), keys, TN, preferred_element_type=f32)
        if b == 4:
            o_rings.step(3)

    forward = ends[0, 0:128, :]
    backward = ends[N_BLOCKS - 1, 128:256, :]
    for i in range(1, N_BLOCKS):
        b = N_BLOCKS - 1 - i
        forward = forward * tall(decay, i, 0) + ends[i, 0:128, :]
        backward = backward * tall(decay, b, 2) + ends[b, 128:256, :]
    sums = total[0:8, :]
    for b in range(1, N_BLOCKS):
        sums = sums + total[b * 8 : b * 8 + 8, :]
    incl[0] = forward
    incl[1] = backward
    excl[...] = jnp.zeros_like(excl)
    itot[...] = jnp.broadcast_to(sums[None], (4, 8, 128))
    etot[...] = jnp.zeros_like(etot)

    def message(way, h, i, where):
        return remote(
            msg_out.at[way, h, i], msg_in.at[way, h, i],
            msg_send.at[way, h, i], msg_recv.at[way, h, i], where,
        )

    def exchange(i, h):
        d = distances[i]
        for way in (0, 1):
            ok = z + d < n_sp if way == 0 else z >= d
            logs8 = itot[2 * way + h]
            high = logs8.astype(bf16)
            low = (logs8 - high.astype(f32)).astype(bf16)
            msg_out[way, h, i, 0:64, :] = incl[way, h * 64 : (h + 1) * 64, :].astype(bf16)
            msg_out[way, h, i, 64:MSG, :] = jnp.concatenate([high, low], axis=0)
            where = {"sp": (z + d) % n_sp if way == 0 else (z + n_sp - d) % n_sp}

            @pl.when(ok)
            def _():
                message(way, h, i, where).start()

    def combine(i, h):
        d = distances[i]
        for way in (0, 1):
            ok = z >= d if way == 0 else z + d < n_sp
            s, r, part = 2 * way + h, 2 * way + h, slice(h * 64, (h + 1) * 64)

            @pl.when(ok)
            def _():
                message(way, h, i, to_d).wait_recv()
                state = msg_in[way, h, i, 0:64, :].astype(f32)
                pair = msg_in[way, h, i, 64:MSG, :].astype(f32)
                logs8 = pair[0:8, :] + pair[8:16, :]
                incl[way, part, :] = incl[way, part, :] + jnp.exp(itot[s][r : r + 1, :]) * state
                itot[s] = itot[s] + logs8
                excl[way, part, :] = excl[way, part, :] + jnp.exp(etot[s][r : r + 1, :]) * state
                etot[s] = etot[s] + logs8

    row = lax.broadcasted_iota(jnp.int32, (128, 128), 0)
    col = lax.broadcasted_iota(jnp.int32, (128, 128), 1)

    def within(b):
        at = slice(b * SPAN, (b + 1) * SPAN)
        queries = conv(b, 2, tap_q).astype(bf16)
        qbuf[at, :] = queries
        scores = lax.dot_general(queries, kbuf[at, :], NT, preferred_element_type=f32)
        masked = []
        for h in (0, 1):
            jf, jb = b * 8 + h, b * 8 + 2 + h
            ahead = cum_tail_t[:, jf : jf + 1] - cum[jf : jf + 1, :]
            behind = cum_tail_t[:, jb : jb + 1] - cum[jb : jb + 1, :]
            gaps = jnp.where(col < row, ahead, jnp.where(col > row, behind, 0.0))
            df, db = steps[jf : jf + 1, :], steps[jb : jb + 1, :]
            sizes = jnp.where(col < row, df, jnp.where(col > row, db, df + db))
            masked.append((scores * jnp.exp(jnp.minimum(gaps, 0.0)) * sizes).astype(bf16))
        values = xbuf[at, :]
        stacked = jnp.concatenate(
            [jnp.where(col < 64, values, 0.0), jnp.where(col >= 64, values, 0.0)], axis=0
        ).astype(bf16)
        ybuf[at, :] = jnp.dot(
            jnp.concatenate(masked, axis=1), stacked, preferred_element_type=f32
        )

    def pool(b):
        at = slice(b * SPAN, (b + 1) * SPAN)
        n = SPAN + 16
        v = window(b, 3)
        w2 = v + pltpu.roll(v, 1, 0)
        w4 = pltpu.roll(w2, 1, 0) + pltpu.roll(w2, n - 1, 0)
        w8 = pltpu.roll(w4, 2, 0) + pltpu.roll(w4, n - 2, 0)
        w16 = pltpu.roll(w8, 4, 0) + pltpu.roll(w8, n - 4, 0)
        which = t % 4
        summed = jnp.where(
            which == 0, w2, jnp.where(which == 1, w4, jnp.where(which == 2, w8, w16))
        )[8 : 8 + SPAN, :]
        reach = jnp.where(which == 0, 1, jnp.where(which == 1, 2, jnp.where(which == 2, 4, 8)))
        place = z * rows + b * SPAN + row
        upper = jnp.minimum(place + reach, n_sp * rows)
        lower = jnp.maximum(place - reach, 0)
        differences = summed / (upper - lower).astype(f32) - v[8 : 8 + SPAN, :]
        mapped = jnp.dot(differences.astype(bf16), pmix[t], preferred_element_type=f32)
        mix[at, 128:256] = (mapped * pgain[:, pl.ds(lane0, 128)]).astype(bf16)

    def turn(i):
        for h in (0, 1):
            combine(i, h)
            if i + 1 < len(distances):
                exchange(i + 1, h)

    exchange(0, 0)
    exchange(0, 1)
    within(0)
    within(1)
    turn(0)
    o_rings.step(4)
    within(2)
    within(3)
    turn(1)
    o_rings.step(5)
    within(4)
    within(5)
    o_rings.step(6)
    within(6)
    within(7)
    turn(2)
    for b in range(N_BLOCKS):
        pool(b)
        if b == 2:
            o_rings.step(7)
        if b == 5:
            o_rings.step(8)
    o_rings.finish()
    turn(3)

    forward, backward = excl[0], excl[1]
    entering = [None] * N_BLOCKS
    leaving = [None] * N_BLOCKS
    for i in range(N_BLOCKS):
        b = N_BLOCKS - 1 - i
        entering[i] = forward.astype(bf16)
        leaving[b] = backward.astype(bf16)
        forward = forward * tall(decay, i, 0) + ends[i, 0:128, :]
        backward = backward * tall(decay, b, 2) + ends[b, 128:256, :]
    squares = []
    for b in range(N_BLOCKS):
        at = slice(b * SPAN, (b + 1) * SPAN)
        states = jnp.concatenate([entering[b], leaving[b]], axis=0)
        carried = lax.dot_general(qbuf[at, :], states, NT, preferred_element_type=f32)
        heads_out = (
            ybuf[at, :]
            + carried[:, 0:128] * wide(reach_t, b, 0)
            + carried[:, 128:256] * wide(reach_t, b, 2)
        )
        gated = heads_out * silu(gates[at, :].astype(f32))
        ybuf[at, :] = gated
        squares.append(
            lax.dot_general(
                jnp.ones((8, 128), f32), gated * gated, NT,
                precision=HIGHEST, preferred_element_type=f32,
            )[0:1, :]
        )
    own_squares = jnp.concatenate(squares, axis=0)
    ss_out[...] = own_squares
    ss_copies = []
    for r in range(1, n_tp):
        copy = remote(
            ss_out, ss_in.at[r - 1], ss_send.at[r - 1], ss_recv.at[r - 1],
            {"tp": (t + r) % n_tp},
        )
        copy.start()
        ss_copies.append(copy)
    all_squares = own_squares
    for r in range(1, n_tp):
        ss_copies[r - 1].wait_recv()
        all_squares = all_squares + ss_in[r - 1]
    scale = lax.rsqrt(all_squares / D_SSM + EPSILON)
    scale_t = jnp.concatenate([scale, jnp.zeros((120, 128), f32)], axis=0).T
    mix_gain_here = mgain[:, pl.ds(lane0, 128)]
    for b in range(N_BLOCKS):
        at = slice(b * SPAN, (b + 1) * SPAN)
        mix[at, 0:128] = (ybuf[at, :] * scale_t[:, b : b + 1] * mix_gain_here).astype(bf16)

    def partial(xx, cc, begin=0, count=TOK_ROWS):
        at = pl.multiple_of((xx * 2 + cc) * TOK_ROWS + begin, 16)
        return lax.dot_general(
            mix[pl.ds(at, count), :], wout[...], NT, preferred_element_type=f32
        )

    half = TOK_ROWS // 2
    d_copies = []
    for i, xx in enumerate((xo, xp, xm, x)):
        d_out[i] = partial(xx, 1 - c).astype(bf16)
        copy = remote(d_out.at[i], d_in.at[i], d_send.at[i], d_recv.at[i], to_d)
        copy.start()
        d_copies.append(copy)

    def chip(i, xx, begin, count=half):
        return partial(xx, c, begin, count) + d_in[i, begin : begin + count, :].astype(f32)

    def send(i, value, where, out_ref, in_ref, send_sem, recv_sem):
        out_ref[i] = value.astype(bf16)
        copy = remote(out_ref.at[i], in_ref.at[i], send_sem.at[i], recv_sem.at[i], where)
        copy.start()
        return copy

    relay = (r_out, r_in, r_send, r_recv)
    near = (n_out, n_in, n_send, n_recv)
    d_copies[0].wait_recv()
    relay_p = send(0, chip(0, xo, 0), to_xp, *relay)
    relay_m = send(1, chip(0, xo, half), to_xm, *relay)
    d_copies[1].wait_recv()
    dir_p = send(0, chip(1, xp, half), to_xp, *near)
    d_copies[2].wait_recv()
    dir_m = send(1, chip(2, xm, 0), to_xm, *near)
    relay_p.wait_recv()
    comb_p = send(2, chip(1, xp, 0) + r_in[0].astype(f32), to_xp, *near)
    relay_m.wait_recv()
    comb_m = send(3, chip(2, xm, half) + r_in[1].astype(f32), to_xm, *near)
    d_copies[3].wait_recv()
    top, bottom = chip(3, x, 0), chip(3, x, half)
    dir_p.wait_recv()
    dir_m.wait_recv()
    bottom = bottom + n_in[0].astype(f32)
    top = top + n_in[1].astype(f32)
    comb_p.wait_recv()
    out[0, 0:half, :] = (top + n_in[2].astype(f32)).astype(bf16)
    comb_m.wait_recv()
    out[0, half:TOK_ROWS, :] = (bottom + n_in[3].astype(f32)).astype(bf16)

    for i, d in enumerate(distances):
        for way in (0, 1):
            ok = z + d < n_sp if way == 0 else z >= d

            @pl.when(ok)
            def _():
                for h in (0, 1):
                    message(way, h, i, to_d).wait_send()

    last = [relay_p, relay_m, dir_p, dir_m, comb_p, comb_m]
    for copy in t_sent + w_rings.sent + o_rings.sent + ss_copies + d_copies + last:
        copy.wait_send()


N_TOKEN_SENDS = 27
N_RING_SENDS = 127


def mixer(n_sp, n_fs, n_x, *operands):
    any_spec = pl.BlockSpec(memory_space=pl.ANY)
    vmem = pl.BlockSpec(memory_space=pltpu.VMEM)
    smem = pl.BlockSpec(memory_space=pltpu.SMEM)
    dma = pltpu.SemaphoreType.DMA
    f32, bf16 = jnp.float32, jnp.bfloat16
    rows = N_BLOCKS * SPAN
    half = TOK_ROWS // 2

    def ring_sems():
        return [dma((n,)) for n in (3, 36, 36, 9, 9, 16, 16, 16, N_RING_SENDS)]

    return pl.pallas_call(
        functools.partial(mixer_kernel, n_sp, n_fs, n_x),
        out_shape=jax.ShapeDtypeStruct((1, TOK_ROWS, 2048), bf16),
        in_specs=[any_spec] * 8 + [vmem] + [smem] * 2 + [vmem] * 7,
        out_specs=vmem,
        scratch_shapes=[
            pltpu.VMEM((rows + 2 * HALO, 2048), bf16),
            pltpu.VMEM((rows + 2 * HALO, 2048), bf16),
            pltpu.VMEM((2048, 768), bf16),
            pltpu.VMEM((2048, 256), bf16),
            pltpu.VMEM((rows, 128), bf16),
            pltpu.VMEM((rows, 128), f32),
            pltpu.VMEM((rows + 2 * HALO, 512), f32),
            pltpu.VMEM((rows, 128), f32),
            pltpu.VMEM((rows, 128), bf16),
            pltpu.VMEM((rows, 128), bf16),
            pltpu.VMEM((N_BLOCKS, 256, 128), f32),
            pltpu.VMEM((rows, 128), f32),
            pltpu.VMEM((rows, 256), bf16),
            pltpu.VMEM((2, 128, 128), f32),
            pltpu.VMEM((2, 128, 128), f32),
            pltpu.VMEM((4, 8, 128), f32),
            pltpu.VMEM((4, 8, 128), f32),
            pltpu.VMEM((2, 2, 4, MSG, 128), bf16),
            pltpu.VMEM((2, 2, 4, MSG, 128), bf16),
            pltpu.VMEM((8, 128), f32),
            pltpu.VMEM((7, 8, 128), f32),
            pltpu.VMEM((4, TOK_ROWS, 2048), bf16),
            pltpu.VMEM((4, TOK_ROWS, 2048), bf16),
            pltpu.VMEM((2, half, 2048), bf16),
            pltpu.VMEM((2, half, 2048), bf16),
            pltpu.VMEM((4, half, 2048), bf16),
            pltpu.VMEM((4, half, 2048), bf16),
            dma((8,)), dma((4,)), dma((4,)), dma((4,)), dma((13,)), dma((2,)),
            dma((N_TOKEN_SENDS,)),
            *ring_sems(),
            *ring_sems(),
            dma((2, 2, 4)), dma((2, 2, 4)), dma((7,)), dma((7,)),
            dma((4,)), dma((4,)), dma((2,)), dma((2,)), dma((4,)), dma((4,)),
        ],
        compiler_params=pltpu.CompilerParams(
            collective_id=0, has_side_effects=True, vmem_limit_bytes=56 * 1024 * 1024
        ),
        name="mixer",
    )(*operands)


def local(
    tokens, norm_gain, w_gate, w_value, w_bkey, w_query, w_pool_in, w_step, step_bias,
    decay_rate, decay_shift, conv_value, conv_bkey, conv_query, mix_gain, pool_mix, pool_gain,
    w_out_ssd, w_out_pool,
):
    n_tp, n_sp, n_fs = lax.axis_size("tp"), lax.axis_size("sp"), lax.axis_size("fs")
    heads_dev = DUALITY_HEADS // n_tp
    step_cols = lax.dynamic_slice_in_dim(w_step, lax.axis_index("tp") * heads_dev, heads_dev, 2)
    step_cols = jnp.pad(step_cols.reshape(w_step.shape[0], 2 * heads_dev), ((0, 0), (0, 124)))
    out_turned = jnp.concatenate([w_out_ssd.T, w_out_pool.T], axis=1)
    return mixer(
        n_sp, n_fs, n_tp // 2, tokens, w_gate, w_value, w_bkey, w_query, w_pool_in,
        out_turned, step_cols, norm_gain[None], step_bias, decay_rate, decay_shift,
        conv_value, conv_bkey, conv_query, mix_gain[None], pool_mix, pool_gain[None],
    )


def solution(mesh):
    return jax.shard_map(
        local,
        mesh=mesh,
        in_specs=(
            P("fs", ("sp", "tp"), None),
            P(),
            P(("sp", "fs"), "tp"),
            P(("sp", "fs"), "tp"),
            P(("sp", "fs"), "tp"),
            P(("sp", "fs"), "tp"),
            P(("sp", "fs"), "tp"),
            P(),
            P(),
            P(),
            P("fs", "tp", None, "sp"),
            P(),
            P(),
            P(),
            P(),
            P(),
            P(),
            P("tp", ("sp", "fs")),
            P("tp", ("sp", "fs")),
        ),
        out_specs=P("fs", ("sp", "tp"), None),
        check_vma=False,
    )
```

time: 130 us -> 129 us (level)
  local copies, waits for them, and re-layouts: 6.05 us -> 4.72 us
    unnamed x23 -> x7, local copies, waits for them, and re-layouts: 5.59 us -> 3.47 us
    pallas_call x2 -> x1, Pallas kernels: 123 us -> 124 us  [mixer(): pl.pallas_call(functools.partial(mixer_kernel, n_sp, n_fs, n_x), out_shap...]
where the time goes in v3:
time: 129 us
  Pallas kernels  124 us (96%)
  local copies, waits for them, and re-layouts  4.72 us (4%)
    pallas_call x1, Pallas kernels, mixer(): pl.pallas_call(functools.partial(mixer_kernel, n_sp, n_fs, n_x), out_shap...  124 us
    unnamed x7, local copies, waits for them, and re-layouts  3.47 us

profile of v3, /device:TPU:1, one launch (start us, length us, event | category | flops | bytes accessed | tf_op | source)
XLA Modules:
  0.0 129.0 jit_solution(15762450291212347441)
XLA Ops:
  0.0 0.0 copy-start
  0.0 0.9 copy-done
  0.9 0.0 copy-start.1
  0.9 0.0 copy-start.2
  1.0 0.7 copy-done.1
  1.6 0.0 copy-done.2
  1.6 0.6 pad_maximum_fusion.wo
  2.3 0.3 copy.21
  2.6 0.9 pad.4.wstep
  3.5 123.6 %mixer.1 = bf16[1,128,2048]{2,1,0:T(8,128)(2,1)} custom-call(bf16[1,128,2048]{2,1,0:T(8,128)(2,1)} %tok.1, bf16[32,128]{1,0:T(8,128)(2,1)} %wg.1, bf16[32,128]{1,0:T(8,128)(2,1)} %wv.1, bf16[32,128]{1,0:T(8,128)(2,1)} %wk.1, bf16[32,128]{1,0:T(8,128)(2,1)} %wq.1, bf16[32,128]{1,0:T(8,128)(2,1)} %wp.1, bf16[32,256]{1,0:T(8,128)(2,1)} %pad_maximum_fusion.wo, ...), custom_call_target="tpu_custom_call" | custom-call | tf_op jit(solution)/shard_map/mixer/pallas_call | solution.py:629
  127.1 1.9 %copy.23 = bf16[1,128,2048]{2,1,0:T(8,128)(2,1)} copy(bf16[1,128,2048]{2,1,0:T(8,128)(2,1)} %mixer.1) | data formatting | bytes 1048576
  (2 shorter events, 0.0 us)
Async XLA Ops:
  0.0 0.9 copy-start
  0.9 0.7 copy-start.1
  0.9 0.7 copy-start.2

commit v4 on v3

--- a/solution.py
+++ b/solution.py
@@ -35,6 +35,7 @@
 
 
 class Rings:
+
     def __init__(self, buf, a_cols, b_cols, sems, send_sem, place, sizes):
         self.buf, self.a_cols, self.b_cols = buf, a_cols, b_cols
         self.ay, self.azp, self.azm, self.bzp, self.bzm, self.byp, self.bym, self.byo = sems
@@ -45,6 +46,7 @@
         self.yp, self.ym, self.yo = (y + 1) % n_fs, (y + n_fs - 1) % n_fs, (y + 2) % n_fs
         self.to_yp, self.to_ym = {"fs": self.yp}, {"fs": self.ym}
         self.to_zp, self.to_zm = {"sp": (z + 1) % n_sp}, {"sp": (z + n_sp - 1) % n_sp}
+        self.to_zpp, self.to_zmm = {"sp": (z + 2) % n_sp}, {"sp": (z + n_sp - 2) % n_sp}
         self.half = n_sp // 2
         self.pending = [0]
 
@@ -67,15 +69,24 @@
         remote(ref, ref, self.send_sem.at[0], recv, self.to_yp).wait_recv()
 
     def begin(self):
-        own_a, own_b = self.a(self.z, self.y), self.b(self.z, self.y)
+        own_b = self.b(self.z, self.y)
+        self.send(own_b, self.bzp.at[2], self.to_zpp)
+        self.send(own_b, self.bzm.at[2], self.to_zmm)
         self.send(own_b, self.bzp.at[1], self.to_zp)
         self.send(own_b, self.bzm.at[1], self.to_zm)
-        self.send(own_a, self.ay.at[0], self.to_yp)
-        self.send(own_a, self.ay.at[1], self.to_ym)
-        self.send(own_a, self.azp.at[4], self.to_zp)
-        self.send(own_a, self.azm.at[4], self.to_zm)
+        if self.a_cols is not None:
+            own_a = self.a(self.z, self.y)
+            self.send(own_a, self.ay.at[0], self.to_yp)
+            self.send(own_a, self.ay.at[1], self.to_ym)
+            self.outward(own_a, 0)
         self.send(own_b, self.byp.at[0], self.to_yp)
         self.send(own_b, self.bym.at[0], self.to_ym)
+
+    def outward(self, ref, j):
+        self.send(ref, self.azp.at[8 + j], self.to_zpp)
+        self.send(ref, self.azm.at[8 + j], self.to_zmm)
+        self.send(ref, self.azp.at[4 + j], self.to_zp)
+        self.send(ref, self.azm.at[4 + j], self.to_zm)
 
     def spread(self):
         for j, yy in ((1, self.ym), (2, self.yp), (3, self.yo)):
@@ -83,8 +94,7 @@
             self.arrived(ref, self.ay.at[j - 1])
             if j == 1:
                 self.send(ref, self.ay.at[2], self.to_yp)
-            self.send(ref, self.azp.at[4 + j], self.to_zp)
-            self.send(ref, self.azm.at[4 + j], self.to_zm)
+            self.outward(ref, j)
 
     def back(self, o):
         return (self.z + self.n_sp - o) % self.n_sp
@@ -106,31 +116,31 @@
     def step(self, k, between=None):
         half, fresh = self.half, []
         far = k == half
-        for o, recv, onward, where in (
-            (k, self.bzp, k < half, self.to_zp),
-            (self.n_sp - k, self.bzm, k + 1 < half, self.to_zm),
+        for o, recv, mine, where in (
+            (k, self.bzp, True, self.to_zpp),
+            (self.n_sp - k, self.bzm, False, self.to_zmm),
         ):
             if o in fresh:
                 continue
             ref = self.b(self.back(o), self.y)
             self.arrived(ref, recv.at[k])
-            if onward:
-                self.send(ref, recv.at[k + 1], where)
+            if k + 2 < half or (k + 2 == half and mine):
+                self.send(ref, recv.at[k + 2], where)
             self.send(ref, self.byp.at[o], self.to_yp)
             self.send(ref, self.bym.at[o], self.to_ym)
             fresh.append(o)
         y_of = (self.y, self.ym, self.yp, self.yo)
         for j in range(4):
             for recv, zz, mine, where in (
-                (self.azp, self.back(k), j < 2, self.to_zp),
-                (self.azm, (self.z + k) % self.n_sp, j >= 2, self.to_zm),
+                (self.azp, self.back(k), j < 2, self.to_zpp),
+                (self.azm, (self.z + k) % self.n_sp, j >= 2, self.to_zmm),
             ):
-                if far and not mine:
+                if self.a_cols is None or (far and not mine):
                     continue
                 ref = self.a(zz, y_of[j])
                 self.arrived(ref, recv.at[4 * k + j])
-                if k + 1 < half or (k + 1 == half and mine):
-                    self.send(ref, recv.at[4 * (k + 1) + j], where)
+                if k + 2 < half or (k + 2 == half and mine):
+                    self.send(ref, recv.at[4 * (k + 2) + j], where)
             if j == 1:
                 self.relay_pending()
                 if between is not None:
@@ -145,16 +155,17 @@
 
 def mixer_kernel(
     n_sp, n_fs, n_x,
-    tok, wg, wv, wk, wq, wp, wo, wstep, gain,
-    bias, rate, shift, tap_v, tap_k, tap_q, mgain, pmix, pgain,
+    tok, wg, wv, wk, wq, wp, wo_s, wo_p, wstep_in, gain_in,
+    bias_in, rate_in, shift_in, tap_v_in, tap_k_in, tap_q_in, mgain_in, pmix_in, pgain_in,
     out,
+    wo_2, wstep, gain, bias, rate, shift, tap_v, tap_k, tap_q, mgain, pmix, pgain, small_sem,
     tokbuf, normbuf, wbuf, wout, gates, raw,
     p32, xbuf, kbuf, qbuf, ends, ybuf, mix,
     incl, excl, itot, etot, msg_out, msg_in, ss_out, ss_in,
     d_out, d_in, r_out, r_in, n_out, n_in,
     local_sem, tp_sem, tm_sem, tr_sem, td_sem, h_sem, t_send,
     w_ay, w_azp, w_azm, w_bzp, w_bzm, w_byp, w_bym, w_byo, w_send,
-    o_ay, o_azp, o_azm, o_bzp, o_bzm, o_byp, o_bym, o_byo, o_send,
+    o_bzp, o_bzm, o_byp, o_bym, o_byo, o_send,
     msg_send, msg_recv, ss_send, ss_recv, d_send, d_recv, r_send, r_recv, n_send, n_recv,
 ):
     f32, bf16 = jnp.float32, jnp.bfloat16
@@ -168,12 +179,12 @@
     rows = N_BLOCKS * SPAN
 
     w_rings = Rings(
-        wbuf, (0, 256), (256, 384),
+        wbuf, (0, 128), (128, 512),
         (w_ay, w_azp, w_azm, w_bzp, w_bzm, w_byp, w_bym, w_byo), w_send, (z, y), (n_sp, n_fs),
     )
     o_rings = Rings(
-        wout, (0, 128), (128, 128),
-        (o_ay, o_azp, o_azm, o_bzp, o_bzm, o_byp, o_bym, o_byo), o_send, (z, y), (n_sp, n_fs),
+        wout, None, (0, 256),
+        (None, None, None, o_bzp, o_bzm, o_byp, o_bym, o_byo), o_send, (z, y), (n_sp, n_fs),
     )
 
     def t_at(xx, cc, q=0, count=PIECE):
@@ -186,16 +197,28 @@
         for i, w in enumerate((wg, wv, wk, wq, wp))
     ]
     locals_.append(pltpu.make_async_copy(tok.at[0], t_at(x, c, 0, TOK_ROWS), local_sem.at[5]))
-    locals_.append(pltpu.make_async_copy(wo, wout.at[own_row, :], local_sem.at[6]))
-    locals_.append(pltpu.make_async_copy(wstep, wbuf.at[:, pl.ds(640, 128)], local_sem.at[7]))
-    for copy in locals_:
+    lane0 = pl.multiple_of(t * 128, 128)
+    here = pl.ds(lane0, 128)
+    small = [
+        pltpu.make_async_copy(src, dst, small_sem.at[i])
+        for i, (src, dst) in enumerate(
+            (
+                (gain_in, gain), (wo_s, wo_2.at[0]), (wo_p, wo_2.at[1]), (wstep_in, wstep),
+                (bias_in, bias), (rate_in, rate), (shift_in, shift),
+                (tap_v_in.at[:, here], tap_v), (tap_k_in.at[:, here], tap_k),
+                (tap_q_in.at[:, here], tap_q), (mgain_in.at[:, here], mgain),
+                (pmix_in.at[t], pmix), (pgain_in.at[:, here], pgain),
+            )
+        )
+    ]
+    for copy in locals_ + small:
         copy.start()
 
     barrier = pltpu.get_barrier_semaphore()
-    partners = [{"tp": (t + r) % n_tp} for r in range(1, n_tp)]
-    partners += [{"sp": (z + d) % n_sp} for d in distances]
-    partners += [{"sp": (z + n_sp - d) % n_sp} for d in distances if 2 * d != n_sp]
-    partners += [w_rings.to_yp, w_rings.to_ym]
+    partners = [
+        to_xp, to_xm, to_d, to_zp, to_zm, w_rings.to_zpp, w_rings.to_zmm,
+        w_rings.to_yp, w_rings.to_ym,
+    ]
     for where in partners:
         pl.semaphore_signal(barrier, inc=1, device_id=where, device_id_type=MESH)
     pl.semaphore_wait(barrier, len(partners))
@@ -261,6 +284,12 @@
         t_go(t_at(x, c, q), t_at(x, c, q), tm_sem.at[q], to_xm)
     t_go(t_at(x, c, 0, TOK_ROWS), t_at(x, c, 0, TOK_ROWS), td_sem.at[12], to_d)
     w_rings.spread()
+    for copy in small:
+        copy.wait()
+    for i in (0, 1):
+        turned = jnp.concatenate([wo_2[i].astype(f32), jnp.zeros((128, 96), f32)], axis=1).T
+        wout[own_row, i * 128 : (i + 1) * 128] = turned[0:PIECE, :].astype(bf16)
+    wbuf[:, 640:768] = jnp.concatenate([wstep[...], jnp.zeros((2048, 124), bf16)], axis=1)
     for k in range(1, n_sp // 2 + 1):
         w_rings.step(k, functools.partial(token_step, k))
     for q in range(4):
@@ -269,10 +298,8 @@
     t_go(tokbuf.at[pl.ds(rows, HALO), :], before, h_sem.at[0], to_zp)
     t_go(tokbuf.at[pl.ds(HALO, HALO), :], after, h_sem.at[1], to_zm)
     w_rings.relay_pending()
-    locals_[6].wait()
     o_rings.begin()
     norm_block(xo, cs)
-    locals_[7].wait()
     w_rings.finish()
 
     def rounded(v):
@@ -286,10 +313,8 @@
         raw[i * 256 : (i + 1) * 256, :] = dots[:, 640:768]
 
     project(0)
-    o_rings.spread()
     project(1)
     project(2)
-    o_rings.step(1)
     project(3)
     t_came(before, h_sem.at[0])
     t_came(after, h_sem.at[1])
@@ -299,9 +324,7 @@
             normbuf[begin : begin + HALO, :], wbuf[:, 128:640], preferred_element_type=f32
         )
         p32[begin : begin + HALO, :] = jnp.where(real, rounded(edge), 0.0)
-    o_rings.step(2)
-
-    lane0 = pl.multiple_of(t * 128, 128)
+
     row8 = lax.broadcasted_iota(jnp.int32, (8, 128), 0)
 
     def by_kind(parts):
@@ -353,7 +376,7 @@
 
     def conv(b, j, taps):
         v = window(b, j)
-        weights = taps[:, pl.ds(lane0, 128)].astype(f32)
+        weights = taps[...].astype(f32)
         total_ = v * weights[2:3, :]
         for i in (0, 1, 3, 4):
             total_ = total_ + pltpu.roll(v, (2 - i) % (SPAN + 16), 0) * weights[i : i + 1, :]
@@ -369,8 +392,6 @@
             [values * wide(cum_tail_t, b, 64), values * wide(cum_tail_t, b, 66)], axis=1
         )
         ends[b] = lax.dot_general(both.astype(bf16), keys, TN, preferred_element_type=f32)
-        if b == 4:
-            o_rings.step(3)
 
     forward = ends[0, 0:128, :]
     backward = ends[N_BLOCKS - 1, 128:256, :]
@@ -467,8 +488,8 @@
         upper = jnp.minimum(place + reach, n_sp * rows)
         lower = jnp.maximum(place - reach, 0)
         differences = summed / (upper - lower).astype(f32) - v[8 : 8 + SPAN, :]
-        mapped = jnp.dot(differences.astype(bf16), pmix[t], preferred_element_type=f32)
-        mix[at, 128:256] = (mapped * pgain[:, pl.ds(lane0, 128)]).astype(bf16)
+        mapped = jnp.dot(differences.astype(bf16), pmix[...], preferred_element_type=f32)
+        mix[at, 128:256] = (mapped * pgain[...]).astype(bf16)
 
     def turn(i):
         for h in (0, 1):
@@ -478,26 +499,27 @@
 
     exchange(0, 0)
     exchange(0, 1)
+    o_rings.step(1)
+    o_rings.step(2)
     within(0)
     within(1)
     turn(0)
+    o_rings.step(3)
     o_rings.step(4)
     within(2)
     within(3)
     turn(1)
     o_rings.step(5)
+    o_rings.step(6)
     within(4)
     within(5)
-    o_rings.step(6)
     within(6)
     within(7)
     turn(2)
+    o_rings.step(7)
+    o_rings.step(8)
     for b in range(N_BLOCKS):
         pool(b)
-        if b == 2:
-            o_rings.step(7)
-        if b == 5:
-            o_rings.step(8)
     o_rings.finish()
     turn(3)
 
@@ -544,7 +566,7 @@
         all_squares = all_squares + ss_in[r - 1]
     scale = lax.rsqrt(all_squares / D_SSM + EPSILON)
     scale_t = jnp.concatenate([scale, jnp.zeros((120, 128), f32)], axis=0).T
-    mix_gain_here = mgain[:, pl.ds(lane0, 128)]
+    mix_gain_here = mgain[...]
     for b in range(N_BLOCKS):
         at = slice(b * SPAN, (b + 1) * SPAN)
         mix[at, 0:128] = (ybuf[at, :] * scale_t[:, b : b + 1] * mix_gain_here).astype(bf16)
@@ -617,21 +639,33 @@
 def mixer(n_sp, n_fs, n_x, *operands):
     any_spec = pl.BlockSpec(memory_space=pl.ANY)
     vmem = pl.BlockSpec(memory_space=pltpu.VMEM)
-    smem = pl.BlockSpec(memory_space=pltpu.SMEM)
     dma = pltpu.SemaphoreType.DMA
     f32, bf16 = jnp.float32, jnp.bfloat16
     rows = N_BLOCKS * SPAN
     half = TOK_ROWS // 2
 
-    def ring_sems():
-        return [dma((n,)) for n in (3, 36, 36, 9, 9, 16, 16, 16, N_RING_SENDS)]
+    def ring_sems(counts):
+        return [dma((n,)) for n in counts]
 
     return pl.pallas_call(
         functools.partial(mixer_kernel, n_sp, n_fs, n_x),
         out_shape=jax.ShapeDtypeStruct((1, TOK_ROWS, 2048), bf16),
-        in_specs=[any_spec] * 8 + [vmem] + [smem] * 2 + [vmem] * 7,
+        in_specs=[any_spec] * 19,
         out_specs=vmem,
         scratch_shapes=[
+            pltpu.VMEM((2, 128, 32), bf16),
+            pltpu.VMEM((2048, 4), bf16),
+            pltpu.VMEM((1, 2048), f32),
+            pltpu.SMEM((2, 16), f32),
+            pltpu.SMEM((2, 16), f32),
+            pltpu.VMEM((1, 2, 2, 1024), f32),
+            pltpu.VMEM((5, 128), bf16),
+            pltpu.VMEM((5, 128), bf16),
+            pltpu.VMEM((5, 128), bf16),
+            pltpu.VMEM((1, 128), f32),
+            pltpu.VMEM((128, 128), bf16),
+            pltpu.VMEM((1, 128), f32),
+            dma((13,)),
             pltpu.VMEM((rows + 2 * HALO, 2048), bf16),
             pltpu.VMEM((rows + 2 * HALO, 2048), bf16),
             pltpu.VMEM((2048, 768), bf16),
@@ -659,10 +693,10 @@
             pltpu.VMEM((2, half, 2048), bf16),
             pltpu.VMEM((4, half, 2048), bf16),
             pltpu.VMEM((4, half, 2048), bf16),
-            dma((8,)), dma((4,)), dma((4,)), dma((4,)), dma((13,)), dma((2,)),
+            dma((6,)), dma((4,)), dma((4,)), dma((4,)), dma((13,)), dma((2,)),
             dma((N_TOKEN_SENDS,)),
-            *ring_sems(),
-            *ring_sems(),
+            *ring_sems((3, 36, 36, 9, 9, 16, 16, 16, N_RING_SENDS)),
+            *ring_sems((9, 9, 16, 16, 16, N_RING_SENDS)),
             dma((2, 2, 4)), dma((2, 2, 4)), dma((7,)), dma((7,)),
             dma((4,)), dma((4,)), dma((2,)), dma((2,)), dma((4,)), dma((4,)),
         ],
@@ -681,11 +715,10 @@
     n_tp, n_sp, n_fs = lax.axis_size("tp"), lax.axis_size("sp"), lax.axis_size("fs")
     heads_dev = DUALITY_HEADS // n_tp
     step_cols = lax.dynamic_slice_in_dim(w_step, lax.axis_index("tp") * heads_dev, heads_dev, 2)
-    step_cols = jnp.pad(step_cols.reshape(w_step.shape[0], 2 * heads_dev), ((0, 0), (0, 124)))
-    out_turned = jnp.concatenate([w_out_ssd.T, w_out_pool.T], axis=1)
+    step_cols = step_cols.reshape(w_step.shape[0], 2 * heads_dev)
     return mixer(
         n_sp, n_fs, n_tp // 2, tokens, w_gate, w_value, w_bkey, w_query, w_pool_in,
-        out_turned, step_cols, norm_gain[None], step_bias, decay_rate, decay_shift,
+        w_out_ssd, w_out_pool, step_cols, norm_gain[None], step_bias, decay_rate, decay_shift,
         conv_value, conv_bkey, conv_query, mix_gain[None], pool_mix, pool_gain[None],
     )
 

time: 129 us -> 115 us (0.89)
  Pallas kernels: 124 us -> 109 us
    pallas_call x1, Pallas kernels: 124 us -> 109 us  [mixer(): pl.pallas_call(functools.partial(mixer_kernel, n_sp, n_fs, n_x), out_shap...]
    unnamed x7 -> x9, local copies, waits for them, and re-layouts: 3.47 us -> 4.91 us
where the time goes in v4:
time: 115 us
  Pallas kernels  109 us (95%)
  local copies, waits for them, and re-layouts  6 us (5%)
    pallas_call x1, Pallas kernels, mixer(): pl.pallas_call(functools.partial(mixer_kernel, n_sp, n_fs, n_x), out_shap...  109 us
    unnamed x9, local copies, waits for them, and re-layouts  4.91 us

profile of v4, /device:TPU:1, one launch (start us, length us, event | category | flops | bytes accessed | tf_op | source)
XLA Modules:
  0.0 114.7 jit_solution(9551256530649531640)
XLA Ops:
  0.0 0.0 copy-start
  0.0 0.9 copy-done
  0.9 0.0 copy-start.1
  1.0 0.7 copy-done.1
  1.6 0.0 copy-start.2
  1.6 0.7 copy.23.wo_s
  2.4 0.0 copy-done.2
  2.4 0.7 copy.24.wo_p
  3.1 1.1 copy.25.wstep_in
  4.1 108.7 %mixer.1 = bf16[1,128,2048]{2,1,0:T(8,128)(2,1)} custom-call(bf16[1,128,2048]{2,1,0:T(8,128)(2,1)} %tok.1, bf16[32,128]{1,0:T(8,128)(2,1)} %wg.1, bf16[32,128]{1,0:T(8,128)(2,1)} %wv.1, bf16[32,128]{1,0:T(8,128)(2,1)} %wk.1, bf16[32,128]{1,0:T(8,128)(2,1)} %wq.1, bf16[32,128]{1,0:T(8,128)(2,1)} %wp.1, bf16[128,32]{1,0:T(8,128)(2,1)} %copy.23.wo_s, ...), custom_call_target="tpu_custom_call" | custom-call | tf_op jit(solution)/shard_map/mixer/pallas_call | solution.py:650
  112.9 1.9 %copy.27 = bf16[1,128,2048]{2,1,0:T(8,128)(2,1)} copy(bf16[1,128,2048]{2,1,0:T(8,128)(2,1)} %mixer.1) | data formatting | bytes 1048576
  (2 shorter events, 0.0 us)
Async XLA Ops:
  0.0 0.9 copy-start
  0.9 0.7 copy-start.1
  1.6 0.7 copy-start.2

commit v5 on v4

--- a/solution.py
+++ b/solution.py
@@ -36,29 +36,21 @@
 
 class Rings:
 
-    def __init__(self, buf, a_cols, b_cols, sems, send_sem, place, sizes):
-        self.buf, self.a_cols, self.b_cols = buf, a_cols, b_cols
-        self.ay, self.azp, self.azm, self.bzp, self.bzm, self.byp, self.bym, self.byo = sems
+    def __init__(self, buf, cols, stride, sems, send_sem, place, sizes):
+        self.buf, self.cols, self.stride = buf, cols, stride
+        self.zp_sem, self.zm_sem, self.yp_sem, self.ym_sem, self.yo_sem = sems
         self.send_sem, self.sent = send_sem, []
         self.z, self.y = place
         self.n_sp, self.n_fs = sizes
         z, y, n_sp, n_fs = self.z, self.y, *sizes
         self.yp, self.ym, self.yo = (y + 1) % n_fs, (y + n_fs - 1) % n_fs, (y + 2) % n_fs
         self.to_yp, self.to_ym = {"fs": self.yp}, {"fs": self.ym}
-        self.to_zp, self.to_zm = {"sp": (z + 1) % n_sp}, {"sp": (z + n_sp - 1) % n_sp}
-        self.to_zpp, self.to_zmm = {"sp": (z + 2) % n_sp}, {"sp": (z + n_sp - 2) % n_sp}
         self.half = n_sp // 2
-        self.pending = [0]
-
-    def at(self, zz, yy, cols):
+
+    def at(self, o, yy):
+        zz = (self.z + self.n_sp - o) % self.n_sp
         row = pl.multiple_of((zz * self.n_fs + yy) * PIECE, PIECE)
-        return self.buf.at[pl.ds(row, PIECE), pl.ds(*cols)]
-
-    def a(self, zz, yy):
-        return self.at(zz, yy, self.a_cols)
-
-    def b(self, zz, yy):
-        return self.at(zz, yy, self.b_cols)
+        return self.buf.at[pl.ds(row, PIECE), pl.ds(*self.cols)]
 
     def send(self, ref, recv, where):
         copy = remote(ref, ref, self.send_sem.at[len(self.sent)], recv, where)
@@ -68,89 +60,53 @@
     def arrived(self, ref, recv):
         remote(ref, ref, self.send_sem.at[0], recv, self.to_yp).wait_recv()
 
+    def up(self, ref, k, stride):
+        if k <= self.half:
+            self.send(ref, self.zp_sem.at[k], {"sp": (self.z + stride) % self.n_sp})
+
+    def down(self, ref, k, stride):
+        if k < self.half:
+            self.send(ref, self.zm_sem.at[k], {"sp": (self.z + self.n_sp - stride) % self.n_sp})
+
     def begin(self):
-        own_b = self.b(self.z, self.y)
-        self.send(own_b, self.bzp.at[2], self.to_zpp)
-        self.send(own_b, self.bzm.at[2], self.to_zmm)
-        self.send(own_b, self.bzp.at[1], self.to_zp)
-        self.send(own_b, self.bzm.at[1], self.to_zm)
-        if self.a_cols is not None:
-            own_a = self.a(self.z, self.y)
-            self.send(own_a, self.ay.at[0], self.to_yp)
-            self.send(own_a, self.ay.at[1], self.to_ym)
-            self.outward(own_a, 0)
-        self.send(own_b, self.byp.at[0], self.to_yp)
-        self.send(own_b, self.bym.at[0], self.to_ym)
-
-    def outward(self, ref, j):
-        self.send(ref, self.azp.at[8 + j], self.to_zpp)
-        self.send(ref, self.azm.at[8 + j], self.to_zmm)
-        self.send(ref, self.azp.at[4 + j], self.to_zp)
-        self.send(ref, self.azm.at[4 + j], self.to_zm)
-
-    def spread(self):
-        for j, yy in ((1, self.ym), (2, self.yp), (3, self.yo)):
-            ref = self.a(self.z, yy)
-            self.arrived(ref, self.ay.at[j - 1])
-            if j == 1:
-                self.send(ref, self.ay.at[2], self.to_yp)
-            self.outward(ref, j)
-
-    def back(self, o):
-        return (self.z + self.n_sp - o) % self.n_sp
-
-    def relay(self, o):
-        low, high = self.b(self.back(o), self.ym), self.b(self.back(o), self.yp)
-        self.arrived(low, self.byp.at[o])
-        if o % 2 == 0:
-            self.send(low, self.byo.at[o], self.to_yp)
-        self.arrived(high, self.bym.at[o])
-        if o % 2 == 1:
-            self.send(high, self.byo.at[o], self.to_ym)
-
-    def relay_pending(self):
-        for o in self.pending:
-            self.relay(o)
-        self.pending = []
-
-    def step(self, k, between=None):
-        half, fresh = self.half, []
-        far = k == half
-        for o, recv, mine, where in (
-            (k, self.bzp, True, self.to_zpp),
-            (self.n_sp - k, self.bzm, False, self.to_zmm),
-        ):
-            if o in fresh:
-                continue
-            ref = self.b(self.back(o), self.y)
-            self.arrived(ref, recv.at[k])
-            if k + 2 < half or (k + 2 == half and mine):
-                self.send(ref, recv.at[k + 2], where)
-            self.send(ref, self.byp.at[o], self.to_yp)
-            self.send(ref, self.bym.at[o], self.to_ym)
-            fresh.append(o)
-        y_of = (self.y, self.ym, self.yp, self.yo)
-        for j in range(4):
-            for recv, zz, mine, where in (
-                (self.azp, self.back(k), j < 2, self.to_zpp),
-                (self.azm, (self.z + k) % self.n_sp, j >= 2, self.to_zmm),
-            ):
-                if self.a_cols is None or (far and not mine):
-                    continue
-                ref = self.a(zz, y_of[j])
-                self.arrived(ref, recv.at[4 * k + j])
-                if k + 2 < half or (k + 2 == half and mine):
-                    self.send(ref, recv.at[4 * (k + 2) + j], where)
-            if j == 1:
-                self.relay_pending()
-                if between is not None:
-                    between()
-        self.pending = fresh
+        own = self.at(0, self.y)
+        for k in range(self.stride, 0, -1):
+            self.up(own, k, k)
+            self.down(own, k, k)
+
+    def places(self, k):
+        if k == 0:
+            return (0,)
+        return (k, self.n_sp - k) if k < self.half else (k,)
+
+    def along_z(self, k):
+        ref = self.at(k, self.y)
+        self.arrived(ref, self.zp_sem.at[k])
+        self.up(ref, k + self.stride, self.stride)
+        if k < self.half:
+            ref = self.at(self.n_sp - k, self.y)
+            self.arrived(ref, self.zm_sem.at[k])
+            self.down(ref, k + self.stride, self.stride)
+
+    def along_y(self, k):
+        for o in self.places(k):
+            ref = self.at(o, self.y)
+            self.send(ref, self.yp_sem.at[o], self.to_yp)
+            self.send(ref, self.ym_sem.at[o], self.to_ym)
+
+    def relay(self, k):
+        for o in self.places(k):
+            low, high = self.at(o, self.ym), self.at(o, self.yp)
+            self.arrived(low, self.yp_sem.at[o])
+            if o % 2 == 0:
+                self.send(low, self.yo_sem.at[o], self.to_yp)
+            self.arrived(high, self.ym_sem.at[o])
+            if o % 2 == 1:
+                self.send(high, self.yo_sem.at[o], self.to_ym)
 
     def finish(self):
-        self.relay_pending()
         for o in range(self.n_sp):
-            self.arrived(self.b(self.back(o), self.yo), self.byo.at[o])
+            self.arrived(self.at(o, self.yo), self.yo_sem.at[o])
 
 
 def mixer_kernel(
@@ -159,13 +115,13 @@
     bias_in, rate_in, shift_in, tap_v_in, tap_k_in, tap_q_in, mgain_in, pmix_in, pgain_in,
     out,
     wo_2, wstep, gain, bias, rate, shift, tap_v, tap_k, tap_q, mgain, pmix, pgain, small_sem,
-    tokbuf, normbuf, wbuf, wout, gates, raw,
+    tokbuf, normbuf, wbuf, obuf, gates, raw,
     p32, xbuf, kbuf, qbuf, ends, ybuf, mix,
     incl, excl, itot, etot, msg_out, msg_in, ss_out, ss_in,
     d_out, d_in, r_out, r_in, n_out, n_in,
     local_sem, tp_sem, tm_sem, tr_sem, td_sem, h_sem, t_send,
-    w_ay, w_azp, w_azm, w_bzp, w_bzm, w_byp, w_bym, w_byo, w_send,
-    o_bzp, o_bzm, o_byp, o_bym, o_byo, o_send,
+    w_zp, w_zm, w_yp, w_ym, w_yo, w_send,
+    o_zp, o_zm, o_yp, o_ym, o_yo, o_send,
     msg_send, msg_recv, ss_send, ss_recv, d_send, d_recv, r_send, r_recv, n_send, n_recv,
 ):
     f32, bf16 = jnp.float32, jnp.bfloat16
@@ -179,12 +135,10 @@
     rows = N_BLOCKS * SPAN
 
     w_rings = Rings(
-        wbuf, (0, 128), (128, 512),
-        (w_ay, w_azp, w_azm, w_bzp, w_bzm, w_byp, w_bym, w_byo), w_send, (z, y), (n_sp, n_fs),
+        wbuf, (0, 256), 2, (w_zp, w_zm, w_yp, w_ym, w_yo), w_send, (z, y), (n_sp, n_fs)
     )
     o_rings = Rings(
-        wout, None, (0, 256),
-        (None, None, None, o_bzp, o_bzm, o_byp, o_bym, o_byo), o_send, (z, y), (n_sp, n_fs),
+        obuf, (0, 640), 2, (o_zp, o_zm, o_yp, o_ym, o_yo), o_send, (z, y), (n_sp, n_fs)
     )
 
     def t_at(xx, cc, q=0, count=PIECE):
@@ -192,9 +146,12 @@
         return tokbuf.at[pl.ds(row, count), :]
 
     own_row = pl.ds(pl.multiple_of((z * n_fs + y) * PIECE, PIECE), PIECE)
+    shards = (
+        (wv, wbuf, 0), (wk, wbuf, 1), (wg, obuf, 0), (wq, obuf, 1), (wp, obuf, 2)
+    )
     locals_ = [
-        pltpu.make_async_copy(w, wbuf.at[own_row, pl.ds(i * 128, 128)], local_sem.at[i])
-        for i, w in enumerate((wg, wv, wk, wq, wp))
+        pltpu.make_async_copy(w, buf.at[own_row, pl.ds(i * 128, 128)], local_sem.at[n])
+        for n, (w, buf, i) in enumerate(shards)
     ]
     locals_.append(pltpu.make_async_copy(tok.at[0], t_at(x, c, 0, TOK_ROWS), local_sem.at[5]))
     lane0 = pl.multiple_of(t * 128, 128)
@@ -216,11 +173,18 @@
 
     barrier = pltpu.get_barrier_semaphore()
     partners = [
-        to_xp, to_xm, to_d, to_zp, to_zm, w_rings.to_zpp, w_rings.to_zmm,
+        to_xp, to_xm, to_d, to_zp, to_zm, {"sp": (z + 2) % n_sp}, {"sp": (z + n_sp - 2) % n_sp},
         w_rings.to_yp, w_rings.to_ym,
     ]
     for where in partners:
         pl.semaphore_signal(barrier, inc=1, device_id=where, device_id_type=MESH)
+    for copy in small:
+        copy.wait()
+    for i in (0, 1):
+        turned = jnp.concatenate([wo_2[i].astype(f32), jnp.zeros((128, 96), f32)], axis=1).T
+        begin = 384 + i * 128
+        obuf[own_row, begin : begin + 128] = turned[0:PIECE, :].astype(bf16)
+    wbuf[:, 256:384] = jnp.concatenate([wstep[...], jnp.zeros((2048, 124), bf16)], axis=1)
     pl.semaphore_wait(barrier, len(partners))
 
     t_sent = []
@@ -283,47 +247,50 @@
     for q in (2, 3, 0, 1):
         t_go(t_at(x, c, q), t_at(x, c, q), tm_sem.at[q], to_xm)
     t_go(t_at(x, c, 0, TOK_ROWS), t_at(x, c, 0, TOK_ROWS), td_sem.at[12], to_d)
-    w_rings.spread()
-    for copy in small:
-        copy.wait()
-    for i in (0, 1):
-        turned = jnp.concatenate([wo_2[i].astype(f32), jnp.zeros((128, 96), f32)], axis=1).T
-        wout[own_row, i * 128 : (i + 1) * 128] = turned[0:PIECE, :].astype(bf16)
-    wbuf[:, 640:768] = jnp.concatenate([wstep[...], jnp.zeros((2048, 124), bf16)], axis=1)
-    for k in range(1, n_sp // 2 + 1):
-        w_rings.step(k, functools.partial(token_step, k))
+    w_rings.along_y(0)
+    o_rings.begin()
+    steps_z = n_sp // 2
+    for k in range(1, steps_z + 1):
+        w_rings.along_z(k)
+        w_rings.along_y(k)
+        w_rings.relay(k - 1)
+        token_step(k)
+        if k > 1:
+            o_rings.along_z(k - 1)
+        if k > 1:
+            o_rings.along_y(k - 2)
     for q in range(4):
         t_came(t_at(xo, cs, q), td_sem.at[8 + q])
     before, after = tokbuf.at[pl.ds(0, HALO), :], tokbuf.at[pl.ds(HALO + rows, HALO), :]
     t_go(tokbuf.at[pl.ds(rows, HALO), :], before, h_sem.at[0], to_zp)
     t_go(tokbuf.at[pl.ds(HALO, HALO), :], after, h_sem.at[1], to_zm)
-    w_rings.relay_pending()
-    o_rings.begin()
+    w_rings.relay(steps_z)
     norm_block(xo, cs)
+    o_rings.along_z(steps_z)
     w_rings.finish()
+    for k in range(7, steps_z + 1):
+        o_rings.along_y(k)
 
     def rounded(v):
         return v.astype(bf16).astype(f32)
 
-    def project(i):
+    def dots(at, count, rhs):
+        return jnp.dot(normbuf[at : at + count, :], rhs, preferred_element_type=f32)
+
+    for i in range(4):
         at = HALO + i * 256
-        dots = jnp.dot(normbuf[at : at + 256, :], wbuf[...], preferred_element_type=f32)
-        gates[i * 256 : (i + 1) * 256, :] = dots[:, 0:128].astype(bf16)
-        p32[at : at + 256, :] = rounded(dots[:, 128:640])
-        raw[i * 256 : (i + 1) * 256, :] = dots[:, 640:768]
-
-    project(0)
-    project(1)
-    project(2)
-    project(3)
+        found = dots(at, 256, wbuf[...])
+        p32[at : at + 256, 0:256] = rounded(found[:, 0:256])
+        raw[i * 256 : (i + 1) * 256, :] = found[:, 256:384]
+    edges = ((0, z > 0), (HALO + rows, z < n_sp - 1))
     t_came(before, h_sem.at[0])
     t_came(after, h_sem.at[1])
-    for begin, real in ((0, z > 0), (HALO + rows, z < n_sp - 1)):
+    for begin, real in edges:
         norm_rows(begin, HALO)
-        edge = jnp.dot(
-            normbuf[begin : begin + HALO, :], wbuf[:, 128:640], preferred_element_type=f32
-        )
-        p32[begin : begin + HALO, :] = jnp.where(real, rounded(edge), 0.0)
+        edge = dots(begin, HALO, wbuf[:, 0:256])
+        p32[begin : begin + HALO, 0:256] = jnp.where(real, rounded(edge), 0.0)
+    for k in range(3):
+        o_rings.relay(k)
 
     row8 = lax.broadcasted_iota(jnp.int32, (8, 128), 0)
 
@@ -499,28 +466,28 @@
 
     exchange(0, 0)
     exchange(0, 1)
-    o_rings.step(1)
-    o_rings.step(2)
-    within(0)
-    within(1)
+    o_rings.relay(3)
+    o_rings.relay(4)
     turn(0)
-    o_rings.step(3)
-    o_rings.step(4)
-    within(2)
-    within(3)
+    o_rings.relay(5)
+    o_rings.relay(6)
     turn(1)
-    o_rings.step(5)
-    o_rings.step(6)
-    within(4)
-    within(5)
-    within(6)
-    within(7)
+    o_rings.relay(7)
+    o_rings.relay(8)
+    o_rings.finish()
     turn(2)
-    o_rings.step(7)
-    o_rings.step(8)
+    for i in range(4):
+        at = HALO + i * 256
+        found = dots(at, 256, obuf[:, 0:384])
+        gates[i * 256 : (i + 1) * 256, :] = found[:, 0:128].astype(bf16)
+        p32[at : at + 256, 256:512] = rounded(found[:, 128:384])
+    for begin, real in edges:
+        edge = dots(begin, HALO, obuf[:, 128:384])
+        p32[begin : begin + HALO, 256:512] = jnp.where(real, rounded(edge), 0.0)
+    for b in range(N_BLOCKS):
+        within(b)
     for b in range(N_BLOCKS):
         pool(b)
-    o_rings.finish()
     turn(3)
 
     forward, backward = excl[0], excl[1]
@@ -532,7 +499,7 @@
         leaving[b] = backward.astype(bf16)
         forward = forward * tall(decay, i, 0) + ends[i, 0:128, :]
         backward = backward * tall(decay, b, 2) + ends[b, 128:256, :]
-    squares = []
+    squares = jnp.zeros((128, 128), f32)
     for b in range(N_BLOCKS):
         at = slice(b * SPAN, (b + 1) * SPAN)
         states = jnp.concatenate([entering[b], leaving[b]], axis=0)
@@ -544,13 +511,9 @@
         )
         gated = heads_out * silu(gates[at, :].astype(f32))
         ybuf[at, :] = gated
-        squares.append(
-            lax.dot_general(
-                jnp.ones((8, 128), f32), gated * gated, NT,
-                precision=HIGHEST, preferred_element_type=f32,
-            )[0:1, :]
-        )
-    own_squares = jnp.concatenate(squares, axis=0)
+        summed = jnp.sum(gated * gated, axis=1, keepdims=True)
+        squares = jnp.where(col == b, summed, squares)
+    own_squares = squares.T[0:8, :]
     ss_out[...] = own_squares
     ss_copies = []
     for r in range(1, n_tp):
@@ -574,7 +537,7 @@
     def partial(xx, cc, begin=0, count=TOK_ROWS):
         at = pl.multiple_of((xx * 2 + cc) * TOK_ROWS + begin, 16)
         return lax.dot_general(
-            mix[pl.ds(at, count), :], wout[...], NT, preferred_element_type=f32
+            mix[pl.ds(at, count), :], obuf[:, 384:640], NT, preferred_element_type=f32
         )
 
     half = TOK_ROWS // 2
@@ -633,7 +596,7 @@
 
 
 N_TOKEN_SENDS = 27
-N_RING_SENDS = 127
+N_RING_SENDS = 66
 
 
 def mixer(n_sp, n_fs, n_x, *operands):
@@ -668,8 +631,8 @@
             dma((13,)),
             pltpu.VMEM((rows + 2 * HALO, 2048), bf16),
             pltpu.VMEM((rows + 2 * HALO, 2048), bf16),
-            pltpu.VMEM((2048, 768), bf16),
-            pltpu.VMEM((2048, 256), bf16),
+            pltpu.VMEM((2048, 384), bf16),
+            pltpu.VMEM((2048, 640), bf16),
             pltpu.VMEM((rows, 128), bf16),
             pltpu.VMEM((rows, 128), f32),
             pltpu.VMEM((rows + 2 * HALO, 512), f32),
@@ -695,7 +658,7 @@
             pltpu.VMEM((4, half, 2048), bf16),
             dma((6,)), dma((4,)), dma((4,)), dma((4,)), dma((13,)), dma((2,)),
             dma((N_TOKEN_SENDS,)),
-            *ring_sems((3, 36, 36, 9, 9, 16, 16, 16, N_RING_SENDS)),
+            *ring_sems((9, 9, 16, 16, 16, N_RING_SENDS)),
             *ring_sems((9, 9, 16, 16, 16, N_RING_SENDS)),
             dma((2, 2, 4)), dma((2, 2, 4)), dma((7,)), dma((7,)),
             dma((4,)), dma((4,)), dma((2,)), dma((2,)), dma((4,)), dma((4,)),

time: 115 us -> 110 us (0.957)
  Pallas kernels: 109 us -> 104 us
    pallas_call x1, Pallas kernels: 109 us -> 104 us  [mixer(): pl.pallas_call(functools.partial(mixer_kernel, n_sp, n_fs, n_x), out_shap...]
where the time goes in v5:
time: 110 us
  Pallas kernels  104 us (95%)
  local copies, waits for them, and re-layouts  6 us (5%)
    pallas_call x1, Pallas kernels, mixer(): pl.pallas_call(functools.partial(mixer_kernel, n_sp, n_fs, n_x), out_shap...  104 us
    unnamed x9, local copies, waits for them, and re-layouts  4.91 us

profile of v5, /device:TPU:1, one launch (start us, length us, event | category | flops | bytes accessed | tf_op | source)
XLA Modules:
  0.0 109.9 jit_solution(5430411528684015632)
XLA Ops:
  0.0 0.0 copy-start
  0.0 0.9 copy-done
  0.9 0.0 copy-start.1
  1.0 0.7 copy-done.1
  1.6 0.0 copy-start.2
  1.6 0.7 copy.23.wo_s
  2.4 0.0 copy-done.2
  2.4 0.7 copy.24.wo_p
  3.1 1.1 copy.25.wstep_in
  4.1 103.9 %mixer.1 = bf16[1,128,2048]{2,1,0:T(8,128)(2,1)} custom-call(bf16[1,128,2048]{2,1,0:T(8,128)(2,1)} %tok.1, bf16[32,128]{1,0:T(8,128)(2,1)} %wg.1, bf16[32,128]{1,0:T(8,128)(2,1)} %wv.1, bf16[32,128]{1,0:T(8,128)(2,1)} %wk.1, bf16[32,128]{1,0:T(8,128)(2,1)} %wq.1, bf16[32,128]{1,0:T(8,128)(2,1)} %wp.1, bf16[128,32]{1,0:T(8,128)(2,1)} %copy.23.wo_s, ...), custom_call_target="tpu_custom_call" | custom-call | tf_op jit(solution)/shard_map/mixer/pallas_call | solution.py:613
  108.1 1.9 %copy.27 = bf16[1,128,2048]{2,1,0:T(8,128)(2,1)} copy(bf16[1,128,2048]{2,1,0:T(8,128)(2,1)} %mixer.1) | data formatting | bytes 1048576
  (2 shorter events, 0.0 us)
Async XLA Ops:
  0.0 0.9 copy-start
  0.9 0.7 copy-start.1
  1.6 0.7 copy-start.2

commit v6 on v5

--- a/solution.py
+++ b/solution.py
@@ -7,7 +7,6 @@
 from jax.experimental.pallas import tpu as pltpu
 from jax.sharding import PartitionSpec as P
 
-DUALITY_HEADS = 16
 STATE = 128
 SPAN = 128
 D_SSM = 1024
@@ -114,10 +113,10 @@
     tok, wg, wv, wk, wq, wp, wo_s, wo_p, wstep_in, gain_in,
     bias_in, rate_in, shift_in, tap_v_in, tap_k_in, tap_q_in, mgain_in, pmix_in, pgain_in,
     out,
-    wo_2, wstep, gain, bias, rate, shift, tap_v, tap_k, tap_q, mgain, pmix, pgain, small_sem,
+    wstep, raw_t, gain, bias, rate, shift, tap_v, tap_k, tap_q, mgain, pmix, pgain, small_sem,
     tokbuf, normbuf, wbuf, obuf, gates, raw,
     p32, xbuf, kbuf, qbuf, ends, ybuf, mix,
-    incl, excl, itot, etot, msg_out, msg_in, ss_out, ss_in,
+    incl, excl, itot, etot, msg_out, msg_in, ss_out, ss_in, part_s, part_p, scales,
     d_out, d_in, r_out, r_in, n_out, n_in,
     local_sem, tp_sem, tm_sem, tr_sem, td_sem, h_sem, t_send,
     w_zp, w_zm, w_yp, w_ym, w_yo, w_send,
@@ -147,20 +146,21 @@
 
     own_row = pl.ds(pl.multiple_of((z * n_fs + y) * PIECE, PIECE), PIECE)
     shards = (
-        (wv, wbuf, 0), (wk, wbuf, 1), (wg, obuf, 0), (wq, obuf, 1), (wp, obuf, 2)
+        (wv, wbuf, 0), (wk, wbuf, 1), (wg, obuf, 0), (wq, obuf, 1), (wp, obuf, 2),
+        (wo_s, obuf, 3), (wo_p, obuf, 4),
     )
     locals_ = [
         pltpu.make_async_copy(w, buf.at[own_row, pl.ds(i * 128, 128)], local_sem.at[n])
         for n, (w, buf, i) in enumerate(shards)
     ]
-    locals_.append(pltpu.make_async_copy(tok.at[0], t_at(x, c, 0, TOK_ROWS), local_sem.at[5]))
+    locals_.append(pltpu.make_async_copy(tok.at[0], t_at(x, c, 0, TOK_ROWS), local_sem.at[7]))
     lane0 = pl.multiple_of(t * 128, 128)
     here = pl.ds(lane0, 128)
     small = [
         pltpu.make_async_copy(src, dst, small_sem.at[i])
         for i, (src, dst) in enumerate(
             (
-                (gain_in, gain), (wo_s, wo_2.at[0]), (wo_p, wo_2.at[1]), (wstep_in, wstep),
+                (gain_in, gain), (wstep_in, wstep),
                 (bias_in, bias), (rate_in, rate), (shift_in, shift),
                 (tap_v_in.at[:, here], tap_v), (tap_k_in.at[:, here], tap_k),
                 (tap_q_in.at[:, here], tap_q), (mgain_in.at[:, here], mgain),
@@ -180,11 +180,6 @@
         pl.semaphore_signal(barrier, inc=1, device_id=where, device_id_type=MESH)
     for copy in small:
         copy.wait()
-    for i in (0, 1):
-        turned = jnp.concatenate([wo_2[i].astype(f32), jnp.zeros((128, 96), f32)], axis=1).T
-        begin = 384 + i * 128
-        obuf[own_row, begin : begin + 128] = turned[0:PIECE, :].astype(bf16)
-    wbuf[:, 256:384] = jnp.concatenate([wstep[...], jnp.zeros((2048, 124), bf16)], axis=1)
     pl.semaphore_wait(barrier, len(partners))
 
     t_sent = []
@@ -238,10 +233,10 @@
         else:
             norm_block(xo, c)
 
-    for copy in locals_[:5]:
+    for copy in locals_[:7]:
         copy.wait()
     w_rings.begin()
-    locals_[5].wait()
+    locals_[7].wait()
     for q in (0, 1, 2, 3):
         t_go(t_at(x, c, q), t_at(x, c, q), tp_sem.at[q], to_xp)
     for q in (2, 3, 0, 1):
@@ -249,6 +244,10 @@
     t_go(t_at(x, c, 0, TOK_ROWS), t_at(x, c, 0, TOK_ROWS), td_sem.at[12], to_d)
     w_rings.along_y(0)
     o_rings.begin()
+    for i in range(16):
+        cols = [wstep[r, :, i * 128 : (i + 1) * 128].astype(f32) for r in (0, 1)]
+        tall_cols = jnp.concatenate([*cols, jnp.zeros((96, 128), f32)], axis=0).T
+        wbuf[i * 128 : (i + 1) * 128, 256:384] = tall_cols.astype(bf16)
     steps_z = n_sp // 2
     for k in range(1, steps_z + 1):
         w_rings.along_z(k)
@@ -305,7 +304,8 @@
     rate8 = by_kind([rate[r, 2 * t + h] for r, h in kinds])
     steps_l, logs_l = [], []
     for b in range(N_BLOCKS):
-        cols = raw[b * SPAN : (b + 1) * SPAN, :].T[0:8, :] + bias8
+        raw_t[b] = raw[b * SPAN : (b + 1) * SPAN, :].T[0:32, :]
+        cols = by_kind([raw_t[b, pl.ds(r * 16 + 2 * t + h, 1), :] for r, h in kinds]) + bias8
         steps = jnp.maximum(cols, 0.0) + jnp.log1p(jnp.exp(-jnp.abs(cols)))
         moved = by_kind([shift[0, h, r : r + 1, b * SPAN : (b + 1) * SPAN] for r, h in kinds])
         steps_l.append(steps)
@@ -488,6 +488,12 @@
         within(b)
     for b in range(N_BLOCKS):
         pool(b)
+    order = (xo, xp, xm, x)
+    for i, xx in enumerate(order):
+        pair = pl.ds(pl.multiple_of(xx * 2 * TOK_ROWS, 2 * TOK_ROWS), 2 * TOK_ROWS)
+        part_p[i] = lax.dot_general(
+            mix[pair, 128:256], obuf[:, 512:640], NT, preferred_element_type=f32
+        )
     turn(3)
 
     forward, backward = excl[0], excl[1]
@@ -510,7 +516,7 @@
             + carried[:, 128:256] * wide(reach_t, b, 2)
         )
         gated = heads_out * silu(gates[at, :].astype(f32))
-        ybuf[at, :] = gated
+        mix[at, 0:128] = (gated * mgain[...]).astype(bf16)
         summed = jnp.sum(gated * gated, axis=1, keepdims=True)
         squares = jnp.where(col == b, summed, squares)
     own_squares = squares.T[0:8, :]
@@ -523,33 +529,36 @@
         )
         copy.start()
         ss_copies.append(copy)
+    for i, xx in enumerate(order):
+        pair = pl.ds(pl.multiple_of(xx * 2 * TOK_ROWS, 2 * TOK_ROWS), 2 * TOK_ROWS)
+        part_s[i] = lax.dot_general(
+            mix[pair, 0:128], obuf[:, 384:512], NT, preferred_element_type=f32
+        )
     all_squares = own_squares
     for r in range(1, n_tp):
         ss_copies[r - 1].wait_recv()
         all_squares = all_squares + ss_in[r - 1]
     scale = lax.rsqrt(all_squares / D_SSM + EPSILON)
     scale_t = jnp.concatenate([scale, jnp.zeros((120, 128), f32)], axis=0).T
-    mix_gain_here = mgain[...]
     for b in range(N_BLOCKS):
-        at = slice(b * SPAN, (b + 1) * SPAN)
-        mix[at, 0:128] = (ybuf[at, :] * scale_t[:, b : b + 1] * mix_gain_here).astype(bf16)
-
-    def partial(xx, cc, begin=0, count=TOK_ROWS):
-        at = pl.multiple_of((xx * 2 + cc) * TOK_ROWS + begin, 16)
-        return lax.dot_general(
-            mix[pl.ds(at, count), :], obuf[:, 384:640], NT, preferred_element_type=f32
-        )
+        scales[b * SPAN : (b + 1) * SPAN, :] = jnp.broadcast_to(scale_t[:, b : b + 1], (128, 128))
+
+    def partial(i, cc, begin=0, count=TOK_ROWS):
+        at = pl.multiple_of(cc * TOK_ROWS + begin, 16)
+        there = pl.multiple_of(order[i] * 2 * TOK_ROWS + at, 16)
+        scaling = scales[pl.ds(there, count), :][:, 0:1]
+        return part_s[i, pl.ds(at, count), :] * scaling + part_p[i, pl.ds(at, count), :]
 
     half = TOK_ROWS // 2
     d_copies = []
-    for i, xx in enumerate((xo, xp, xm, x)):
-        d_out[i] = partial(xx, 1 - c).astype(bf16)
+    for i in range(4):
+        d_out[i] = partial(i, 1 - c).astype(bf16)
         copy = remote(d_out.at[i], d_in.at[i], d_send.at[i], d_recv.at[i], to_d)
         copy.start()
         d_copies.append(copy)
 
-    def chip(i, xx, begin, count=half):
-        return partial(xx, c, begin, count) + d_in[i, begin : begin + count, :].astype(f32)
+    def chip(i, begin, count=half):
+        return partial(i, c, begin, count) + d_in[i, begin : begin + count, :].astype(f32)
 
     def send(i, value, where, out_ref, in_ref, send_sem, recv_sem):
         out_ref[i] = value.astype(bf16)
@@ -560,18 +569,18 @@
     relay = (r_out, r_in, r_send, r_recv)
     near = (n_out, n_in, n_send, n_recv)
     d_copies[0].wait_recv()
-    relay_p = send(0, chip(0, xo, 0), to_xp, *relay)
-    relay_m = send(1, chip(0, xo, half), to_xm, *relay)
+    relay_p = send(0, chip(0, 0), to_xp, *relay)
+    relay_m = send(1, chip(0, half), to_xm, *relay)
     d_copies[1].wait_recv()
-    dir_p = send(0, chip(1, xp, half), to_xp, *near)
+    dir_p = send(0, chip(1, half), to_xp, *near)
     d_copies[2].wait_recv()
-    dir_m = send(1, chip(2, xm, 0), to_xm, *near)
+    dir_m = send(1, chip(2, 0), to_xm, *near)
     relay_p.wait_recv()
-    comb_p = send(2, chip(1, xp, 0) + r_in[0].astype(f32), to_xp, *near)
+    comb_p = send(2, chip(1, 0) + r_in[0].astype(f32), to_xp, *near)
     relay_m.wait_recv()
-    comb_m = send(3, chip(2, xm, half) + r_in[1].astype(f32), to_xm, *near)
+    comb_m = send(3, chip(2, half) + r_in[1].astype(f32), to_xm, *near)
     d_copies[3].wait_recv()
-    top, bottom = chip(3, x, 0), chip(3, x, half)
+    top, bottom = chip(3, 0), chip(3, half)
     dir_p.wait_recv()
     dir_m.wait_recv()
     bottom = bottom + n_in[0].astype(f32)
@@ -616,8 +625,8 @@
         in_specs=[any_spec] * 19,
         out_specs=vmem,
         scratch_shapes=[
-            pltpu.VMEM((2, 128, 32), bf16),
-            pltpu.VMEM((2048, 4), bf16),
+            pltpu.VMEM((2, 16, 2048), bf16),
+            pltpu.VMEM((N_BLOCKS, 32, 128), f32),
             pltpu.VMEM((1, 2048), f32),
             pltpu.SMEM((2, 16), f32),
             pltpu.SMEM((2, 16), f32),
@@ -628,7 +637,7 @@
             pltpu.VMEM((1, 128), f32),
             pltpu.VMEM((128, 128), bf16),
             pltpu.VMEM((1, 128), f32),
-            dma((13,)),
+            dma((11,)),
             pltpu.VMEM((rows + 2 * HALO, 2048), bf16),
             pltpu.VMEM((rows + 2 * HALO, 2048), bf16),
             pltpu.VMEM((2048, 384), bf16),
@@ -650,13 +659,16 @@
             pltpu.VMEM((2, 2, 4, MSG, 128), bf16),
             pltpu.VMEM((8, 128), f32),
             pltpu.VMEM((7, 8, 128), f32),
+            pltpu.VMEM((4, 2 * TOK_ROWS, 2048), f32),
+            pltpu.VMEM((4, 2 * TOK_ROWS, 2048), f32),
+            pltpu.VMEM((rows, 128), f32),
             pltpu.VMEM((4, TOK_ROWS, 2048), bf16),
             pltpu.VMEM((4, TOK_ROWS, 2048), bf16),
             pltpu.VMEM((2, half, 2048), bf16),
             pltpu.VMEM((2, half, 2048), bf16),
             pltpu.VMEM((4, half, 2048), bf16),
             pltpu.VMEM((4, half, 2048), bf16),
-            dma((6,)), dma((4,)), dma((4,)), dma((4,)), dma((13,)), dma((2,)),
+            dma((8,)), dma((4,)), dma((4,)), dma((4,)), dma((13,)), dma((2,)),
             dma((N_TOKEN_SENDS,)),
             *ring_sems((9, 9, 16, 16, 16, N_RING_SENDS)),
             *ring_sems((9, 9, 16, 16, 16, N_RING_SENDS)),
@@ -676,12 +688,9 @@
     w_out_ssd, w_out_pool,
 ):
     n_tp, n_sp, n_fs = lax.axis_size("tp"), lax.axis_size("sp"), lax.axis_size("fs")
-    heads_dev = DUALITY_HEADS // n_tp
-    step_cols = lax.dynamic_slice_in_dim(w_step, lax.axis_index("tp") * heads_dev, heads_dev, 2)
-    step_cols = step_cols.reshape(w_step.shape[0], 2 * heads_dev)
     return mixer(
         n_sp, n_fs, n_tp // 2, tokens, w_gate, w_value, w_bkey, w_query, w_pool_in,
-        w_out_ssd, w_out_pool, step_cols, norm_gain[None], step_bias, decay_rate, decay_shift,
+        w_out_ssd.T, w_out_pool.T, w_step.transpose(1, 2, 0), norm_gain[None], step_bias, decay_rate, decay_shift,
         conv_value, conv_bkey, conv_query, mix_gain[None], pool_mix, pool_gain[None],
     )
 

time: 110 us -> 105 us (0.955)
  local copies, waits for them, and re-layouts: 6 us -> 1.88 us
    unnamed x9 -> x1, local copies, waits for them, and re-layouts: 4.91 us -> 1.88 us
where the time goes in v6:
time: 105 us
  Pallas kernels  103 us (98%)
  local copies, waits for them, and re-layouts  1.88 us (2%)
    pallas_call x1, Pallas kernels, mixer(): pl.pallas_call(functools.partial(mixer_kernel, n_sp, n_fs, n_x), out_shap...  103 us

profile of v6, /device:TPU:1, one launch (start us, length us, event | category | flops | bytes accessed | tf_op | source)
XLA Modules:
  0.0 105.2 jit_solution(1090116818539466469)
XLA Ops:
  0.0 103.3 %mixer.1 = bf16[1,128,2048]{2,1,0:T(8,128)(2,1)} custom-call(bf16[1,128,2048]{2,1,0:T(8,128)(2,1)} %tok.1, bf16[32,128]{1,0:T(8,128)(2,1)} %wg.1, bf16[32,128]{1,0:T(8,128)(2,1)} %wv.1, bf16[32,128]{1,0:T(8,128)(2,1)} %wk.1, bf16[32,128]{1,0:T(8,128)(2,1)} %wq.1, bf16[32,128]{1,0:T(8,128)(2,1)} %wp.1, bf16[32,128]{1,0:T(8,128)(2,1)} %bitcast.7, ...), custom_call_target="tpu_custom_call" | custom-call | tf_op jit(solution)/shard_map/mixer/pallas_call | solution.py:622
  103.4 1.9 %copy.21 = bf16[1,128,2048]{2,1,0:T(8,128)(2,1)} copy(bf16[1,128,2048]{2,1,0:T(8,128)(2,1)} %mixer.1) | data formatting | bytes 1048576

commit v7 on v6

--- a/solution.py
+++ b/solution.py
@@ -258,29 +258,33 @@
             o_rings.along_z(k - 1)
         if k > 1:
             o_rings.along_y(k - 2)
+    def rounded(v):
+        return v.astype(bf16).astype(f32)
+
+    def dots(at, count, rhs):
+        return jnp.dot(normbuf[pl.ds(at, count), :], rhs, preferred_element_type=f32)
+
+    def project(xx):
+        at = pl.multiple_of(xx * 256, 256)
+        found = dots(pl.multiple_of(HALO + at, 16), 256, wbuf[...])
+        p32[pl.ds(pl.multiple_of(HALO + at, 16), 256), 0:256] = rounded(found[:, 0:256])
+        raw[pl.ds(at, 256), :] = found[:, 256:384]
+
+    w_rings.relay(steps_z)
+    o_rings.along_z(steps_z)
     for q in range(4):
         t_came(t_at(xo, cs, q), td_sem.at[8 + q])
     before, after = tokbuf.at[pl.ds(0, HALO), :], tokbuf.at[pl.ds(HALO + rows, HALO), :]
     t_go(tokbuf.at[pl.ds(rows, HALO), :], before, h_sem.at[0], to_zp)
     t_go(tokbuf.at[pl.ds(HALO, HALO), :], after, h_sem.at[1], to_zm)
-    w_rings.relay(steps_z)
+    w_rings.finish()
+    for xx in (x, xm, xp):
+        project(xx)
     norm_block(xo, cs)
-    o_rings.along_z(steps_z)
-    w_rings.finish()
     for k in range(7, steps_z + 1):
         o_rings.along_y(k)
 
-    def rounded(v):
-        return v.astype(bf16).astype(f32)
-
-    def dots(at, count, rhs):
-        return jnp.dot(normbuf[at : at + count, :], rhs, preferred_element_type=f32)
-
-    for i in range(4):
-        at = HALO + i * 256
-        found = dots(at, 256, wbuf[...])
-        p32[at : at + 256, 0:256] = rounded(found[:, 0:256])
-        raw[i * 256 : (i + 1) * 256, :] = found[:, 256:384]
+    project(xo)
     edges = ((0, z > 0), (HALO + rows, z < n_sp - 1))
     t_came(before, h_sem.at[0])
     t_came(after, h_sem.at[1])

time: 105 us -> 106 us (level)
  no operation moved by 1% of the time
where the time goes in v7:
time: 106 us
  Pallas kernels  104 us (98%)
  local copies, waits for them, and re-layouts  1.88 us (2%)
    pallas_call x1, Pallas kernels, mixer(): pl.pallas_call(functools.partial(mixer_kernel, n_sp, n_fs, n_x), out_shap...  104 us

profile of v7, /device:TPU:1, one launch (start us, length us, event | category | flops | bytes accessed | tf_op | source)
XLA Modules:
  0.0 105.8 jit_solution(15831195090307988511)
XLA Ops:
  0.0 103.9 %mixer.1 = bf16[1,128,2048]{2,1,0:T(8,128)(2,1)} custom-call(bf16[1,128,2048]{2,1,0:T(8,128)(2,1)} %tok.1, bf16[32,128]{1,0:T(8,128)(2,1)} %wg.1, bf16[32,128]{1,0:T(8,128)(2,1)} %wv.1, bf16[32,128]{1,0:T(8,128)(2,1)} %wk.1, bf16[32,128]{1,0:T(8,128)(2,1)} %wq.1, bf16[32,128]{1,0:T(8,128)(2,1)} %wp.1, bf16[32,128]{1,0:T(8,128)(2,1)} %bitcast.7, ...), custom_call_target="tpu_custom_call" | custom-call | tf_op jit(solution)/shard_map/mixer/pallas_call | solution.py:626
  103.9 1.9 %copy.21 = bf16[1,128,2048]{2,1,0:T(8,128)(2,1)} copy(bf16[1,128,2048]{2,1,0:T(8,128)(2,1)} %mixer.1) | data formatting | bytes 1048576
